TPU v7x, 512 devices: a whole 4x4x16 slice. The times are simulated.
512 devices in a mesh: kv: 32 (over z, core), tp: 16 (over y, x).
Axes of the slice: x: 4, y: 4, z: 16, core: 2. Of those that a mesh axis runs over, the one named last changes fastest.
Arguments:
- tokens: bfloat16 [512, 4096], P(None, 'kv'), may hold values from -40 to 40
- gain_first: float32 [4096], P('kv'), may hold values from 0.1 to 1.9
- gate_first: bfloat16 [4096, 11008], P('kv', 'tp'), may hold values from -0.09375 to 0.09375
- up_first: bfloat16 [4096, 11008], P('kv', 'tp'), may hold values from -0.09375 to 0.09375
- down_first: bfloat16 [11008, 4096], P('tp', 'kv'), may hold values from -0.0546875 to 0.0546875
- gain_mix: float32 [4096], P('kv'), may hold values from 0.1 to 1.9
- w_query: bfloat16 [4096, 2048], P('kv', 'tp'), may hold values from -0.09375 to 0.09375
- w_key: bfloat16 [4096, 2048], P('kv', 'tp'), may hold values from -0.09375 to 0.09375
- w_value: bfloat16 [4096, 2048], P('kv', 'tp'), may hold values from -0.09375 to 0.09375
- w_outgate: bfloat16 [4096, 2048], P('kv', 'tp'), may hold values from -0.09375 to 0.09375
- w_ingate: bfloat16 [4096, 16], P('kv'), may hold values from -0.046875 to 0.046875
- w_forget: bfloat16 [4096, 16], P('kv'), may hold values from -0.09375 to 0.09375
- forget_bias: float32 [16], P('tp'), may hold values from -1 to 4
- memory: float32 [512, 16, 128, 128], P('kv', 'tp'), may hold values from -0.6 to 0.6
- normalizer: float32 [512, 16, 128], P('kv', 'tp'), may hold values from -0.6 to 0.6
- stabilizer: float32 [512, 16], P('kv', 'tp'), may hold values from -3 to 0.5
- w_project: bfloat16 [2048, 4096], P('tp', 'kv'), may hold values from -0.75 to 0.75
- gain_second: float32 [4096], P('kv'), may hold values from 0.3 to 3
- gate_second: bfloat16 [4096, 11008], P('kv', 'tp'), may hold values from -0.09375 to 0.09375
- up_second: bfloat16 [4096, 11008], P('kv', 'tp'), may hold values from -0.09375 to 0.09375
- down_second: bfloat16 [11008, 4096], P('tp', 'kv'), may hold values from -0.0546875 to 0.0546875
Outputs:
- mixed_out: bfloat16 [512, 4096], P(None, 'kv')
- memory_new: float32 [512, 16, 128, 128], P('kv', 'tp')
- normalizer_new: float32 [512, 16, 128], P('kv', 'tp')
- stabilizer_new: float32 [512, 16], P('kv', 'tp')
All inputs are finite; a program needn't handle non-finite values.
Results may differ from a plain program's by a relative error of at most 0.04.
Values may be sent and summed in bfloat16 or wider, within the bound.
No kernel may reach another device: no remote copies, remote signals or barrier semaphores. Data moves between devices by JAX's collectives and lax.ppermute only.
A program may use at most 64 MiB of HBM per device.

v0:
```python
import jax
import jax.numpy as jnp
from jax import lax
from jax.experimental import pallas as pl
from jax.experimental.pallas import tpu as pltpu
from jax.sharding import Mesh
from jax.sharding import PartitionSpec as P


D = 4096
EPSILON = 1e-06
NP = 2
KV = ("zq", "zp", "c")
BF = jnp.bfloat16
F32 = jnp.float32
FFL = 688
HEAD = 640
TAIL = 48
WIDE = 1408
MIX = 640
NT_DIMS = (((1,), (1,)), ((), ()))


def swap(array):
    return lax.ppermute(array, "zp", [(0, 1), (1, 0)])


def both_cores(array):
    return lax.all_gather(array, "c")


def exchange(parts, axis):
    return lax.all_to_all(parts, axis, split_axis=0, concat_axis=0, tiled=True)


def pieces(gain):
    hi = gain.astype(BF)
    rest = gain - hi.astype(F32)
    mid = rest.astype(BF)
    low = (rest - mid.astype(F32)).astype(BF)
    return [hi, mid, low]


def gate_up(gate, up):
    return [
        (gate, 0, HEAD),
        (up, 0, HEAD),
        (gate, HEAD, TAIL),
        (gate, 0, 64 - TAIL),
        (up, HEAD, TAIL),
        (up, 0, 64 - TAIL),
    ]


def scaled_rows(x_ref, gain_ref):
    groups, rows, width = x_ref.shape
    x = x_ref[...].astype(F32).reshape(groups * rows, width)
    squares = jnp.sum(x * x, axis=1, keepdims=True)
    return (x * gain_ref[...]).astype(BF), squares


def put_squares(block, squares, at):
    hi = squares.astype(BF).astype(F32)
    low = squares - hi
    column = lax.broadcasted_iota(jnp.int32, block.shape, 1)
    return jnp.where(column == at, hi, jnp.where(column == at + 1, low, block))


def dot(a, b, dims=(((1,), (0,)), ((), ()))):
    return lax.dot_general(a, b, dims, preferred_element_type=F32)


def wide_kernel(x_ref, gain_ref, own_ref, other_ref, out_ref):
    scaled, squares = scaled_rows(x_ref, gain_ref)
    total = None
    for core in range(2):
        weight = jnp.concatenate([own_ref[core, :WIDE], other_ref[core, :WIDE]], axis=1)
        part = dot(scaled[:, 256 * core : 256 * (core + 1)], weight, NT_DIMS)
        total = part if total is None else total + part
    out_ref[:, : WIDE - 128] = total[:, : WIDE - 128].astype(BF)
    out_ref[:, WIDE - 128 :] = put_squares(total[:, WIDE - 128 :], squares, 112).astype(BF)


def prep_kernel(pair_ref, tokens_ref, first_ref, mix_ref, second_ref, kept_ref, sent_ref):
    gains = []
    for ref in (first_ref, mix_ref, second_ref):
        gains += pieces(ref[...])
    for ref, which in ((kept_ref, pair_ref[0]), (sent_ref, 1 - pair_ref[0])):
        for core in range(2):
            for group in range(8):
                at = 128 * core + 16 * group
                ref[at : at + 16] = tokens_ref[group, which, core]
        rows = [g.astype(F32) for g in gains] + [jnp.zeros((7, 128), F32)]
        ref[256:] = jnp.concatenate(rows, axis=0).astype(BF)


def pack_kernel(plan):
    def kernel(*refs):
        sources, out, sems = refs[:-2], refs[-2], refs[-1]
        started, at = [], 0
        for i, (source, start, count) in enumerate(plan):
            copy = pltpu.make_async_copy(
                sources[source].at[pl.ds(start, count)], out.at[pl.ds(at, count)], sems.at[i]
            )
            copy.start()
            started.append(copy)
            at += count
        for copy in started:
            copy.wait()

    return kernel


def pack(plan, *arrays):
    anywhere = pl.BlockSpec(memory_space=pl.ANY)
    return pl.pallas_call(
        pack_kernel(plan),
        in_specs=[pl.BlockSpec(memory_space=pltpu.HBM)] * len(arrays),
        out_specs=anywhere,
        out_shape=jax.ShapeDtypeStruct((sum(count for _, _, count in plan), 128), BF),
        scratch_shapes=[pltpu.SemaphoreType.DMA((len(plan),))],
        compiler_params=pltpu.CompilerParams(vmem_limit_bytes=2**20),
    )(*arrays)


def first_kernel(core_ref, kept_ref, came_ref, own_ref, other_ref, out_ref, rows_ref, gains_ref):
    start = pl.multiple_of(128 * core_ref[0], 128)
    total, squares = None, None
    for core in range(2):
        x, gain = [], []
        for chip, here_ref in enumerate((kept_ref, came_ref)):
            at = 128 * (2 * core + chip)
            block = here_ref[core, pl.ds(start, 128)]
            rows_ref[:, :, at : at + 128] = block.reshape(16, 8, 128)
            x.append(block.astype(F32))
            parts = here_ref[core, 256:].astype(F32)
            for i in range(3):
                whole = (parts[3 * i : 3 * i + 1] + parts[3 * i + 1 : 3 * i + 2]) + parts[
                    3 * i + 2 : 3 * i + 3
                ]
                gains_ref[i, :, at : at + 128] = whole
                if i == 0:
                    gain.append(whole)
        x, gain = jnp.concatenate(x, axis=1), jnp.concatenate(gain, axis=1)
        square = jnp.sum(x * x, axis=1, keepdims=True)
        squares = square if squares is None else squares + square
        weight = jnp.concatenate([own_ref[core, :WIDE], other_ref[core, :WIDE]], axis=1)
        part = dot((x * gain).astype(BF), weight, NT_DIMS)
        total = part if total is None else total + part
    out_ref[:, : WIDE - 128] = total[:, : WIDE - 128].astype(BF)
    out_ref[:, WIDE - 128 :] = put_squares(total[:, WIDE - 128 :], squares, 112).astype(BF)


def mix_kernel(x_ref, gain_ref, own_ref, other_ref, out_ref):
    scaled, squares = scaled_rows(x_ref, gain_ref)
    for pair in range(2):
        total = None
        for core in range(2):
            columns = [
                jnp.concatenate(
                    [own_ref[core, 128 * m : 128 * (m + 1)], other_ref[core, 128 * m : 128 * (m + 1)]],
                    axis=0,
                )
                for m in (2 * pair, 2 * pair + 1)
            ]
            part = dot(scaled[:, 256 * core : 256 * (core + 1)], jnp.concatenate(columns, axis=1))
            total = part if total is None else total + part
        out_ref[:, 256 * pair : 256 * (pair + 1)] = total.astype(BF)
    total = None
    for core in range(2):
        weight = jnp.concatenate([own_ref[core, 512:544], other_ref[core, 512:544]], axis=1)
        weight = jnp.concatenate([weight, jnp.zeros((128 - weight.shape[0], 256), BF)], axis=0)
        part = dot(scaled[:, 256 * core : 256 * (core + 1)], weight, NT_DIMS)
        total = part if total is None else total + part
    out_ref[:, 512:] = put_squares(total, squares, 112).astype(BF)


def act_kernel(x_ref, out_ref):
    total = x_ref[0].astype(F32)
    for i in range(1, x_ref.shape[0]):
        total = total + x_ref[i].astype(F32)
    last = total[:, WIDE - 128 :]
    scale = lax.rsqrt((last[:, 112:113] + last[:, 113:114]) / D + EPSILON)

    def act(gate, up):
        gate, up = scale * gate, scale * up
        return (gate * jax.nn.sigmoid(gate) * up).astype(BF)

    head = act(total[:, :HEAD], total[:, HEAD : 2 * HEAD])
    tail = act(last, pltpu.roll(last, 64, 1))[:, :TAIL]
    for i in range(out_ref.shape[0]):
        out_ref[i, :, :HEAD] = head
        out_ref[i, :, HEAD:] = tail


def out_kernel(spans):
    def kernel(x_ref, *refs):
        out_ref = refs[-1]
        groups, rows, width = x_ref.shape
        x = x_ref[...].reshape(groups * rows, width)
        for core in range(2):
            columns = []
            for chip in range(2):
                blocks = [
                    refs[2 * source + chip][core, start : start + count]
                    for source, start, count in spans
                ]
                columns.append(blocks[0] if len(blocks) == 1 else jnp.concatenate(blocks, axis=0))
            part = dot(x, jnp.concatenate(columns, axis=1)).astype(BF)
            out_ref[:, 256 * core : 256 * (core + 1)] = part

    return kernel


def residual_kernel(factor):
    def kernel(at_ref, sum_ref, old_ref, new_ref, copies_ref):
        total = sum_ref[0].astype(F32)
        for i in range(1, sum_ref.shape[0]):
            total = total + sum_ref[i].astype(F32)
        new = (old_ref[at_ref[0]].astype(F32) + factor * total).astype(BF)
        new_ref[0] = new
        for i in range(copies_ref.shape[0]):
            copies_ref[i] = new

    return kernel


def last_kernel(at_ref, sum_ref, old_ref, out_ref):
    total = sum_ref[0].astype(F32)
    for i in range(1, sum_ref.shape[0]):
        total = total + sum_ref[i].astype(F32)
    new = (old_ref[0].astype(F32) + 0.5 * total).astype(BF)
    first = at_ref[0] == 0
    for core in range(2):
        own = new[:, 256 * core : 256 * core + 128]
        other = new[:, 256 * core + 128 : 256 * (core + 1)]
        blocks = (jnp.where(first, own, other), jnp.where(first, other, own))
        for pair in range(2):
            for i in range(16):
                out_ref[(2 * pair + core) * 16 + i] = blocks[pair]


def call(kernel, out_shapes, scalars=0):
    smem = pl.BlockSpec(memory_space=pltpu.SMEM)
    vmem = pl.BlockSpec(memory_space=pltpu.VMEM)

    def run(*args):
        return pl.pallas_call(
            kernel,
            in_specs=[smem] * scalars + [vmem] * (len(args) - scalars),
            out_specs=jax.tree.map(lambda s: vmem, out_shapes),
            out_shape=out_shapes,
            compiler_params=pltpu.CompilerParams(vmem_limit_bytes=12 * 2**20),
        )(*args)

    return run


def half_step(wide, down):
    came = exchange(wide.reshape(8, 16, WIDE), "zq")
    hidden = call(act_kernel, jax.ShapeDtypeStruct((8, 16, FFL), BF))(came)
    hidden = exchange(hidden, "zq")
    spans, weights = down
    part = call(out_kernel(spans), jax.ShapeDtypeStruct((128, 512), BF))(hidden, *weights)
    return exchange(part.reshape(16, 8, 512), "tp")


def cell_update(query_bf, key_proj, value_proj, outgate, ingate, forget, memory, normalizer, stabilizer):
    seq_count, heads_here, head_size = normalizer.shape
    query_heads = query_bf.astype(F32).reshape(seq_count, heads_here, head_size)
    key_heads = key_proj.astype(F32).reshape(seq_count, heads_here, head_size) * head_size ** (-0.5)
    value_heads = value_proj.astype(F32).reshape(seq_count, heads_here, head_size)
    log_forget = jax.nn.log_sigmoid(forget)
    ceiling = jnp.maximum(log_forget + stabilizer, ingate)
    fresh_weight = jnp.exp(ingate - ceiling)
    carried = jnp.exp(log_forget + stabilizer - ceiling)
    own_score = jnp.sum(query_heads * key_heads, axis=-1) * fresh_weight
    recall = jnp.einsum("bhde,bhe->bhd", memory, query_heads, precision=lax.Precision.HIGHEST)
    numerator = own_score[..., None] * value_heads + carried[..., None] * recall
    denominator = own_score + carried * jnp.sum(normalizer * query_heads, axis=-1)
    readout = numerator / jnp.maximum(jnp.abs(denominator), jnp.exp(-ceiling))[..., None]
    memory_new = (
        carried[..., None, None] * memory
        + (fresh_weight[..., None] * value_heads)[..., :, None] * key_heads[..., None, :]
    )
    normalizer_new = carried[..., None] * normalizer + fresh_weight[..., None] * key_heads
    gated_out = (
        jax.nn.sigmoid(outgate.astype(F32)) * readout.reshape(seq_count, -1)
    ).astype(BF)
    return (gated_out, memory_new, normalizer_new, ceiling)


def on_device(
    tokens,
    gain_first,
    gate_first,
    up_first,
    down_first,
    gain_mix,
    w_query,
    w_key,
    w_value,
    w_outgate,
    w_ingate,
    w_forget,
    forget_bias,
    memory,
    normalizer,
    stabilizer,
    w_project,
    gain_second,
    gate_second,
    up_second,
    down_second,
):
    pair = lax.axis_index("zp")
    core = lax.axis_index("c")
    at = lax.axis_index("tp")

    pair_at = jnp.reshape(pair, (1,)).astype(jnp.int32)
    core_at = jnp.reshape(core, (1,)).astype(jnp.int32)
    shard_at = jnp.reshape(at, (1,)).astype(jnp.int32)
    zero = jnp.zeros((1,), jnp.int32)
    wide_shape = jax.ShapeDtypeStruct((128, WIDE), BF)

    first = pack(gate_up(0, 1), gate_first.T, up_first.T)
    first_came = swap(first)
    packed = jax.ShapeDtypeStruct((272, 128), BF)
    kept, sent = call(prep_kernel, (packed, packed), 1)(
        pair_at,
        tokens.reshape(8, NP, 2, 16, 128),
        gain_first.reshape(1, 128),
        gain_mix.reshape(1, 128),
        gain_second.reshape(1, 128),
    )
    came = swap(sent)
    heads = w_ingate.shape[1]
    middle = pack(
        [(i, 0, 128) for i in range(4)]
        + [(4, 0, heads), (5, 0, heads), (6, 0, FFL), (7, 0, 128), (8, FFL - 64, 64)],
        w_query,
        w_key,
        w_value,
        w_outgate,
        w_ingate.T,
        w_forget.T,
        down_first,
        w_project,
        down_second,
    )
    middle_came = swap(middle)
    last = pack(gate_up(0, 1) + [(2, 0, FFL - 64)], gate_second.T, up_second.T, down_second)
    last_came = swap(last)

    kept, came = both_cores(kept), both_cores(came)
    first_own, first_other = both_cores(first), both_cores(first_came)
    middle_own = both_cores(middle)
    middle_other = both_cores(middle_came)
    last_own = both_cores(last)
    last_other = both_cores(last_came)

    shard = jax.ShapeDtypeStruct((1, 8, 512), BF)
    copied = jax.ShapeDtypeStruct((16, 8, 512), BF)
    wide, rows, gains = call(
        first_kernel, (wide_shape, copied, jax.ShapeDtypeStruct((3, 1, 512), F32)), 1
    )(core_at, kept, came, first_own, first_other)
    came = half_step(wide, (((0, 544, FFL),), (middle_own, middle_other)))
    after_first, copies = call(residual_kernel(0.5), (shard, copied), 1)(shard_at, came, rows)
    copies = exchange(copies, "tp")

    mixed = call(mix_kernel, jax.ShapeDtypeStruct((128, MIX), BF))(
        copies, gains[1], middle_own, middle_other
    )
    summed = exchange(mixed.reshape(8, 16, MIX), "zq")
    summed = jnp.sum(summed.astype(F32), axis=0)
    scale = lax.rsqrt((summed[:, 624:625] + summed[:, 625:626]) / D + EPSILON)
    query_bf, key_proj, value_proj, outgate = (
        (scale * summed[:, 128 * i : 128 * (i + 1)]).astype(BF) for i in range(4)
    )
    ingate = scale * lax.dynamic_slice_in_dim(summed[:, 512 : 512 + heads], at, 1, 1)
    forget = scale * lax.dynamic_slice_in_dim(summed[:, 512 + heads : 512 + 2 * heads], at, 1, 1)
    gated_out, memory_new, normalizer_new, stabilizer_new = cell_update(
        query_bf, key_proj, value_proj, outgate, ingate, forget + forget_bias, memory, normalizer, stabilizer
    )
    gated = exchange(jnp.broadcast_to(gated_out, (8, *gated_out.shape)), "zq")
    part = call(out_kernel(((0, 1232, 128),)), jax.ShapeDtypeStruct((128, 512), BF))(
        gated, middle_own, middle_other
    )
    came = exchange(part.reshape(16, 8, 512), "tp")
    after_mix, copies = call(residual_kernel(1.0), (shard, copied), 1)(zero, came, after_first)
    copies = exchange(copies, "tp")

    wide = call(wide_kernel, wide_shape)(copies, gains[2], last_own, last_other)
    came = half_step(
        wide,
        (
            ((0, WIDE, FFL - 64), (1, 1360, 64)),
            (last_own, last_other, middle_own, middle_other),
        ),
    )
    outgoing = call(last_kernel, jax.ShapeDtypeStruct((64, 8, 128), BF), 1)(
        pair_at, came, after_mix
    )
    came = exchange(outgoing, ("zp", "c", "tp"))
    came = came.reshape(NP, 2, 8, 16, 128).transpose(2, 0, 1, 3, 4)
    return (came.reshape(-1, 128), memory_new, normalizer_new, stabilizer_new)


def solution(mesh):
    kv, tp = mesh.shape["kv"], mesh.shape["tp"]
    finer = Mesh(mesh.devices.reshape(kv // (2 * NP), NP, 2, tp), ("zq", "zp", "c", "tp"))
    return jax.shard_map(
        on_device,
        mesh=finer,
        in_specs=(
            P(None, KV),
            P(KV),
            P(KV, "tp"),
            P(KV, "tp"),
            P("tp", KV),
            P(KV),
            P(KV, "tp"),
            P(KV, "tp"),
            P(KV, "tp"),
            P(KV, "tp"),
            P(KV, None),
            P(KV, None),
            P("tp"),
            P(KV, "tp", None, None),
            P(KV, "tp", None),
            P(KV, "tp"),
            P("tp", KV),
            P(KV),
            P(KV, "tp"),
            P(KV, "tp"),
            P("tp", KV),
        ),
        out_specs=(P(None, KV), P(KV, "tp", None, None), P(KV, "tp", None), P(KV, "tp")),
        check_vma=False,
    )
```

profile of v0, /device:TPU:1, one launch (start us, length us, event | category | flops | bytes accessed | tf_op | source)
XLA Modules:
  0.0 265.9 jit_solution(16751398015991985330)
XLA Ops:
  0.6 0.9 copy-done.2
  1.6 0.9 copy-done.3
  3.0 4.4 %collective-permute-start.1 = (bf16[1408,128]{1,0:T(8,128)(2,1)S(1)}, bf16[1408,128]{1,0:T(8,128)(2,1)S(1)}, u32[]{:S(2)}, u32[]{:S(2)}) collective-permute-start(bf16[1408,128]{1,0:T(8,128)(2,1)S(1)} %shard_map.229), channel_id=1, source_target_pairs={{0,32},{32,0},{1,33},{33,1},{2,34},{34,2},{3,35},{35,3},{4,36},{36... | collective-permute-start | bytes 1081352 | tf_op jit(solution)/shard_map/ppermute | solution.py:25
  8.1 1.9 collective-permute-start
  10.0 8.3 %all-gather.2 = bf16[2816,128]{1,0:T(8,128)(2,1)S(1)} all-gather(bf16[1408,128]{1,0:T(8,128)(2,1)S(1)} %shard_map.229), channel_id=4, replica_groups=mesh['zq'=8,'zp'=2,'c'=2,'tp'=16] {'c'}, dimensions={0}, use_global_device_ids=true | all-gather | bytes 1081344 | tf_op jit(solution)/shard_map/all_gather | solution.py:29
  18.3 1.9 all-gather
  20.3 1.9 all-gather.1
  22.2 2.3 all-gather.3
  25.1 35.4 %all_to_all.60.x_ref = bf16[8,16,1408]{2,1,0:T(8,128)(2,1)S(1)} all-to-all(bf16[8,16,1408]{2,1,0:T(8,128)(2,1)S(1)} %bitcast.76), channel_id=1, replica_groups=mesh['zq'=8,'zp'=2,'c'=2,'tp'=16] {'zq'}, dimensions={0} | all-to-all | bytes 720896 | tf_op jit(solution)/shard_map/all_to_all | solution.py:33
  60.5 0.9 shard_map.231
  61.4 4.7 %all-to-all-start.1 = ((bf16[8,16,688]{2,1,0:T(8,128)(2,1)}), bf16[8,16,688]{2,1,0:T(8,128)(2,1)S(1)}, u32[]{:S(2)}, u32[]{:S(2)}) async-start(bf16[8,16,688]{2,1,0:T(8,128)(2,1)} %shard_map.231), calls=%async_computation.1 | async-start | bytes 393216 | tf_op jit(solution)/shard_map/all_to_all | solution.py:33
  66.7 3.2 %collective-permute-start.2 = (bf16[1424,128]{1,0:T(8,128)(2,1)S(1)}, bf16[1424,128]{1,0:T(8,128)(2,1)S(1)}, u32[]{:S(2)}, u32[]{:S(2)}) collective-permute-start(bf16[1424,128]{1,0:T(8,128)(2,1)S(1)} %shard_map.232), channel_id=1, source_target_pairs={{0,32},{32,0},{1,33},{33,1},{2,34},{34,2},{3,35},{35,3},{4,36},{36... | collective-permute-start | bytes 1093640 | tf_op jit(solution)/shard_map/ppermute | solution.py:25
  70.0 3.2 %all-gather.4 = bf16[2848,128]{1,0:T(8,128)(2,1)S(1)} all-gather(bf16[1424,128]{1,0:T(8,128)(2,1)S(1)} %shard_map.232), channel_id=6, replica_groups=mesh['zq'=8,'zp'=2,'c'=2,'tp'=16] {'c'}, dimensions={0}, use_global_device_ids=true | all-gather | bytes 1093632 | tf_op jit(solution)/shard_map/all_gather | solution.py:29
  73.1 11.4 %collective-permute-done.2 = bf16[1424,128]{1,0:T(8,128)(2,1)S(1)} collective-permute-done((bf16[1424,128]{1,0:T(8,128)(2,1)S(1)}, bf16[1424,128]{1,0:T(8,128)(2,1)S(1)}, u32[]{:S(2)}, u32[]{:S(2)}) %collective-permute-start.2) | collective-permute-done | bytes 364576 | tf_op jit(solution)/shard_map/ppermute | solution.py:25
  84.6 2.9 %all-gather.5 = bf16[2848,128]{1,0:T(8,128)(2,1)S(1)} all-gather(bf16[1424,128]{1,0:T(8,128)(2,1)S(1)} %collective-permute-done.2), channel_id=7, replica_groups=mesh['zq'=8,'zp'=2,'c'=2,'tp'=16] {'c'}, dimensions={0}, use_global_device_ids=true | all-gather | bytes 1093632 | tf_op jit(solution)/shard_map/all_gather | solution.py:29
  87.5 0.9 shard_map.233
  88.4 6.8 %all-to-all-start.2 = ((bf16[16,8,512]{2,1,0:T(8,128)(2,1)}), bf16[16,8,512]{2,1,0:T(8,128)(2,1)S(1)}, u32[]{:S(2)}, u32[]{:S(2)}) async-start(bf16[16,8,512]{2,1,0:T(8,128)(2,1)} %bitcast.18), calls=%async_computation.2 | async-start | bytes 262144 | tf_op jit(solution)/shard_map/all_to_all | solution.py:33
  95.2 6.8 %all-to-all-done.2.sum_ref = bf16[16,8,512]{2,1,0:T(8,128)(2,1)S(1)} async-done(((bf16[16,8,512]{2,1,0:T(8,128)(2,1)}), bf16[16,8,512]{2,1,0:T(8,128)(2,1)S(1)}, u32[]{:S(2)}, u32[]{:S(2)}) %all-to-all-start.2) | async-done | bytes 131104 | tf_op jit(solution)/shard_map/all_to_all | solution.py:33
  102.0 0.7 shard_map.234
  102.7 3.5 %all-to-all-start.3 = ((bf16[16,8,512]{2,1,0:T(8,128)(2,1)}), bf16[16,8,512]{2,1,0:T(8,128)(2,1)S(1)}, u32[]{:S(2)}, u32[]{:S(2)}) async-start(bf16[16,8,512]{2,1,0:T(8,128)(2,1)} %get-tuple-element.17), calls=%async_computation.3 | async-start | bytes 262144 | tf_op jit(solution)/shard_map/all_to_all | solution.py:33
  106.2 6.8 %all-to-all-done.3.x_ref = bf16[16,8,512]{2,1,0:T(8,128)(2,1)S(1)} async-done(((bf16[16,8,512]{2,1,0:T(8,128)(2,1)}), bf16[16,8,512]{2,1,0:T(8,128)(2,1)S(1)}, u32[]{:S(2)}, u32[]{:S(2)}) %all-to-all-start.3) | async-done | bytes 131104 | tf_op jit(solution)/shard_map/all_to_all | solution.py:33
  113.0 0.9 shard_map.235
  114.0 10.5 %all-to-all-start.4 = ((bf16[8,16,640]{2,1,0:T(8,128)(2,1)}), bf16[8,16,640]{2,1,0:T(8,128)(2,1)S(1)}, u32[]{:S(2)}, u32[]{:S(2)}) async-start(bf16[8,16,640]{2,1,0:T(8,128)(2,1)} %bitcast.20), calls=%async_computation.4 | async-start | bytes 327680 | tf_op jit(solution)/shard_map/all_to_all | solution.py:33
  124.5 0.7 shard_map.238
  125.2 3.1 %collective-permute-start.3 = (bf16[2032,128]{1,0:T(8,128)(2,1)S(1)}, bf16[2032,128]{1,0:T(8,128)(2,1)}, u32[]{:S(2)}, u32[]{:S(2)}) collective-permute-start(bf16[2032,128]{1,0:T(8,128)(2,1)S(1)} %shard_map.238), channel_id=1, source_target_pairs={{0,32},{32,0},{1,33},{33,1},{2,34},{34,2},{3,35},{35,3},{4,36},{36... | collective-permute-start | bytes 1560584 | tf_op jit(solution)/shard_map/ppermute | solution.py:25
  128.3 0.6 copy-done.27
  129.7 9.3 %all-to-all-done.4 = bf16[8,16,640]{2,1,0:T(8,128)(2,1)S(1)} async-done(((bf16[8,16,640]{2,1,0:T(8,128)(2,1)}), bf16[8,16,640]{2,1,0:T(8,128)(2,1)S(1)}, u32[]{:S(2)}, u32[]{:S(2)}) %all-to-all-start.4) | async-done | bytes 163872 | tf_op jit(solution)/shard_map/all_to_all | solution.py:33
  139.4 0.7 convert_multiply_fusion.3
  140.5 2.1 fusion
  143.4 0.7 convert_multiply_fusion
  144.1 14.1 %all_to_all.61.x_ref = bf16[8,16,128]{2,1,0:T(8,128)(2,1)S(1)} all-to-all(bf16[8,16,128]{2,1,0:T(8,128)(2,1)S(1)} %broadcast_in_dim.2), channel_id=1, replica_groups=mesh['zq'=8,'zp'=2,'c'=2,'tp'=16] {'zq'}, dimensions={0} | all-to-all | bytes 65536 | tf_op jit(solution)/shard_map/all_to_all | solution.py:33
  158.2 0.8 shard_map.236
  159.0 4.1 %all-to-all-start.6 = ((bf16[16,8,512]{2,1,0:T(8,128)(2,1)}), bf16[16,8,512]{2,1,0:T(8,128)(2,1)S(1)}, u32[]{:S(2)}, u32[]{:S(2)}) async-start(bf16[16,8,512]{2,1,0:T(8,128)(2,1)} %bitcast.30), calls=%async_computation.6 | async-start | bytes 262144 | tf_op jit(solution)/shard_map/all_to_all | solution.py:33
  163.2 8.6 %all-gather.6 = bf16[4064,128]{1,0:T(8,128)(2,1)S(1)} all-gather(bf16[2032,128]{1,0:T(8,128)(2,1)S(1)} %shard_map.238), channel_id=8, replica_groups=mesh['zq'=8,'zp'=2,'c'=2,'tp'=16] {'c'}, dimensions={0}, use_global_device_ids=true | all-gather | bytes 1560576 | tf_op jit(solution)/shard_map/all_gather | solution.py:29
  171.8 0.7 shard_map.237
  172.4 6.9 %all-to-all-start.7 = ((bf16[16,8,512]{2,1,0:T(8,128)(2,1)}), bf16[16,8,512]{2,1,0:T(8,128)(2,1)}, u32[]{:S(2)}, u32[]{:S(2)}) async-start(bf16[16,8,512]{2,1,0:T(8,128)(2,1)} %get-tuple-element.20), calls=%async_computation.7 | async-start | bytes 262144 | tf_op jit(solution)/shard_map/all_to_all | solution.py:33
  179.4 5.4 %all-gather.7 = bf16[4064,128]{1,0:T(8,128)(2,1)S(1)} all-gather(bf16[2032,128]{1,0:T(8,128)(2,1)} %collective-permute-done.3), channel_id=9, replica_groups=mesh['zq'=8,'zp'=2,'c'=2,'tp'=16] {'c'}, dimensions={0}, use_global_device_ids=true | all-gather | bytes 1560576 | tf_op jit(solution)/shard_map/all_gather | solution.py:29
  184.8 1.5 all-to-all-done.7.x_ref
  186.3 1.5 shard_map.239
  187.8 22.2 %all_to_all.62.x_ref = bf16[8,16,1408]{2,1,0:T(8,128)(2,1)S(1)} all-to-all(bf16[8,16,1408]{2,1,0:T(8,128)(2,1)S(1)} %bitcast.72), channel_id=1, replica_groups=mesh['zq'=8,'zp'=2,'c'=2,'tp'=16] {'zq'}, dimensions={0} | all-to-all | bytes 720896 | tf_op jit(solution)/shard_map/all_to_all | solution.py:33
  210.1 21.7 %all_to_all.63.x_ref = bf16[8,16,688]{2,1,0:T(8,128)(2,1)S(1)} all-to-all(bf16[8,16,688]{2,1,0:T(8,128)(2,1)S(1)} %shard_map.240), channel_id=1, replica_groups=mesh['zq'=8,'zp'=2,'c'=2,'tp'=16] {'zq'}, dimensions={0} | all-to-all | bytes 352256 | tf_op jit(solution)/shard_map/all_to_all | solution.py:33
  232.1 14.4 %all_to_all.64.sum_ref = bf16[16,8,512]{2,1,0:T(8,128)(2,1)S(1)} all-to-all(bf16[16,8,512]{2,1,0:T(8,128)(2,1)S(1)} %bitcast.75), channel_id=1, replica_groups=mesh['zq'=8,'zp'=2,'c'=2,'tp'=16] {'tp'}, dimensions={0} | all-to-all | bytes 262144 | tf_op jit(solution)/shard_map/all_to_all | solution.py:33
  246.5 0.7 shard_map.242
  247.2 9.6 %all-to-all-start.11 = ((bf16[64,8,128]{2,1,0:T(8,128)(2,1)}), bf16[64,8,128]{2,1,0:T(8,128)(2,1)S(1)}, u32[]{:S(2)}, u32[]{:S(2)}) async-start(bf16[64,8,128]{2,1,0:T(8,128)(2,1)} %shard_map.242), calls=%async_computation.11 | async-start | bytes 262144 | tf_op jit(solution)/shard_map/all_to_all | solution.py:33
  257.5 0.7 fusion.6
  258.2 2.5 multiply_add_fusion
  260.8 4.4 %all-to-all-done.11 = bf16[64,8,128]{2,1,0:T(8,128)(2,1)S(1)} async-done(((bf16[64,8,128]{2,1,0:T(8,128)(2,1)}), bf16[64,8,128]{2,1,0:T(8,128)(2,1)S(1)}, u32[]{:S(2)}, u32[]{:S(2)}) %all-to-all-start.11) | async-done | bytes 131104 | tf_op jit(solution)/shard_map/all_to_all | solution.py:33
  265.2 0.7 copy.45
  (78 shorter events, 5.2 us)
Async XLA Ops:
  0.6 0.9 copy-start.2
  1.6 0.9 copy-start.3
  2.5 4.9 %copy-start.6 = (bf16[512,128]{1,0:T(8,128)(2,1)S(1)}, bf16[512,128]{1,0:T(8,128)(2,1)}, u32[]{:S(2)}) copy-start(bf16[512,128]{1,0:T(8,128)(2,1)} %param.21) | copy-start | bytes 393220
  3.0 19.2 %collective-permute-start.1 = (bf16[1408,128]{1,0:T(8,128)(2,1)S(1)}, bf16[1408,128]{1,0:T(8,128)(2,1)S(1)}, u32[]{:S(2)}, u32[]{:S(2)}) collective-permute-start(bf16[1408,128]{1,0:T(8,128)(2,1)S(1)} %shard_map.229), channel_id=1, source_target_pairs={{0,32},{32,0},{1,33},{33,1},{2,34},{34,2},{3,35},{35,3},{4,36},{36... | collective-permute-start | bytes 1081352 | tf_op jit(solution)/shard_map/ppermute | solution.py:25
  7.4 0.7 copy-start.14
  7.4 0.7 copy-start.15
  7.4 0.7 copy-start.16
  8.1 12.2 %collective-permute-start = (bf16[272,128]{1,0:T(8,128)(2,1)S(1)}, bf16[272,128]{1,0:T(8,128)(2,1)S(1)}, u32[]{:S(2)}, u32[]{:S(2)}) collective-permute-start(bf16[272,128]{1,0:T(8,128)(2,1)S(1)} %get-tuple-element.14), channel_id=1, source_target_pairs={{0,32},{32,0},{1,33},{33,1},{2,34},{34,2},{3,35},{35,3},{4,36},{36... | collective-permute-start | bytes 208904 | tf_op jit(solution)/shard_map/ppermute | solution.py:25
  60.5 5.6 %copy-start.8 = (bf16[128,128]{1,0:T(8,128)(2,1)S(1)}, bf16[128,128]{1,0:T(8,128)(2,1)}, u32[]{:S(2)}) copy-start(bf16[128,128]{1,0:T(8,128)(2,1)} %refs_1_.1) | copy-start | bytes 98308
  60.5 5.6 %copy-start.9 = (bf16[128,128]{1,0:T(8,128)(2,1)S(1)}, bf16[128,128]{1,0:T(8,128)(2,1)}, u32[]{:S(2)}) copy-start(bf16[128,128]{1,0:T(8,128)(2,1)} %refs_2_.2) | copy-start | bytes 98308
  60.5 5.6 %copy-start.10 = (bf16[128,128]{1,0:T(8,128)(2,1)S(1)}, bf16[128,128]{1,0:T(8,128)(2,1)}, u32[]{:S(2)}) copy-start(bf16[128,128]{1,0:T(8,128)(2,1)} %refs_3_.1) | copy-start | bytes 98308
  60.5 5.6 %copy-start.11 = (bf16[128,128]{1,0:T(8,128)(2,1)S(1)}, bf16[128,128]{1,0:T(8,128)(2,1)}, u32[]{:S(2)}) copy-start(bf16[128,128]{1,0:T(8,128)(2,1)} %refs_7_.1) | copy-start | bytes 98308
  61.3 4.8 %copy-start = (bf16[688,128]{1,0:T(8,128)(2,1)S(1)}, bf16[688,128]{1,0:T(8,128)(2,1)}, u32[]{:S(2)}) copy-start(bf16[688,128]{1,0:T(8,128)(2,1)} %refs_2_.3) | copy-start | bytes 528388
  61.3 4.8 %copy-start.1 = (bf16[688,128]{1,0:T(8,128)(2,1)S(1)}, bf16[688,128]{1,0:T(8,128)(2,1)}, u32[]{:S(2)}) copy-start(bf16[688,128]{1,0:T(8,128)(2,1)} %refs_6_.1) | copy-start | bytes 528388
  61.3 4.8 %copy-start.7 = (bf16[128,128]{1,0:T(8,128)(2,1)S(1)}, bf16[128,128]{1,0:T(8,128)(2,1)}, u32[]{:S(2)}) copy-start(bf16[128,128]{1,0:T(8,128)(2,1)} %refs_0_.1) | copy-start | bytes 98308
  61.3 4.8 %copy-start.12 = (bf16[128,16]{0,1:T(8,128)(2,1)S(1)}, bf16[128,16]{0,1:T(8,128)(2,1)}, u32[]{:S(2)}) copy-start(bf16[128,16]{0,1:T(8,128)(2,1)} %param.31) | copy-start | bytes 12292
  61.4 4.8 %copy-start.13 = (bf16[128,16]{0,1:T(8,128)(2,1)S(1)}, bf16[128,16]{0,1:T(8,128)(2,1)}, u32[]{:S(2)}) copy-start(bf16[128,16]{0,1:T(8,128)(2,1)} %param.32) | copy-start | bytes 12292
  61.4 26.1 %all-to-all-start.1 = ((bf16[8,16,688]{2,1,0:T(8,128)(2,1)}), bf16[8,16,688]{2,1,0:T(8,128)(2,1)S(1)}, u32[]{:S(2)}, u32[]{:S(2)}) async-start(bf16[8,16,688]{2,1,0:T(8,128)(2,1)} %shard_map.231), calls=%async_computation.1 | async-start | bytes 393216 | tf_op jit(solution)/shard_map/all_to_all | solution.py:33
  66.7 17.8 %collective-permute-start.2 = (bf16[1424,128]{1,0:T(8,128)(2,1)S(1)}, bf16[1424,128]{1,0:T(8,128)(2,1)S(1)}, u32[]{:S(2)}, u32[]{:S(2)}) collective-permute-start(bf16[1424,128]{1,0:T(8,128)(2,1)S(1)} %shard_map.232), channel_id=1, source_target_pairs={{0,32},{32,0},{1,33},{33,1},{2,34},{34,2},{3,35},{35,3},{4,36},{36... | collective-permute-start | bytes 1093640 | tf_op jit(solution)/shard_map/ppermute | solution.py:25
  88.4 13.6 %all-to-all-start.2 = ((bf16[16,8,512]{2,1,0:T(8,128)(2,1)}), bf16[16,8,512]{2,1,0:T(8,128)(2,1)S(1)}, u32[]{:S(2)}, u32[]{:S(2)}) async-start(bf16[16,8,512]{2,1,0:T(8,128)(2,1)} %bitcast.18), calls=%async_computation.2 | async-start | bytes 262144 | tf_op jit(solution)/shard_map/all_to_all | solution.py:33
  102.7 10.3 %all-to-all-start.3 = ((bf16[16,8,512]{2,1,0:T(8,128)(2,1)}), bf16[16,8,512]{2,1,0:T(8,128)(2,1)S(1)}, u32[]{:S(2)}, u32[]{:S(2)}) async-start(bf16[16,8,512]{2,1,0:T(8,128)(2,1)} %get-tuple-element.17), calls=%async_computation.3 | async-start | bytes 262144 | tf_op jit(solution)/shard_map/all_to_all | solution.py:33
  113.0 11.5 %copy-start.5 = (bf16[128,688]{0,1:T(8,128)(2,1)S(1)}, bf16[128,688]{0,1:T(8,128)(2,1)}, u32[]{:S(2)}) copy-start(bf16[128,688]{0,1:T(8,128)(2,1)} %param.40) | copy-start | bytes 528388
  113.9 10.5 %copy-start.4 = (bf16[128,688]{0,1:T(8,128)(2,1)S(1)}, bf16[128,688]{0,1:T(8,128)(2,1)}, u32[]{:S(2)}) copy-start(bf16[128,688]{0,1:T(8,128)(2,1)} %param.39) | copy-start | bytes 528388
  114.0 25.1 %all-to-all-start.4 = ((bf16[8,16,640]{2,1,0:T(8,128)(2,1)}), bf16[8,16,640]{2,1,0:T(8,128)(2,1)S(1)}, u32[]{:S(2)}, u32[]{:S(2)}) async-start(bf16[8,16,640]{2,1,0:T(8,128)(2,1)} %bitcast.20), calls=%async_computation.4 | async-start | bytes 327680 | tf_op jit(solution)/shard_map/all_to_all | solution.py:33
  125.2 54.1 %collective-permute-start.3 = (bf16[2032,128]{1,0:T(8,128)(2,1)S(1)}, bf16[2032,128]{1,0:T(8,128)(2,1)}, u32[]{:S(2)}, u32[]{:S(2)}) collective-permute-start(bf16[2032,128]{1,0:T(8,128)(2,1)S(1)} %shard_map.238), channel_id=1, source_target_pairs={{0,32},{32,0},{1,33},{33,1},{2,34},{34,2},{3,35},{35,3},{4,36},{36... | collective-permute-start | bytes 1560584 | tf_op jit(solution)/shard_map/ppermute | solution.py:25
  128.3 0.7 copy-start.27
  139.2 3.4 %copy-start.17 = (f32[16,1]{1,0:T(8,128)}, f32[16,1]{1,0:T(8,128)S(1)}, u32[]{:S(2)}) copy-start(f32[16,1]{1,0:T(8,128)S(1)} %get-tuple-element.43) | copy-start | bytes 196
  139.4 0.7 copy-start.21
  142.8 0.5 copy-start.23
  142.9 0.5 copy-start.25
  159.0 12.7 %all-to-all-start.6 = ((bf16[16,8,512]{2,1,0:T(8,128)(2,1)}), bf16[16,8,512]{2,1,0:T(8,128)(2,1)S(1)}, u32[]{:S(2)}, u32[]{:S(2)}) async-start(bf16[16,8,512]{2,1,0:T(8,128)(2,1)} %bitcast.30), calls=%async_computation.6 | async-start | bytes 262144 | tf_op jit(solution)/shard_map/all_to_all | solution.py:33
  172.4 13.8 %all-to-all-start.7 = ((bf16[16,8,512]{2,1,0:T(8,128)(2,1)}), bf16[16,8,512]{2,1,0:T(8,128)(2,1)}, u32[]{:S(2)}, u32[]{:S(2)}) async-start(bf16[16,8,512]{2,1,0:T(8,128)(2,1)} %get-tuple-element.20), calls=%async_computation.7 | async-start | bytes 262144 | tf_op jit(solution)/shard_map/all_to_all | solution.py:33
  247.2 9.6 %copy-start.26 = (f32[16]{0:T(128)S(1)}, f32[16]{0:T(128)}, u32[]{:S(2)}) copy-start(f32[16]{0:T(128)} %copy-done.25) | copy-start | bytes 196
  247.2 9.7 %copy-start.18 = (f32[16,1]{1,0:T(8,128)S(1)}, f32[16,1]{1,0:T(8,128)}, u32[]{:S(2)}) copy-start(f32[16,1]{1,0:T(8,128)} %copy-done.17) | copy-start | bytes 196
  247.2 18.0 %all-to-all-start.11 = ((bf16[64,8,128]{2,1,0:T(8,128)(2,1)}), bf16[64,8,128]{2,1,0:T(8,128)(2,1)S(1)}, u32[]{:S(2)}, u32[]{:S(2)}) async-start(bf16[64,8,128]{2,1,0:T(8,128)(2,1)} %shard_map.242), calls=%async_computation.11 | async-start | bytes 262144 | tf_op jit(solution)/shard_map/all_to_all | solution.py:33
  256.8 0.7 copy-start.22
  256.9 0.7 copy-start.24
  257.5 0.7 copy-start.19
  257.5 0.7 copy-start.20
where the time goes:
time: 267 us; the launch traced here: 266 us
  blocking collectives  142 us (53%)
  starting transfers between devices  58.7 us (22%)
  waiting for transfers between devices  40.2 us (15%)
  Pallas kernels  9.98 us (4%)
  local copies, waits for them, and re-layouts  5.46 us (2%)
  other arithmetic  5.3 us (2%)
    all_to_all x5, blocking collectives, exchange(): return lax.all_to_all(parts, axis, split_axis=0, concat_axis=0, tiled=True)  108 us
    all_to_all x7, starting transfers between devices, exchange(): return lax.all_to_all(parts, axis, split_axis=0, concat_axis=0, tiled=True)  46.1 us
    all_gather x8, blocking collectives, both_cores(): return lax.all_gather(array, 'c')  34.5 us
    all_to_all x7, waiting for transfers between devices, exchange(): return lax.all_to_all(parts, axis, split_axis=0, concat_axis=0, tiled=True)  28.8 us
    ppermute x4, starting transfers between devices, swap(): return lax.ppermute(array, 'zp', [(0, 1), (1, 0)])  12.6 us
    ppermute x4, waiting for transfers between devices, swap(): return lax.ppermute(array, 'zp', [(0, 1), (1, 0)])  11.4 us
    pallas_call x12, Pallas kernels, run(): pl.pallas_call(kernel, in_specs=[smem] * scalars + [vmem] * (len(args) -...  8.16 us
  transfers between devices with their start and end apart: 11, of which 6 were waited for; matrix products, arithmetic and copies ran while one was open for 3% of the time, Pallas kernels for 1%

commit v1 on v0

--- a/solution.py
+++ b/solution.py
@@ -18,6 +18,7 @@
 TAIL = 48
 WIDE = 1408
 MIX = 640
+HERE = 272
 NT_DIMS = (((1,), (1,)), ((), ()))
 
 
@@ -81,17 +82,31 @@
     out_ref[:, WIDE - 128 :] = put_squares(total[:, WIDE - 128 :], squares, 112).astype(BF)
 
 
-def prep_kernel(pair_ref, tokens_ref, first_ref, mix_ref, second_ref, kept_ref, sent_ref):
+def prep_kernel(pair_ref, tokens_ref, first_ref, mix_ref, second_ref, gate_ref, up_ref, *refs):
+    kept_ref, sent_ref, sems = refs
+    copies = []
+    for ref in (kept_ref, sent_ref):
+        at = HERE
+        for source, start, count in gate_up(gate_ref, up_ref):
+            copy = pltpu.make_async_copy(
+                source.at[pl.ds(start, count)], ref.at[pl.ds(at, count)], sems.at[len(copies)]
+            )
+            copy.start()
+            copies.append(copy)
+            at += count
     gains = []
     for ref in (first_ref, mix_ref, second_ref):
         gains += pieces(ref[...])
+    rows = [g.astype(F32) for g in gains] + [jnp.zeros((7, 128), F32)]
+    rows = jnp.concatenate(rows, axis=0).astype(BF)
     for ref, which in ((kept_ref, pair_ref[0]), (sent_ref, 1 - pair_ref[0])):
         for core in range(2):
             for group in range(8):
                 at = 128 * core + 16 * group
                 ref[at : at + 16] = tokens_ref[group, which, core]
-        rows = [g.astype(F32) for g in gains] + [jnp.zeros((7, 128), F32)]
-        ref[256:] = jnp.concatenate(rows, axis=0).astype(BF)
+        ref[256:HERE] = rows
+    for copy in copies:
+        copy.wait()
 
 
 def pack_kernel(plan):
@@ -123,17 +138,17 @@
     )(*arrays)
 
 
-def first_kernel(core_ref, kept_ref, came_ref, own_ref, other_ref, out_ref, rows_ref, gains_ref):
+def first_kernel(core_ref, own_ref, other_ref, out_ref, rows_ref, gains_ref):
     start = pl.multiple_of(128 * core_ref[0], 128)
     total, squares = None, None
     for core in range(2):
         x, gain = [], []
-        for chip, here_ref in enumerate((kept_ref, came_ref)):
+        for chip, here_ref in enumerate((own_ref, other_ref)):
             at = 128 * (2 * core + chip)
             block = here_ref[core, pl.ds(start, 128)]
             rows_ref[:, :, at : at + 128] = block.reshape(16, 8, 128)
             x.append(block.astype(F32))
-            parts = here_ref[core, 256:].astype(F32)
+            parts = here_ref[core, 256:HERE].astype(F32)
             for i in range(3):
                 whole = (parts[3 * i : 3 * i + 1] + parts[3 * i + 1 : 3 * i + 2]) + parts[
                     3 * i + 2 : 3 * i + 3
@@ -144,7 +159,7 @@
         x, gain = jnp.concatenate(x, axis=1), jnp.concatenate(gain, axis=1)
         square = jnp.sum(x * x, axis=1, keepdims=True)
         squares = square if squares is None else squares + square
-        weight = jnp.concatenate([own_ref[core, :WIDE], other_ref[core, :WIDE]], axis=1)
+        weight = jnp.concatenate([own_ref[core, HERE:], other_ref[core, HERE:]], axis=1)
         part = dot((x * gain).astype(BF), weight, NT_DIMS)
         total = part if total is None else total + part
     out_ref[:, : WIDE - 128] = total[:, : WIDE - 128].astype(BF)
@@ -265,29 +280,49 @@
     return exchange(part.reshape(16, 8, 512), "tp")
 
 
-def cell_update(query_bf, key_proj, value_proj, outgate, ingate, forget, memory, normalizer, stabilizer):
-    seq_count, heads_here, head_size = normalizer.shape
-    query_heads = query_bf.astype(F32).reshape(seq_count, heads_here, head_size)
-    key_heads = key_proj.astype(F32).reshape(seq_count, heads_here, head_size) * head_size ** (-0.5)
-    value_heads = value_proj.astype(F32).reshape(seq_count, heads_here, head_size)
-    log_forget = jax.nn.log_sigmoid(forget)
+def cell_kernel(at_ref, bias_ref, x_ref, memory_ref, normalizer_ref, stabilizer_ref, *out_refs):
+    copies_ref, carried_ref, value_ref, key_ref, normalizer_out, stabilizer_out = out_refs
+    total = x_ref[0].astype(F32)
+    for i in range(1, x_ref.shape[0]):
+        total = total + x_ref[i].astype(F32)
+    gates = total[:, 512:]
+    scale = lax.rsqrt((gates[:, 112:113] + gates[:, 113:114]) / D + EPSILON)
+    query, key, value, outgate = (
+        (scale * total[:, 128 * i : 128 * (i + 1)]).astype(BF).astype(F32) for i in range(4)
+    )
+    key = key * 128 ** (-0.5)
+    column = lax.broadcasted_iota(jnp.int32, gates.shape, 1)
+
+    def own_head(at):
+        return jnp.sum(jnp.where(column == at, gates, 0.0), axis=1, keepdims=True)
+
+    ingate = scale * own_head(at_ref[0])
+    forget = scale * own_head(16 + at_ref[0]) + bias_ref[0]
+    log_forget = -(jnp.maximum(-forget, 0.0) + jnp.log1p(jnp.exp(-jnp.abs(forget))))
+    diagonal = lax.broadcasted_iota(jnp.int32, (16, 16), 0) == lax.broadcasted_iota(
+        jnp.int32, (16, 16), 1
+    )
+    stabilizer = jnp.sum(jnp.where(diagonal, stabilizer_ref[...], 0.0), axis=1, keepdims=True)
     ceiling = jnp.maximum(log_forget + stabilizer, ingate)
-    fresh_weight = jnp.exp(ingate - ceiling)
+    fresh = jnp.exp(ingate - ceiling)
     carried = jnp.exp(log_forget + stabilizer - ceiling)
-    own_score = jnp.sum(query_heads * key_heads, axis=-1) * fresh_weight
-    recall = jnp.einsum("bhde,bhe->bhd", memory, query_heads, precision=lax.Precision.HIGHEST)
-    numerator = own_score[..., None] * value_heads + carried[..., None] * recall
-    denominator = own_score + carried * jnp.sum(normalizer * query_heads, axis=-1)
-    readout = numerator / jnp.maximum(jnp.abs(denominator), jnp.exp(-ceiling))[..., None]
-    memory_new = (
-        carried[..., None, None] * memory
-        + (fresh_weight[..., None] * value_heads)[..., :, None] * key_heads[..., None, :]
-    )
-    normalizer_new = carried[..., None] * normalizer + fresh_weight[..., None] * key_heads
-    gated_out = (
-        jax.nn.sigmoid(outgate.astype(F32)) * readout.reshape(seq_count, -1)
-    ).astype(BF)
-    return (gated_out, memory_new, normalizer_new, ceiling)
+    own = jnp.sum(query * key, axis=1, keepdims=True) * fresh
+    recall = [
+        jnp.sum(memory_ref[i] * query[i : i + 1], axis=1, keepdims=True) for i in range(16)
+    ]
+    recall = jnp.concatenate(recall + [jnp.zeros((128, 112), F32)], axis=1).T[:16]
+    normalizer = normalizer_ref[...]
+    denominator = own + carried * jnp.sum(normalizer * query, axis=1, keepdims=True)
+    numerator = own * value + carried * recall
+    readout = numerator / jnp.maximum(jnp.abs(denominator), jnp.exp(-ceiling))
+    gated = (jax.nn.sigmoid(outgate) * readout).astype(BF)
+    for i in range(copies_ref.shape[0]):
+        copies_ref[i] = gated
+    carried_ref[...] = jnp.broadcast_to(carried, carried_ref.shape)
+    value_ref[...] = fresh * value
+    key_ref[...] = key
+    normalizer_out[...] = carried * normalizer + fresh * key
+    stabilizer_out[...] = jnp.sum(jnp.where(diagonal, ceiling, 0.0), axis=0, keepdims=True)
 
 
 def on_device(
@@ -323,28 +358,38 @@
     zero = jnp.zeros((1,), jnp.int32)
     wide_shape = jax.ShapeDtypeStruct((128, WIDE), BF)
 
-    first = pack(gate_up(0, 1), gate_first.T, up_first.T)
-    first_came = swap(first)
-    packed = jax.ShapeDtypeStruct((272, 128), BF)
-    kept, sent = call(prep_kernel, (packed, packed), 1)(
+    smem = pl.BlockSpec(memory_space=pltpu.SMEM)
+    vmem = pl.BlockSpec(memory_space=pltpu.VMEM)
+    packed = jax.ShapeDtypeStruct((HERE + WIDE, 128), BF)
+    kept, sent = pl.pallas_call(
+        prep_kernel,
+        in_specs=[smem] + [vmem] * 4 + [pl.BlockSpec(memory_space=pl.ANY)] * 2,
+        out_specs=(vmem, vmem),
+        out_shape=(packed, packed),
+        scratch_shapes=[pltpu.SemaphoreType.DMA((12,))],
+        name="prep",
+        compiler_params=pltpu.CompilerParams(vmem_limit_bytes=4 * 2**20),
+    )(
         pair_at,
         tokens.reshape(8, NP, 2, 16, 128),
         gain_first.reshape(1, 128),
         gain_mix.reshape(1, 128),
         gain_second.reshape(1, 128),
+        gate_first.T,
+        up_first.T,
     )
     came = swap(sent)
+    down_came = swap(down_first)
     heads = w_ingate.shape[1]
     middle = pack(
         [(i, 0, 128) for i in range(4)]
-        + [(4, 0, heads), (5, 0, heads), (6, 0, FFL), (7, 0, 128), (8, FFL - 64, 64)],
+        + [(4, 0, heads), (5, 0, heads), (6, 0, 128), (7, FFL - 64, 64)],
         w_query,
         w_key,
         w_value,
         w_outgate,
         w_ingate.T,
         w_forget.T,
-        down_first,
         w_project,
         down_second,
     )
@@ -352,19 +397,17 @@
     last = pack(gate_up(0, 1) + [(2, 0, FFL - 64)], gate_second.T, up_second.T, down_second)
     last_came = swap(last)
 
-    kept, came = both_cores(kept), both_cores(came)
-    first_own, first_other = both_cores(first), both_cores(first_came)
-    middle_own = both_cores(middle)
-    middle_other = both_cores(middle_came)
-    last_own = both_cores(last)
-    last_other = both_cores(last_came)
+    first_own, first_other = both_cores(kept), both_cores(came)
+    down_own, down_other = both_cores(down_first), both_cores(down_came)
+    middle_own, middle_other = both_cores(middle), both_cores(middle_came)
+    last_own, last_other = both_cores(last), both_cores(last_came)
 
     shard = jax.ShapeDtypeStruct((1, 8, 512), BF)
     copied = jax.ShapeDtypeStruct((16, 8, 512), BF)
     wide, rows, gains = call(
         first_kernel, (wide_shape, copied, jax.ShapeDtypeStruct((3, 1, 512), F32)), 1
-    )(core_at, kept, came, first_own, first_other)
-    came = half_step(wide, (((0, 544, FFL),), (middle_own, middle_other)))
+    )(core_at, first_own, first_other)
+    came = half_step(wide, (((0, 0, FFL),), (down_own, down_other)))
     after_first, copies = call(residual_kernel(0.5), (shard, copied), 1)(shard_at, came, rows)
     copies = exchange(copies, "tp")
 
@@ -372,18 +415,26 @@
         copies, gains[1], middle_own, middle_other
     )
     summed = exchange(mixed.reshape(8, 16, MIX), "zq")
-    summed = jnp.sum(summed.astype(F32), axis=0)
-    scale = lax.rsqrt((summed[:, 624:625] + summed[:, 625:626]) / D + EPSILON)
-    query_bf, key_proj, value_proj, outgate = (
-        (scale * summed[:, 128 * i : 128 * (i + 1)]).astype(BF) for i in range(4)
-    )
-    ingate = scale * lax.dynamic_slice_in_dim(summed[:, 512 : 512 + heads], at, 1, 1)
-    forget = scale * lax.dynamic_slice_in_dim(summed[:, 512 + heads : 512 + 2 * heads], at, 1, 1)
-    gated_out, memory_new, normalizer_new, stabilizer_new = cell_update(
-        query_bf, key_proj, value_proj, outgate, ingate, forget + forget_bias, memory, normalizer, stabilizer
-    )
-    gated = exchange(jnp.broadcast_to(gated_out, (8, *gated_out.shape)), "zq")
-    part = call(out_kernel(((0, 1232, 128),)), jax.ShapeDtypeStruct((128, 512), BF))(
+    small = jax.ShapeDtypeStruct((16, 128), F32)
+    copies, carried, value, key, normalizer_new, stabilizer_new = call(
+        cell_kernel,
+        (jax.ShapeDtypeStruct((8, 16, 128), BF), small, small, small, small, jax.ShapeDtypeStruct((1, 16), F32)),
+        2,
+    )(
+        shard_at,
+        forget_bias,
+        summed,
+        memory.reshape(16, 128, 128),
+        normalizer.reshape(16, 128),
+        stabilizer.T,
+    )
+    memory_new = (
+        carried[:, None, :1, None] * memory + value[:, None, :, None] * key[:, None, None, :]
+    )
+    normalizer_new = normalizer_new.reshape(normalizer.shape)
+    stabilizer_new = stabilizer_new.T
+    gated = exchange(copies, "zq")
+    part = call(out_kernel(((0, 544, 128),)), jax.ShapeDtypeStruct((128, 512), BF))(
         gated, middle_own, middle_other
     )
     came = exchange(part.reshape(16, 8, 512), "tp")
@@ -394,7 +445,7 @@
     came = half_step(
         wide,
         (
-            ((0, WIDE, FFL - 64), (1, 1360, 64)),
+            ((0, WIDE, FFL - 64), (1, 672, 64)),
             (last_own, last_other, middle_own, middle_other),
         ),
     )

time: 267 us -> 259 us (0.970)
  waiting for transfers between devices: 40.2 us -> 27.5 us
  blocking collectives: 142 us -> 152 us
  other arithmetic: 5.3 us -> 2.55 us
    ppermute x4, waiting for transfers between devices: 11.4 us -> 3.17 us  [swap(): return lax.ppermute(array, 'zp', [(0, 1), (1, 0)])]
    all_gather x8, blocking collectives: 34.5 us -> 42.4 us  [both_cores(): return lax.all_gather(array, 'c')]
    all_to_all x7, waiting for transfers between devices: 28.8 us -> 24.3 us  [exchange(): return lax.all_to_all(parts, axis, split_axis=0, concat_axis=0, tiled=True)]
  transfers between devices with their start and end apart: 11 -> 11, of which waited for: 6 -> 5; matrix products, arithmetic and copies ran while one was open for 3% -> 1% of each run, Pallas kernels for 1% -> 2%
where the time goes in v1:
time: 259 us; the launch traced here: 258 us
  blocking collectives  152 us (59%)
  starting transfers between devices  58.9 us (23%)
  waiting for transfers between devices  27.5 us (11%)
  Pallas kernels  10.6 us (4%)
  local copies, waits for them, and re-layouts  4.9 us (2%)
    all_to_all x5, blocking collectives, exchange(): return lax.all_to_all(parts, axis, split_axis=0, concat_axis=0, tiled=True)  110 us
    all_to_all x7, starting transfers between devices, exchange(): return lax.all_to_all(parts, axis, split_axis=0, concat_axis=0, tiled=True)  46.2 us
    all_gather x8, blocking collectives, both_cores(): return lax.all_gather(array, 'c')  42.4 us
    all_to_all x7, waiting for transfers between devices, exchange(): return lax.all_to_all(parts, axis, split_axis=0, concat_axis=0, tiled=True)  24.3 us
    ppermute x4, starting transfers between devices, swap(): return lax.ppermute(array, 'zp', [(0, 1), (1, 0)])  12.7 us
    pallas_call x12, Pallas kernels, run(): pl.pallas_call(kernel, in_specs=[smem] * scalars + [vmem] * (len(args) -...  8.43 us
  transfers between devices with their start and end apart: 11, of which 5 were waited for; matrix products, arithmetic and copies ran while one was open for 1% of the time, Pallas kernels for 2%

profile of v1, /device:TPU:1, one launch (start us, length us, event | category | flops | bytes accessed | tf_op | source)
XLA Modules:
  0.0 257.9 jit_solution(15116956368911755437)
XLA Ops:
  0.7 0.6 copy-done.16
  1.3 0.9 copy-done.2
  2.2 0.9 copy-done.3
  3.2 0.9 copy-done.6
  4.1 1.0 prep.1
  5.1 4.4 %collective-permute-start = (bf16[1680,128]{1,0:T(8,128)(2,1)S(1)}, bf16[1680,128]{1,0:T(8,128)(2,1)S(1)}, u32[]{:S(2)}, u32[]{:S(2)}) collective-permute-start(bf16[1680,128]{1,0:T(8,128)(2,1)S(1)} %get-tuple-element.20), channel_id=1, source_target_pairs={{0,32},{32,0},{1,33},{33,1},{2,34},{34,2},{3,35},{35,3},{4,36},{36... | collective-permute-start | bytes 1290248 | tf_op jit(solution)/shard_map/ppermute | solution.py:26
  9.5 6.4 %all-gather = bf16[3360,128]{1,0:T(8,128)(2,1)S(1)} all-gather(bf16[1680,128]{1,0:T(8,128)(2,1)S(1)} %get-tuple-element.19), channel_id=2, replica_groups=mesh['zq'=8,'zp'=2,'c'=2,'tp'=16] {'c'}, dimensions={0}, use_global_device_ids=true | all-gather | bytes 1290240 | tf_op jit(solution)/shard_map/all_gather | solution.py:30
  15.9 8.1 %all-gather.1 = bf16[3360,128]{1,0:T(8,128)(2,1)S(1)} all-gather(bf16[1680,128]{1,0:T(8,128)(2,1)S(1)} %collective-permute-done), channel_id=3, replica_groups=mesh['zq'=8,'zp'=2,'c'=2,'tp'=16] {'c'}, dimensions={0}, use_global_device_ids=true | all-gather | bytes 1290240 | tf_op jit(solution)/shard_map/all_gather | solution.py:30
  24.1 0.6 shard_map.228
  24.6 36.1 %all_to_all.60.x_ref = bf16[8,16,1408]{2,1,0:T(8,128)(2,1)S(1)} all-to-all(bf16[8,16,1408]{2,1,0:T(8,128)(2,1)S(1)} %bitcast.59), channel_id=1, replica_groups=mesh['zq'=8,'zp'=2,'c'=2,'tp'=16] {'zq'}, dimensions={0} | all-to-all | bytes 720896 | tf_op jit(solution)/shard_map/all_to_all | solution.py:34
  60.8 0.9 shard_map.229
  61.7 4.7 %all-to-all-start.1 = ((bf16[8,16,688]{2,1,0:T(8,128)(2,1)}), bf16[8,16,688]{2,1,0:T(8,128)(2,1)S(1)}, u32[]{:S(2)}, u32[]{:S(2)}) async-start(bf16[8,16,688]{2,1,0:T(8,128)(2,1)} %shard_map.229), calls=%async_computation.1 | async-start | bytes 393216 | tf_op jit(solution)/shard_map/all_to_all | solution.py:34
  66.4 3.2 %collective-permute-start.1 = (bf16[688,128]{1,0:T(8,128)(2,1)S(1)}, bf16[688,128]{1,0:T(8,128)(2,1)S(1)}, u32[]{:S(2)}, u32[]{:S(2)}) collective-permute-start(bf16[688,128]{1,0:T(8,128)(2,1)S(1)} %copy-done.19), channel_id=1, source_target_pairs={{0,32},{32,0},{1,33},{33,1},{2,34},{34,2},{3,35},{35,3},{4,36},{36... | collective-permute-start | bytes 528392 | tf_op jit(solution)/shard_map/ppermute | solution.py:26
  70.1 2.1 collective-permute-start.2
  72.1 4.4 %all-gather.2 = bf16[1376,128]{1,0:T(8,128)(2,1)S(1)} all-gather(bf16[688,128]{1,0:T(8,128)(2,1)S(1)} %copy-done.19), channel_id=4, replica_groups=mesh['zq'=8,'zp'=2,'c'=2,'tp'=16] {'c'}, dimensions={0}, use_global_device_ids=true | all-gather | bytes 528384 | tf_op jit(solution)/shard_map/all_gather | solution.py:30
  76.6 3.2 %collective-permute-done.1 = bf16[688,128]{1,0:T(8,128)(2,1)S(1)} collective-permute-done((bf16[688,128]{1,0:T(8,128)(2,1)S(1)}, bf16[688,128]{1,0:T(8,128)(2,1)S(1)}, u32[]{:S(2)}, u32[]{:S(2)}) %collective-permute-start.1) | collective-permute-done | bytes 176160 | tf_op jit(solution)/shard_map/ppermute | solution.py:26
  79.7 4.6 %all-gather.3 = bf16[1376,128]{1,0:T(8,128)(2,1)S(1)} all-gather(bf16[688,128]{1,0:T(8,128)(2,1)S(1)} %collective-permute-done.1), channel_id=5, replica_groups=mesh['zq'=8,'zp'=2,'c'=2,'tp'=16] {'c'}, dimensions={0}, use_global_device_ids=true | all-gather | bytes 528384 | tf_op jit(solution)/shard_map/all_gather | solution.py:30
  84.4 0.9 shard_map.230
  85.3 6.8 %all-to-all-start.2 = ((bf16[16,8,512]{2,1,0:T(8,128)(2,1)}), bf16[16,8,512]{2,1,0:T(8,128)(2,1)S(1)}, u32[]{:S(2)}, u32[]{:S(2)}) async-start(bf16[16,8,512]{2,1,0:T(8,128)(2,1)} %bitcast.14), calls=%async_computation.2 | async-start | bytes 262144 | tf_op jit(solution)/shard_map/all_to_all | solution.py:34
  92.1 5.1 %all-gather.4 = bf16[1472,128]{1,0:T(8,128)(2,1)S(1)} all-gather(bf16[736,128]{1,0:T(8,128)(2,1)S(1)} %shard_map.232), channel_id=6, replica_groups=mesh['zq'=8,'zp'=2,'c'=2,'tp'=16] {'c'}, dimensions={0}, use_global_device_ids=true | all-gather | bytes 565248 | tf_op jit(solution)/shard_map/all_gather | solution.py:30
  97.2 2.1 all-gather.5
  99.3 0.7 shard_map.231
  100.0 7.1 %all-to-all-start.3 = ((bf16[16,8,512]{2,1,0:T(8,128)(2,1)}), bf16[16,8,512]{2,1,0:T(8,128)(2,1)S(1)}, u32[]{:S(2)}, u32[]{:S(2)}) async-start(bf16[16,8,512]{2,1,0:T(8,128)(2,1)} %get-tuple-element.23), calls=%async_computation.3 | async-start | bytes 262144 | tf_op jit(solution)/shard_map/all_to_all | solution.py:34
  107.0 6.8 %all-to-all-done.3.x_ref = bf16[16,8,512]{2,1,0:T(8,128)(2,1)S(1)} async-done(((bf16[16,8,512]{2,1,0:T(8,128)(2,1)}), bf16[16,8,512]{2,1,0:T(8,128)(2,1)S(1)}, u32[]{:S(2)}, u32[]{:S(2)}) %all-to-all-start.3) | async-done | bytes 131104 | tf_op jit(solution)/shard_map/all_to_all | solution.py:34
  113.9 0.9 shard_map.233
  114.8 7.6 %all-to-all-start.4 = ((bf16[8,16,640]{2,1,0:T(8,128)(2,1)}), bf16[8,16,640]{2,1,0:T(8,128)(2,1)S(1)}, u32[]{:S(2)}, u32[]{:S(2)}) async-start(bf16[8,16,640]{2,1,0:T(8,128)(2,1)} %bitcast.20), calls=%async_computation.4 | async-start | bytes 327680 | tf_op jit(solution)/shard_map/all_to_all | solution.py:34
  122.4 0.7 shard_map.237
  123.2 3.0 %collective-permute-start.3 = (bf16[2032,128]{1,0:T(8,128)(2,1)S(1)}, bf16[2032,128]{1,0:T(8,128)(2,1)S(1)}, u32[]{:S(2)}, u32[]{:S(2)}) collective-permute-start(bf16[2032,128]{1,0:T(8,128)(2,1)S(1)} %shard_map.237), channel_id=1, source_target_pairs={{0,32},{32,0},{1,33},{33,1},{2,34},{34,2},{3,35},{35,3},{4,36},{36... | collective-permute-start | bytes 1560584 | tf_op jit(solution)/shard_map/ppermute | solution.py:26
  126.9 9.5 %all-to-all-done.4.x_ref = bf16[8,16,640]{2,1,0:T(8,128)(2,1)S(1)} async-done(((bf16[8,16,640]{2,1,0:T(8,128)(2,1)}), bf16[8,16,640]{2,1,0:T(8,128)(2,1)S(1)}, u32[]{:S(2)}, u32[]{:S(2)}) %all-to-all-start.4) | async-done | bytes 163872 | tf_op jit(solution)/shard_map/all_to_all | solution.py:34
  136.4 0.6 copy-done.15
  137.0 1.2 shard_map.234
  138.2 16.1 %all_to_all.61.x_ref = bf16[8,16,128]{2,1,0:T(8,128)(2,1)S(1)} all-to-all(bf16[8,16,128]{2,1,0:T(8,128)(2,1)S(1)} %get-tuple-element.25), channel_id=1, replica_groups=mesh['zq'=8,'zp'=2,'c'=2,'tp'=16] {'zq'}, dimensions={0} | all-to-all | bytes 65536 | tf_op jit(solution)/shard_map/all_to_all | solution.py:34
  154.3 0.8 shard_map.235
  155.2 3.5 %all-to-all-start.6 = ((bf16[16,8,512]{2,1,0:T(8,128)(2,1)}), bf16[16,8,512]{2,1,0:T(8,128)(2,1)S(1)}, u32[]{:S(2)}, u32[]{:S(2)}) async-start(bf16[16,8,512]{2,1,0:T(8,128)(2,1)} %bitcast.24), calls=%async_computation.6 | async-start | bytes 262144 | tf_op jit(solution)/shard_map/all_to_all | solution.py:34
  158.7 7.0 %all-gather.6 = bf16[4064,128]{1,0:T(8,128)(2,1)S(1)} all-gather(bf16[2032,128]{1,0:T(8,128)(2,1)S(1)} %shard_map.237), channel_id=8, replica_groups=mesh['zq'=8,'zp'=2,'c'=2,'tp'=16] {'c'}, dimensions={0}, use_global_device_ids=true | all-gather | bytes 1560576 | tf_op jit(solution)/shard_map/all_gather | solution.py:30
  165.7 0.7 shard_map.236
  166.4 6.9 %all-to-all-start.7 = ((bf16[16,8,512]{2,1,0:T(8,128)(2,1)}), bf16[16,8,512]{2,1,0:T(8,128)(2,1)S(1)}, u32[]{:S(2)}, u32[]{:S(2)}) async-start(bf16[16,8,512]{2,1,0:T(8,128)(2,1)} %get-tuple-element.27), calls=%async_computation.7 | async-start | bytes 262144 | tf_op jit(solution)/shard_map/all_to_all | solution.py:34
  173.3 4.6 %all-gather.7 = bf16[4064,128]{1,0:T(8,128)(2,1)S(1)} all-gather(bf16[2032,128]{1,0:T(8,128)(2,1)S(1)} %collective-permute-done.3), channel_id=9, replica_groups=mesh['zq'=8,'zp'=2,'c'=2,'tp'=16] {'c'}, dimensions={0}, use_global_device_ids=true | all-gather | bytes 1560576 | tf_op jit(solution)/shard_map/all_gather | solution.py:30
  177.9 2.3 all-to-all-done.7.x_ref
  180.2 0.6 shard_map.238
  180.8 22.2 %all_to_all.62.x_ref = bf16[8,16,1408]{2,1,0:T(8,128)(2,1)S(1)} all-to-all(bf16[8,16,1408]{2,1,0:T(8,128)(2,1)S(1)} %bitcast.55), channel_id=1, replica_groups=mesh['zq'=8,'zp'=2,'c'=2,'tp'=16] {'zq'}, dimensions={0} | all-to-all | bytes 720896 | tf_op jit(solution)/shard_map/all_to_all | solution.py:34
  203.2 19.1 %all_to_all.63.x_ref = bf16[8,16,688]{2,1,0:T(8,128)(2,1)S(1)} all-to-all(bf16[8,16,688]{2,1,0:T(8,128)(2,1)S(1)} %shard_map.239), channel_id=1, replica_groups=mesh['zq'=8,'zp'=2,'c'=2,'tp'=16] {'zq'}, dimensions={0} | all-to-all | bytes 352256 | tf_op jit(solution)/shard_map/all_to_all | solution.py:34
  222.6 16.0 %all_to_all.64.sum_ref = bf16[16,8,512]{2,1,0:T(8,128)(2,1)S(1)} all-to-all(bf16[16,8,512]{2,1,0:T(8,128)(2,1)S(1)} %bitcast.58), channel_id=1, replica_groups=mesh['zq'=8,'zp'=2,'c'=2,'tp'=16] {'tp'}, dimensions={0} | all-to-all | bytes 262144 | tf_op jit(solution)/shard_map/all_to_all | solution.py:34
  238.6 0.7 shard_map.241
  239.3 9.6 %all-to-all-start.11 = ((bf16[64,8,128]{2,1,0:T(8,128)(2,1)}), bf16[64,8,128]{2,1,0:T(8,128)(2,1)S(1)}, u32[]{:S(2)}, u32[]{:S(2)}) async-start(bf16[64,8,128]{2,1,0:T(8,128)(2,1)} %shard_map.241), calls=%async_computation.11 | async-start | bytes 262144 | tf_op jit(solution)/shard_map/all_to_all | solution.py:34
  249.0 2.6 multiply_add_fusion
  251.6 5.7 %all-to-all-done.11 = bf16[64,8,128]{2,1,0:T(8,128)(2,1)S(1)} async-done(((bf16[64,8,128]{2,1,0:T(8,128)(2,1)}), bf16[64,8,128]{2,1,0:T(8,128)(2,1)S(1)}, u32[]{:S(2)}, u32[]{:S(2)}) %all-to-all-start.11) | async-done | bytes 131104 | tf_op jit(solution)/shard_map/all_to_all | solution.py:34
  257.3 0.7 copy.27
  (46 shorter events, 1.0 us)
Async XLA Ops:
  0.6 0.7 copy-start.16
  0.6 0.7 copy-start.17
  0.7 0.7 copy-start.18
  1.3 0.9 copy-start.2
  2.2 0.9 copy-start.3
  3.2 0.9 copy-start.6
  5.1 10.8 %collective-permute-start = (bf16[1680,128]{1,0:T(8,128)(2,1)S(1)}, bf16[1680,128]{1,0:T(8,128)(2,1)S(1)}, u32[]{:S(2)}, u32[]{:S(2)}) collective-permute-start(bf16[1680,128]{1,0:T(8,128)(2,1)S(1)} %get-tuple-element.20), channel_id=1, source_target_pairs={{0,32},{32,0},{1,33},{33,1},{2,34},{34,2},{3,35},{35,3},{4,36},{36... | collective-permute-start | bytes 1290248 | tf_op jit(solution)/shard_map/ppermute | solution.py:26
  60.8 5.6 %copy-start.19 = (bf16[688,128]{1,0:T(8,128)(2,1)S(1)}, bf16[688,128]{1,0:T(8,128)(2,1)}, u32[]{:S(2)}) copy-start(bf16[688,128]{1,0:T(8,128)(2,1)} %param.25) | copy-start | bytes 528388
  61.6 8.0 %copy-start.1 = (bf16[688,128]{1,0:T(8,128)(2,1)S(1)}, bf16[688,128]{1,0:T(8,128)(2,1)}, u32[]{:S(2)}) copy-start(bf16[688,128]{1,0:T(8,128)(2,1)} %refs_2_.3) | copy-start | bytes 528388
  61.6 8.0 %copy-start.7 = (bf16[128,128]{1,0:T(8,128)(2,1)S(1)}, bf16[128,128]{1,0:T(8,128)(2,1)}, u32[]{:S(2)}) copy-start(bf16[128,128]{1,0:T(8,128)(2,1)} %refs_0_.1) | copy-start | bytes 98308
  61.6 8.0 %copy-start.8 = (bf16[128,128]{1,0:T(8,128)(2,1)S(1)}, bf16[128,128]{1,0:T(8,128)(2,1)}, u32[]{:S(2)}) copy-start(bf16[128,128]{1,0:T(8,128)(2,1)} %refs_1_.1) | copy-start | bytes 98308
  61.6 8.0 %copy-start.9 = (bf16[128,128]{1,0:T(8,128)(2,1)S(1)}, bf16[128,128]{1,0:T(8,128)(2,1)}, u32[]{:S(2)}) copy-start(bf16[128,128]{1,0:T(8,128)(2,1)} %refs_2_.2) | copy-start | bytes 98308
  61.7 8.0 %copy-start.10 = (bf16[128,128]{1,0:T(8,128)(2,1)S(1)}, bf16[128,128]{1,0:T(8,128)(2,1)}, u32[]{:S(2)}) copy-start(bf16[128,128]{1,0:T(8,128)(2,1)} %refs_3_.1) | copy-start | bytes 98308
  61.7 8.0 %copy-start.11 = (bf16[128,128]{1,0:T(8,128)(2,1)S(1)}, bf16[128,128]{1,0:T(8,128)(2,1)}, u32[]{:S(2)}) copy-start(bf16[128,128]{1,0:T(8,128)(2,1)} %refs_6_.1) | copy-start | bytes 98308
  61.7 8.0 %copy-start.13 = (bf16[128,16]{0,1:T(8,128)(2,1)S(1)}, bf16[128,16]{0,1:T(8,128)(2,1)}, u32[]{:S(2)}) copy-start(bf16[128,16]{0,1:T(8,128)(2,1)} %param.31) | copy-start | bytes 12292
  61.7 8.0 %copy-start.14 = (bf16[128,16]{0,1:T(8,128)(2,1)S(1)}, bf16[128,16]{0,1:T(8,128)(2,1)}, u32[]{:S(2)}) copy-start(bf16[128,16]{0,1:T(8,128)(2,1)} %param.32) | copy-start | bytes 12292
  61.7 22.7 %all-to-all-start.1 = ((bf16[8,16,688]{2,1,0:T(8,128)(2,1)}), bf16[8,16,688]{2,1,0:T(8,128)(2,1)S(1)}, u32[]{:S(2)}, u32[]{:S(2)}) async-start(bf16[8,16,688]{2,1,0:T(8,128)(2,1)} %shard_map.229), calls=%async_computation.1 | async-start | bytes 393216 | tf_op jit(solution)/shard_map/all_to_all | solution.py:34
  66.4 13.3 %collective-permute-start.1 = (bf16[688,128]{1,0:T(8,128)(2,1)S(1)}, bf16[688,128]{1,0:T(8,128)(2,1)S(1)}, u32[]{:S(2)}, u32[]{:S(2)}) collective-permute-start(bf16[688,128]{1,0:T(8,128)(2,1)S(1)} %copy-done.19), channel_id=1, source_target_pairs={{0,32},{32,0},{1,33},{33,1},{2,34},{34,2},{3,35},{35,3},{4,36},{36... | collective-permute-start | bytes 528392 | tf_op jit(solution)/shard_map/ppermute | solution.py:26
  70.1 27.2 %collective-permute-start.2 = (bf16[736,128]{1,0:T(8,128)(2,1)S(1)}, bf16[736,128]{1,0:T(8,128)(2,1)S(1)}, u32[]{:S(2)}, u32[]{:S(2)}) collective-permute-start(bf16[736,128]{1,0:T(8,128)(2,1)S(1)} %shard_map.232), channel_id=1, source_target_pairs={{0,32},{32,0},{1,33},{33,1},{2,34},{34,2},{3,35},{35,3},{4,36},{36... | collective-permute-start | bytes 565256 | tf_op jit(solution)/shard_map/ppermute | solution.py:26
  85.3 14.0 %all-to-all-start.2 = ((bf16[16,8,512]{2,1,0:T(8,128)(2,1)}), bf16[16,8,512]{2,1,0:T(8,128)(2,1)S(1)}, u32[]{:S(2)}, u32[]{:S(2)}) async-start(bf16[16,8,512]{2,1,0:T(8,128)(2,1)} %bitcast.14), calls=%async_computation.2 | async-start | bytes 262144 | tf_op jit(solution)/shard_map/all_to_all | solution.py:34
  100.0 22.4 %copy-start.5 = (bf16[128,688]{0,1:T(8,128)(2,1)S(1)}, bf16[128,688]{0,1:T(8,128)(2,1)}, u32[]{:S(2)}) copy-start(bf16[128,688]{0,1:T(8,128)(2,1)} %param.40) | copy-start | bytes 528388
  100.0 13.9 %all-to-all-start.3 = ((bf16[16,8,512]{2,1,0:T(8,128)(2,1)}), bf16[16,8,512]{2,1,0:T(8,128)(2,1)S(1)}, u32[]{:S(2)}, u32[]{:S(2)}) async-start(bf16[16,8,512]{2,1,0:T(8,128)(2,1)} %get-tuple-element.23), calls=%async_computation.3 | async-start | bytes 262144 | tf_op jit(solution)/shard_map/all_to_all | solution.py:34
  113.9 22.5 %copy-start = (f32[16,1,128,128]{3,2,1,0:T(8,128)S(1)}, f32[16,1,128,128]{3,2,1,0:T(8,128)}, u32[]{:S(2)}) copy-start(f32[16,1,128,128]{3,2,1,0:T(8,128)} %param.34) | copy-start | bytes 3145732
  114.8 7.6 %copy-start.4 = (bf16[128,688]{0,1:T(8,128)(2,1)S(1)}, bf16[128,688]{0,1:T(8,128)(2,1)}, u32[]{:S(2)}) copy-start(bf16[128,688]{0,1:T(8,128)(2,1)} %param.39) | copy-start | bytes 528388
  114.8 21.5 %all-to-all-start.4 = ((bf16[8,16,640]{2,1,0:T(8,128)(2,1)}), bf16[8,16,640]{2,1,0:T(8,128)(2,1)S(1)}, u32[]{:S(2)}, u32[]{:S(2)}) async-start(bf16[8,16,640]{2,1,0:T(8,128)(2,1)} %bitcast.20), calls=%async_computation.4 | async-start | bytes 327680 | tf_op jit(solution)/shard_map/all_to_all | solution.py:34
  122.4 13.9 %copy-start.12 = (f32[16,1,128]{2,1,0:T(1,128)S(1)}, f32[16,1,128]{2,1,0:T(1,128)}, u32[]{:S(2)}) copy-start(f32[16,1,128]{2,1,0:T(1,128)} %param.35) | copy-start | bytes 24580
  123.2 50.1 %collective-permute-start.3 = (bf16[2032,128]{1,0:T(8,128)(2,1)S(1)}, bf16[2032,128]{1,0:T(8,128)(2,1)S(1)}, u32[]{:S(2)}, u32[]{:S(2)}) collective-permute-start(bf16[2032,128]{1,0:T(8,128)(2,1)S(1)} %shard_map.237), channel_id=1, source_target_pairs={{0,32},{32,0},{1,33},{33,1},{2,34},{34,2},{3,35},{35,3},{4,36},{36... | collective-permute-start | bytes 1560584 | tf_op jit(solution)/shard_map/ppermute | solution.py:26
  136.4 0.7 copy-start.15
  155.2 10.5 %all-to-all-start.6 = ((bf16[16,8,512]{2,1,0:T(8,128)(2,1)}), bf16[16,8,512]{2,1,0:T(8,128)(2,1)S(1)}, u32[]{:S(2)}, u32[]{:S(2)}) async-start(bf16[16,8,512]{2,1,0:T(8,128)(2,1)} %bitcast.24), calls=%async_computation.6 | async-start | bytes 262144 | tf_op jit(solution)/shard_map/all_to_all | solution.py:34
  166.4 13.8 %all-to-all-start.7 = ((bf16[16,8,512]{2,1,0:T(8,128)(2,1)}), bf16[16,8,512]{2,1,0:T(8,128)(2,1)S(1)}, u32[]{:S(2)}, u32[]{:S(2)}) async-start(bf16[16,8,512]{2,1,0:T(8,128)(2,1)} %get-tuple-element.27), calls=%async_computation.7 | async-start | bytes 262144 | tf_op jit(solution)/shard_map/all_to_all | solution.py:34
  239.3 18.0 %all-to-all-start.11 = ((bf16[64,8,128]{2,1,0:T(8,128)(2,1)}), bf16[64,8,128]{2,1,0:T(8,128)(2,1)S(1)}, u32[]{:S(2)}, u32[]{:S(2)}) async-start(bf16[64,8,128]{2,1,0:T(8,128)(2,1)} %shard_map.241), calls=%async_computation.11 | async-start | bytes 262144 | tf_op jit(solution)/shard_map/all_to_all | solution.py:34

commit v2 on v1

--- a/solution.py
+++ b/solution.py
@@ -379,11 +379,10 @@
         up_first.T,
     )
     came = swap(sent)
-    down_came = swap(down_first)
     heads = w_ingate.shape[1]
     middle = pack(
         [(i, 0, 128) for i in range(4)]
-        + [(4, 0, heads), (5, 0, heads), (6, 0, 128), (7, FFL - 64, 64)],
+        + [(4, 0, heads), (5, 0, heads), (6, 0, 128), (7, FFL - 64, 64), (8, 0, FFL)],
         w_query,
         w_key,
         w_value,
@@ -392,13 +391,13 @@
         w_forget.T,
         w_project,
         down_second,
+        down_first,
     )
     middle_came = swap(middle)
     last = pack(gate_up(0, 1) + [(2, 0, FFL - 64)], gate_second.T, up_second.T, down_second)
     last_came = swap(last)
 
     first_own, first_other = both_cores(kept), both_cores(came)
-    down_own, down_other = both_cores(down_first), both_cores(down_came)
     middle_own, middle_other = both_cores(middle), both_cores(middle_came)
     last_own, last_other = both_cores(last), both_cores(last_came)
 
@@ -407,7 +406,7 @@
     wide, rows, gains = call(
         first_kernel, (wide_shape, copied, jax.ShapeDtypeStruct((3, 1, 512), F32)), 1
     )(core_at, first_own, first_other)
-    came = half_step(wide, (((0, 0, FFL),), (down_own, down_other)))
+    came = half_step(wide, (((0, 736, FFL),), (middle_own, middle_other)))
     after_first, copies = call(residual_kernel(0.5), (shard, copied), 1)(shard_at, came, rows)
     copies = exchange(copies, "tp")
 

time: 259 us -> 265 us (1.023)
  waiting for transfers between devices: 27.5 us -> 40.8 us
  blocking collectives: 152 us -> 143 us
    ppermute x4 -> x3, waiting for transfers between devices: 3.17 us -> 11.4 us  [swap(): return lax.ppermute(array, 'zp', [(0, 1), (1, 0)])]
    all_gather x8 -> x6, blocking collectives: 42.4 us -> 34.9 us  [both_cores(): return lax.all_gather(array, 'c')]
    all_to_all x7, waiting for transfers between devices: 24.3 us -> 29.4 us  [exchange(): return lax.all_to_all(parts, axis, split_axis=0, concat_axis=0, tiled=True)]
    unnamed x40 -> x56, local copies, waits for them, and re-layouts: 4.12 us -> 6.19 us
    ppermute x4 -> x3, starting transfers between devices: 12.7 us -> 10.7 us  [swap(): return lax.ppermute(array, 'zp', [(0, 1), (1, 0)])]
  transfers between devices with their start and end apart: 11 -> 10, of which waited for: 5 -> 6; matrix products, arithmetic and copies ran while one was open for 1% -> 1% of each run, Pallas kernels for 2% -> 2%
where the time goes in v2:
time: 265 us; the launch traced here: 263 us
  blocking collectives  143 us (54%)
  starting transfers between devices  56.5 us (21%)
  waiting for transfers between devices  40.8 us (15%)
  Pallas kernels  11.7 us (4%)
  local copies, waits for them, and re-layouts  6.97 us (3%)
    all_to_all x5, blocking collectives, exchange(): return lax.all_to_all(parts, axis, split_axis=0, concat_axis=0, tiled=True)  108 us
    all_to_all x7, starting transfers between devices, exchange(): return lax.all_to_all(parts, axis, split_axis=0, concat_axis=0, tiled=True)  45.8 us
    all_gather x6, blocking collectives, both_cores(): return lax.all_gather(array, 'c')  34.9 us
    all_to_all x7, waiting for transfers between devices, exchange(): return lax.all_to_all(parts, axis, split_axis=0, concat_axis=0, tiled=True)  29.4 us
    ppermute x3, waiting for transfers between devices, swap(): return lax.ppermute(array, 'zp', [(0, 1), (1, 0)])  11.4 us
    ppermute x3, starting transfers between devices, swap(): return lax.ppermute(array, 'zp', [(0, 1), (1, 0)])  10.7 us
    pallas_call x12, Pallas kernels, run(): pl.pallas_call(kernel, in_specs=[smem] * scalars + [vmem] * (len(args) -...  9.34 us
    unnamed x56, local copies, waits for them, and re-layouts  6.19 us
  transfers between devices with their start and end apart: 10, of which 6 were waited for; matrix products, arithmetic and copies ran while one was open for 1% of the time, Pallas kernels for 2%

profile of v2, /device:TPU:1, one launch (start us, length us, event | category | flops | bytes accessed | tf_op | source)
XLA Modules:
  0.0 263.5 jit_solution(12588974449568573717)
XLA Ops:
  0.7 0.6 copy-done.25
  1.3 0.9 copy-done.3
  2.2 0.9 copy-done.4
  3.2 0.9 copy-done.7
  4.1 1.0 prep.1
  5.1 4.4 %collective-permute-start = (bf16[1680,128]{1,0:T(8,128)(2,1)S(1)}, bf16[1680,128]{1,0:T(8,128)(2,1)S(1)}, u32[]{:S(2)}, u32[]{:S(2)}) collective-permute-start(bf16[1680,128]{1,0:T(8,128)(2,1)S(1)} %get-tuple-element.20), channel_id=1, source_target_pairs={{0,32},{32,0},{1,33},{33,1},{2,34},{34,2},{3,35},{35,3},{4,36},{36... | collective-permute-start | bytes 1290248 | tf_op jit(solution)/shard_map/ppermute | solution.py:26
  9.5 6.4 %all-gather = bf16[3360,128]{1,0:T(8,128)(2,1)S(1)} all-gather(bf16[1680,128]{1,0:T(8,128)(2,1)S(1)} %get-tuple-element.19), channel_id=2, replica_groups=mesh['zq'=8,'zp'=2,'c'=2,'tp'=16] {'c'}, dimensions={0}, use_global_device_ids=true | all-gather | bytes 1290240 | tf_op jit(solution)/shard_map/all_gather | solution.py:30
  15.9 8.1 %all-gather.1 = bf16[3360,128]{1,0:T(8,128)(2,1)S(1)} all-gather(bf16[1680,128]{1,0:T(8,128)(2,1)S(1)} %collective-permute-done), channel_id=3, replica_groups=mesh['zq'=8,'zp'=2,'c'=2,'tp'=16] {'c'}, dimensions={0}, use_global_device_ids=true | all-gather | bytes 1290240 | tf_op jit(solution)/shard_map/all_gather | solution.py:30
  24.1 0.6 shard_map.228
  24.6 36.1 %all_to_all.60.x_ref = bf16[8,16,1408]{2,1,0:T(8,128)(2,1)S(1)} all-to-all(bf16[8,16,1408]{2,1,0:T(8,128)(2,1)S(1)} %bitcast.57), channel_id=1, replica_groups=mesh['zq'=8,'zp'=2,'c'=2,'tp'=16] {'zq'}, dimensions={0} | all-to-all | bytes 720896 | tf_op jit(solution)/shard_map/all_to_all | solution.py:34
  60.8 0.9 shard_map.229
  61.7 4.7 %all-to-all-start.1 = ((bf16[8,16,688]{2,1,0:T(8,128)(2,1)}), bf16[8,16,688]{2,1,0:T(8,128)(2,1)S(1)}, u32[]{:S(2)}, u32[]{:S(2)}) async-start(bf16[8,16,688]{2,1,0:T(8,128)(2,1)} %shard_map.229), calls=%async_computation.1 | async-start | bytes 393216 | tf_op jit(solution)/shard_map/all_to_all | solution.py:34
  67.1 3.2 %collective-permute-start.1 = (bf16[1424,128]{1,0:T(8,128)(2,1)S(1)}, bf16[1424,128]{1,0:T(8,128)(2,1)S(1)}, u32[]{:S(2)}, u32[]{:S(2)}) collective-permute-start(bf16[1424,128]{1,0:T(8,128)(2,1)S(1)} %shard_map.230), channel_id=1, source_target_pairs={{0,32},{32,0},{1,33},{33,1},{2,34},{34,2},{3,35},{35,3},{4,36},{36... | collective-permute-start | bytes 1093640 | tf_op jit(solution)/shard_map/ppermute | solution.py:26
  70.3 3.2 %all-gather.2 = bf16[2848,128]{1,0:T(8,128)(2,1)S(1)} all-gather(bf16[1424,128]{1,0:T(8,128)(2,1)S(1)} %shard_map.230), channel_id=4, replica_groups=mesh['zq'=8,'zp'=2,'c'=2,'tp'=16] {'c'}, dimensions={0}, use_global_device_ids=true | all-gather | bytes 1093632 | tf_op jit(solution)/shard_map/all_gather | solution.py:30
  73.4 11.4 %collective-permute-done.1 = bf16[1424,128]{1,0:T(8,128)(2,1)S(1)} collective-permute-done((bf16[1424,128]{1,0:T(8,128)(2,1)S(1)}, bf16[1424,128]{1,0:T(8,128)(2,1)S(1)}, u32[]{:S(2)}, u32[]{:S(2)}) %collective-permute-start.1) | collective-permute-done | bytes 364576 | tf_op jit(solution)/shard_map/ppermute | solution.py:26
  84.9 2.9 %all-gather.3 = bf16[2848,128]{1,0:T(8,128)(2,1)S(1)} all-gather(bf16[1424,128]{1,0:T(8,128)(2,1)S(1)} %collective-permute-done.1), channel_id=5, replica_groups=mesh['zq'=8,'zp'=2,'c'=2,'tp'=16] {'c'}, dimensions={0}, use_global_device_ids=true | all-gather | bytes 1093632 | tf_op jit(solution)/shard_map/all_gather | solution.py:30
  87.8 0.9 shard_map.231
  88.7 6.8 %all-to-all-start.2 = ((bf16[16,8,512]{2,1,0:T(8,128)(2,1)}), bf16[16,8,512]{2,1,0:T(8,128)(2,1)S(1)}, u32[]{:S(2)}, u32[]{:S(2)}) async-start(bf16[16,8,512]{2,1,0:T(8,128)(2,1)} %bitcast.16), calls=%async_computation.2 | async-start | bytes 262144 | tf_op jit(solution)/shard_map/all_to_all | solution.py:34
  95.5 6.8 %all-to-all-done.2.sum_ref = bf16[16,8,512]{2,1,0:T(8,128)(2,1)S(1)} async-done(((bf16[16,8,512]{2,1,0:T(8,128)(2,1)}), bf16[16,8,512]{2,1,0:T(8,128)(2,1)S(1)}, u32[]{:S(2)}, u32[]{:S(2)}) %all-to-all-start.2) | async-done | bytes 131104 | tf_op jit(solution)/shard_map/all_to_all | solution.py:34
  102.3 0.7 shard_map.232
  103.0 0.6 copy-done.18
  103.6 3.5 %all-to-all-start.3 = ((bf16[16,8,512]{2,1,0:T(8,128)(2,1)}), bf16[16,8,512]{2,1,0:T(8,128)(2,1)S(1)}, u32[]{:S(2)}, u32[]{:S(2)}) async-start(bf16[16,8,512]{2,1,0:T(8,128)(2,1)} %get-tuple-element.23), calls=%async_computation.3 | async-start | bytes 262144 | tf_op jit(solution)/shard_map/all_to_all | solution.py:34
  107.1 6.8 %all-to-all-done.3.x_ref = bf16[16,8,512]{2,1,0:T(8,128)(2,1)S(1)} async-done(((bf16[16,8,512]{2,1,0:T(8,128)(2,1)}), bf16[16,8,512]{2,1,0:T(8,128)(2,1)S(1)}, u32[]{:S(2)}, u32[]{:S(2)}) %all-to-all-start.3) | async-done | bytes 131104 | tf_op jit(solution)/shard_map/all_to_all | solution.py:34
  113.9 0.9 shard_map.233
  114.9 10.5 %all-to-all-start.4 = ((bf16[8,16,640]{2,1,0:T(8,128)(2,1)}), bf16[8,16,640]{2,1,0:T(8,128)(2,1)S(1)}, u32[]{:S(2)}, u32[]{:S(2)}) async-start(bf16[8,16,640]{2,1,0:T(8,128)(2,1)} %bitcast.18), calls=%async_computation.4 | async-start | bytes 327680 | tf_op jit(solution)/shard_map/all_to_all | solution.py:34
  125.4 0.9 copy-done.6
  126.3 0.7 shard_map.237
  127.0 3.1 %collective-permute-start.2 = (bf16[2032,128]{1,0:T(8,128)(2,1)S(1)}, bf16[2032,128]{1,0:T(8,128)(2,1)}, u32[]{:S(2)}, u32[]{:S(2)}) collective-permute-start(bf16[2032,128]{1,0:T(8,128)(2,1)S(1)} %shard_map.237), channel_id=1, source_target_pairs={{0,32},{32,0},{1,33},{33,1},{2,34},{34,2},{3,35},{35,3},{4,36},{36... | collective-permute-start | bytes 1560584 | tf_op jit(solution)/shard_map/ppermute | solution.py:26
  130.8 9.1 %all-to-all-done.4.x_ref = bf16[8,16,640]{2,1,0:T(8,128)(2,1)S(1)} async-done(((bf16[8,16,640]{2,1,0:T(8,128)(2,1)}), bf16[8,16,640]{2,1,0:T(8,128)(2,1)S(1)}, u32[]{:S(2)}, u32[]{:S(2)}) %all-to-all-start.4) | async-done | bytes 163872 | tf_op jit(solution)/shard_map/all_to_all | solution.py:34
  139.9 0.6 copy-done.24
  140.6 1.2 shard_map.234
  141.8 14.1 %all_to_all.61.x_ref = bf16[8,16,128]{2,1,0:T(8,128)(2,1)S(1)} all-to-all(bf16[8,16,128]{2,1,0:T(8,128)(2,1)S(1)} %get-tuple-element.25), channel_id=1, replica_groups=mesh['zq'=8,'zp'=2,'c'=2,'tp'=16] {'zq'}, dimensions={0} | all-to-all | bytes 65536 | tf_op jit(solution)/shard_map/all_to_all | solution.py:34
  155.9 0.8 shard_map.235
  156.7 3.8 %all-to-all-start.6 = ((bf16[16,8,512]{2,1,0:T(8,128)(2,1)}), bf16[16,8,512]{2,1,0:T(8,128)(2,1)S(1)}, u32[]{:S(2)}, u32[]{:S(2)}) async-start(bf16[16,8,512]{2,1,0:T(8,128)(2,1)} %bitcast.22), calls=%async_computation.6 | async-start | bytes 262144 | tf_op jit(solution)/shard_map/all_to_all | solution.py:34
  160.6 8.8 %all-gather.4 = bf16[4064,128]{1,0:T(8,128)(2,1)S(1)} all-gather(bf16[2032,128]{1,0:T(8,128)(2,1)S(1)} %shard_map.237), channel_id=6, replica_groups=mesh['zq'=8,'zp'=2,'c'=2,'tp'=16] {'c'}, dimensions={0}, use_global_device_ids=true | all-gather | bytes 1560576 | tf_op jit(solution)/shard_map/all_gather | solution.py:30
  169.4 0.7 shard_map.236
  170.1 6.9 %all-to-all-start.7 = ((bf16[16,8,512]{2,1,0:T(8,128)(2,1)}), bf16[16,8,512]{2,1,0:T(8,128)(2,1)}, u32[]{:S(2)}, u32[]{:S(2)}) async-start(bf16[16,8,512]{2,1,0:T(8,128)(2,1)} %get-tuple-element.27), calls=%async_computation.7 | async-start | bytes 262144 | tf_op jit(solution)/shard_map/all_to_all | solution.py:34
  177.1 5.4 %all-gather.5 = bf16[4064,128]{1,0:T(8,128)(2,1)S(1)} all-gather(bf16[2032,128]{1,0:T(8,128)(2,1)} %collective-permute-done.2), channel_id=7, replica_groups=mesh['zq'=8,'zp'=2,'c'=2,'tp'=16] {'c'}, dimensions={0}, use_global_device_ids=true | all-gather | bytes 1560576 | tf_op jit(solution)/shard_map/all_gather | solution.py:30
  182.5 1.5 all-to-all-done.7.x_ref
  183.9 1.5 shard_map.238
  185.5 22.2 %all_to_all.62.x_ref = bf16[8,16,1408]{2,1,0:T(8,128)(2,1)S(1)} all-to-all(bf16[8,16,1408]{2,1,0:T(8,128)(2,1)S(1)} %bitcast.55), channel_id=1, replica_groups=mesh['zq'=8,'zp'=2,'c'=2,'tp'=16] {'zq'}, dimensions={0} | all-to-all | bytes 720896 | tf_op jit(solution)/shard_map/all_to_all | solution.py:34
  207.8 21.1 %all_to_all.63.x_ref = bf16[8,16,688]{2,1,0:T(8,128)(2,1)S(1)} all-to-all(bf16[8,16,688]{2,1,0:T(8,128)(2,1)S(1)} %shard_map.239), channel_id=1, replica_groups=mesh['zq'=8,'zp'=2,'c'=2,'tp'=16] {'zq'}, dimensions={0} | all-to-all | bytes 352256 | tf_op jit(solution)/shard_map/all_to_all | solution.py:34
  229.2 14.9 %all_to_all.64.sum_ref = bf16[16,8,512]{2,1,0:T(8,128)(2,1)S(1)} all-to-all(bf16[16,8,512]{2,1,0:T(8,128)(2,1)S(1)} %bitcast.56), channel_id=1, replica_groups=mesh['zq'=8,'zp'=2,'c'=2,'tp'=16] {'tp'}, dimensions={0} | all-to-all | bytes 262144 | tf_op jit(solution)/shard_map/all_to_all | solution.py:34
  244.1 0.7 shard_map.241
  244.8 9.6 %all-to-all-start.11 = ((bf16[64,8,128]{2,1,0:T(8,128)(2,1)}), bf16[64,8,128]{2,1,0:T(8,128)(2,1)S(1)}, u32[]{:S(2)}, u32[]{:S(2)}) async-start(bf16[64,8,128]{2,1,0:T(8,128)(2,1)} %shard_map.241), calls=%async_computation.11 | async-start | bytes 262144 | tf_op jit(solution)/shard_map/all_to_all | solution.py:34
  255.1 2.5 multiply_add_fusion
  257.7 5.1 %all-to-all-done.11 = bf16[64,8,128]{2,1,0:T(8,128)(2,1)S(1)} async-done(((bf16[64,8,128]{2,1,0:T(8,128)(2,1)}), bf16[64,8,128]{2,1,0:T(8,128)(2,1)S(1)}, u32[]{:S(2)}, u32[]{:S(2)}) %all-to-all-start.11) | async-done | bytes 131104 | tf_op jit(solution)/shard_map/all_to_all | solution.py:34
  262.8 0.7 copy.27
  (58 shorter events, 1.8 us)
Async XLA Ops:
  0.6 0.7 copy-start.25
  0.6 0.7 copy-start.26
  0.7 0.7 copy-start.27
  1.3 0.9 copy-start.3
  2.2 0.9 copy-start.4
  3.2 0.9 copy-start.7
  5.1 10.8 %collective-permute-start = (bf16[1680,128]{1,0:T(8,128)(2,1)S(1)}, bf16[1680,128]{1,0:T(8,128)(2,1)S(1)}, u32[]{:S(2)}, u32[]{:S(2)}) collective-permute-start(bf16[1680,128]{1,0:T(8,128)(2,1)S(1)} %get-tuple-element.20), channel_id=1, source_target_pairs={{0,32},{32,0},{1,33},{33,1},{2,34},{34,2},{3,35},{35,3},{4,36},{36... | collective-permute-start | bytes 1290248 | tf_op jit(solution)/shard_map/ppermute | solution.py:26
  60.8 5.6 %copy-start.9 = (bf16[128,128]{1,0:T(8,128)(2,1)S(1)}, bf16[128,128]{1,0:T(8,128)(2,1)}, u32[]{:S(2)}) copy-start(bf16[128,128]{1,0:T(8,128)(2,1)} %refs_1_.1) | copy-start | bytes 98308
  60.8 5.6 %copy-start.10 = (bf16[128,128]{1,0:T(8,128)(2,1)S(1)}, bf16[128,128]{1,0:T(8,128)(2,1)}, u32[]{:S(2)}) copy-start(bf16[128,128]{1,0:T(8,128)(2,1)} %refs_2_.2) | copy-start | bytes 98308
  60.8 5.6 %copy-start.11 = (bf16[128,128]{1,0:T(8,128)(2,1)S(1)}, bf16[128,128]{1,0:T(8,128)(2,1)}, u32[]{:S(2)}) copy-start(bf16[128,128]{1,0:T(8,128)(2,1)} %refs_3_.1) | copy-start | bytes 98308
  60.8 5.6 %copy-start.12 = (bf16[128,128]{1,0:T(8,128)(2,1)S(1)}, bf16[128,128]{1,0:T(8,128)(2,1)}, u32[]{:S(2)}) copy-start(bf16[128,128]{1,0:T(8,128)(2,1)} %refs_6_.1) | copy-start | bytes 98308
  61.6 4.8 %copy-start.1 = (bf16[688,128]{1,0:T(8,128)(2,1)S(1)}, bf16[688,128]{1,0:T(8,128)(2,1)}, u32[]{:S(2)}) copy-start(bf16[688,128]{1,0:T(8,128)(2,1)} %refs_2_.3) | copy-start | bytes 528388
  61.7 4.8 %copy-start.2 = (bf16[688,128]{1,0:T(8,128)(2,1)S(1)}, bf16[688,128]{1,0:T(8,128)(2,1)}, u32[]{:S(2)}) copy-start(bf16[688,128]{1,0:T(8,128)(2,1)} %refs_8_.1) | copy-start | bytes 528388
  61.7 4.8 %copy-start.8 = (bf16[128,128]{1,0:T(8,128)(2,1)S(1)}, bf16[128,128]{1,0:T(8,128)(2,1)}, u32[]{:S(2)}) copy-start(bf16[128,128]{1,0:T(8,128)(2,1)} %refs_0_.1) | copy-start | bytes 98308
  61.7 4.8 %copy-start.22 = (bf16[128,16]{0,1:T(8,128)(2,1)S(1)}, bf16[128,16]{0,1:T(8,128)(2,1)}, u32[]{:S(2)}) copy-start(bf16[128,16]{0,1:T(8,128)(2,1)} %param.31) | copy-start | bytes 12292
  61.7 4.8 %copy-start.23 = (bf16[128,16]{0,1:T(8,128)(2,1)S(1)}, bf16[128,16]{0,1:T(8,128)(2,1)}, u32[]{:S(2)}) copy-start(bf16[128,16]{0,1:T(8,128)(2,1)} %param.32) | copy-start | bytes 12292
  61.7 26.1 %all-to-all-start.1 = ((bf16[8,16,688]{2,1,0:T(8,128)(2,1)}), bf16[8,16,688]{2,1,0:T(8,128)(2,1)S(1)}, u32[]{:S(2)}, u32[]{:S(2)}) async-start(bf16[8,16,688]{2,1,0:T(8,128)(2,1)} %shard_map.229), calls=%async_computation.1 | async-start | bytes 393216 | tf_op jit(solution)/shard_map/all_to_all | solution.py:34
  67.1 17.8 %collective-permute-start.1 = (bf16[1424,128]{1,0:T(8,128)(2,1)S(1)}, bf16[1424,128]{1,0:T(8,128)(2,1)S(1)}, u32[]{:S(2)}, u32[]{:S(2)}) collective-permute-start(bf16[1424,128]{1,0:T(8,128)(2,1)S(1)} %shard_map.230), channel_id=1, source_target_pairs={{0,32},{32,0},{1,33},{33,1},{2,34},{34,2},{3,35},{35,3},{4,36},{36... | collective-permute-start | bytes 1093640 | tf_op jit(solution)/shard_map/ppermute | solution.py:26
  88.7 13.6 %all-to-all-start.2 = ((bf16[16,8,512]{2,1,0:T(8,128)(2,1)}), bf16[16,8,512]{2,1,0:T(8,128)(2,1)S(1)}, u32[]{:S(2)}, u32[]{:S(2)}) async-start(bf16[16,8,512]{2,1,0:T(8,128)(2,1)} %bitcast.16), calls=%async_computation.2 | async-start | bytes 262144 | tf_op jit(solution)/shard_map/all_to_all | solution.py:34
  103.0 0.6 copy-start.18
  103.6 10.3 %all-to-all-start.3 = ((bf16[16,8,512]{2,1,0:T(8,128)(2,1)}), bf16[16,8,512]{2,1,0:T(8,128)(2,1)S(1)}, u32[]{:S(2)}, u32[]{:S(2)}) async-start(bf16[16,8,512]{2,1,0:T(8,128)(2,1)} %get-tuple-element.23), calls=%async_computation.3 | async-start | bytes 262144 | tf_op jit(solution)/shard_map/all_to_all | solution.py:34
  113.9 11.4 %copy-start.5 = (bf16[128,688]{0,1:T(8,128)(2,1)S(1)}, bf16[128,688]{0,1:T(8,128)(2,1)}, u32[]{:S(2)}) copy-start(bf16[128,688]{0,1:T(8,128)(2,1)} %param.39) | copy-start | bytes 528388
  114.9 25.0 %copy-start = (f32[16,1,128,128]{3,2,1,0:T(8,128)S(1)}, f32[16,1,128,128]{3,2,1,0:T(8,128)}, u32[]{:S(2)}) copy-start(f32[16,1,128,128]{3,2,1,0:T(8,128)} %param.34) | copy-start | bytes 3145732
  114.9 25.0 %all-to-all-start.4 = ((bf16[8,16,640]{2,1,0:T(8,128)(2,1)}), bf16[8,16,640]{2,1,0:T(8,128)(2,1)S(1)}, u32[]{:S(2)}, u32[]{:S(2)}) async-start(bf16[8,16,640]{2,1,0:T(8,128)(2,1)} %bitcast.18), calls=%async_computation.4 | async-start | bytes 327680 | tf_op jit(solution)/shard_map/all_to_all | solution.py:34
  125.4 0.9 copy-start.6
  126.3 13.6 %copy-start.13 = (f32[16,1,128]{2,1,0:T(1,128)S(1)}, f32[16,1,128]{2,1,0:T(1,128)}, u32[]{:S(2)}) copy-start(f32[16,1,128]{2,1,0:T(1,128)} %param.35) | copy-start | bytes 24580
  127.0 50.0 %collective-permute-start.2 = (bf16[2032,128]{1,0:T(8,128)(2,1)S(1)}, bf16[2032,128]{1,0:T(8,128)(2,1)}, u32[]{:S(2)}, u32[]{:S(2)}) collective-permute-start(bf16[2032,128]{1,0:T(8,128)(2,1)S(1)} %shard_map.237), channel_id=1, source_target_pairs={{0,32},{32,0},{1,33},{33,1},{2,34},{34,2},{3,35},{35,3},{4,36},{36... | collective-permute-start | bytes 1560584 | tf_op jit(solution)/shard_map/ppermute | solution.py:26
  139.9 0.7 copy-start.24
  141.8 14.1 %copy-start.14 = (f32[16,128]{1,0:T(8,128)}, f32[16,128]{1,0:T(8,128)S(1)}, u32[]{:S(2)}) copy-start(f32[16,128]{1,0:T(8,128)S(1)} %get-tuple-element.30) | copy-start | bytes 24580
  141.8 14.1 %copy-start.16 = (f32[16,128]{1,0:T(8,128)}, f32[16,128]{1,0:T(8,128)S(1)}, u32[]{:S(2)}) copy-start(f32[16,128]{1,0:T(8,128)S(1)} %get-tuple-element.31) | copy-start | bytes 24580
  141.8 14.1 %copy-start.20 = (f32[16,128]{1,0:T(8,128)}, f32[16,128]{1,0:T(8,128)S(1)}, u32[]{:S(2)}) copy-start(f32[16,128]{1,0:T(8,128)S(1)} %get-tuple-element.29) | copy-start | bytes 24580
  156.7 12.7 %all-to-all-start.6 = ((bf16[16,8,512]{2,1,0:T(8,128)(2,1)}), bf16[16,8,512]{2,1,0:T(8,128)(2,1)S(1)}, u32[]{:S(2)}, u32[]{:S(2)}) async-start(bf16[16,8,512]{2,1,0:T(8,128)(2,1)} %bitcast.22), calls=%async_computation.6 | async-start | bytes 262144 | tf_op jit(solution)/shard_map/all_to_all | solution.py:34
  160.6 8.9 %copy-start.19 = (bf16[1,8,512]{2,1,0:T(8,128)(2,1)S(1)}, bf16[1,8,512]{2,1,0:T(8,128)(2,1)}, u32[]{:S(2)}) copy-start(bf16[1,8,512]{2,1,0:T(8,128)(2,1)} %copy-done.18) | copy-start | bytes 24580
  170.1 13.8 %all-to-all-start.7 = ((bf16[16,8,512]{2,1,0:T(8,128)(2,1)}), bf16[16,8,512]{2,1,0:T(8,128)(2,1)}, u32[]{:S(2)}, u32[]{:S(2)}) async-start(bf16[16,8,512]{2,1,0:T(8,128)(2,1)} %get-tuple-element.27), calls=%async_computation.7 | async-start | bytes 262144 | tf_op jit(solution)/shard_map/all_to_all | solution.py:34
  244.8 9.6 %copy-start.21 = (f32[16,128]{1,0:T(8,128)S(1)}, f32[16,128]{1,0:T(8,128)}, u32[]{:S(2)}) copy-start(f32[16,128]{1,0:T(8,128)} %copy-done.20) | copy-start | bytes 24580
  244.8 9.7 %copy-start.17 = (f32[16,128]{1,0:T(8,128)S(1)}, f32[16,128]{1,0:T(8,128)}, u32[]{:S(2)}) copy-start(f32[16,128]{1,0:T(8,128)} %copy-done.16) | copy-start | bytes 24580
  244.8 18.0 %all-to-all-start.11 = ((bf16[64,8,128]{2,1,0:T(8,128)(2,1)}), bf16[64,8,128]{2,1,0:T(8,128)(2,1)S(1)}, u32[]{:S(2)}, u32[]{:S(2)}) async-start(bf16[64,8,128]{2,1,0:T(8,128)(2,1)} %shard_map.241), calls=%async_computation.11 | async-start | bytes 262144 | tf_op jit(solution)/shard_map/all_to_all | solution.py:34
  254.4 0.7 copy-start.15

commit v3 on v2

--- a/solution.py
+++ b/solution.py
@@ -31,6 +31,11 @@
 
 
 def exchange(parts, axis):
+    if axis == "zq":
+        groups = [[2 * q + (role ^ (q >= 4)) for q in range(8)] for role in range(2)]
+        return lax.all_to_all(
+            parts, ("zq", "zp"), split_axis=0, concat_axis=0, axis_index_groups=groups, tiled=True
+        )
     return lax.all_to_all(parts, axis, split_axis=0, concat_axis=0, tiled=True)
 
 
@@ -82,7 +87,7 @@
     out_ref[:, WIDE - 128 :] = put_squares(total[:, WIDE - 128 :], squares, 112).astype(BF)
 
 
-def prep_kernel(pair_ref, tokens_ref, first_ref, mix_ref, second_ref, gate_ref, up_ref, *refs):
+def prep_kernel(role_ref, tokens_ref, first_ref, mix_ref, second_ref, gate_ref, up_ref, *refs):
     kept_ref, sent_ref, sems = refs
     copies = []
     for ref in (kept_ref, sent_ref):
@@ -99,11 +104,11 @@
         gains += pieces(ref[...])
     rows = [g.astype(F32) for g in gains] + [jnp.zeros((7, 128), F32)]
     rows = jnp.concatenate(rows, axis=0).astype(BF)
-    for ref, which in ((kept_ref, pair_ref[0]), (sent_ref, 1 - pair_ref[0])):
+    for ref, which in ((kept_ref, role_ref[0]), (sent_ref, 1 - role_ref[0])):
         for core in range(2):
             for group in range(8):
                 at = 128 * core + 16 * group
-                ref[at : at + 16] = tokens_ref[group, which, core]
+                ref[at : at + 16] = tokens_ref[group, which if group < 4 else 1 - which, core]
         ref[256:HERE] = rows
     for copy in copies:
         copy.wait()
@@ -255,6 +260,15 @@
                 out_ref[(2 * pair + core) * 16 + i] = blocks[pair]
 
 
+def unpack_kernel(upper_ref, came_ref, out_ref):
+    for group in range(8):
+        for role in range(2):
+            base = role if group < 4 else 1 - role
+            chip = upper_ref[0] if base == 0 else 1 - upper_ref[0]
+            for core in range(2):
+                out_ref[group, role, core] = came_ref[chip, core, group]
+
+
 def call(kernel, out_shapes, scalars=0):
     smem = pl.BlockSpec(memory_space=pltpu.SMEM)
     vmem = pl.BlockSpec(memory_space=pltpu.VMEM)
@@ -353,6 +367,9 @@
     at = lax.axis_index("tp")
 
     pair_at = jnp.reshape(pair, (1,)).astype(jnp.int32)
+    upper = (lax.axis_index("zq") >= 4).astype(jnp.int32)
+    upper_at = jnp.reshape(upper, (1,))
+    role_at = pair_at + upper_at - 2 * pair_at * upper_at
     core_at = jnp.reshape(core, (1,)).astype(jnp.int32)
     shard_at = jnp.reshape(at, (1,)).astype(jnp.int32)
     zero = jnp.zeros((1,), jnp.int32)
@@ -370,7 +387,7 @@
         name="prep",
         compiler_params=pltpu.CompilerParams(vmem_limit_bytes=4 * 2**20),
     )(
-        pair_at,
+        role_at,
         tokens.reshape(8, NP, 2, 16, 128),
         gain_first.reshape(1, 128),
         gain_mix.reshape(1, 128),
@@ -452,8 +469,10 @@
         pair_at, came, after_mix
     )
     came = exchange(outgoing, ("zp", "c", "tp"))
-    came = came.reshape(NP, 2, 8, 16, 128).transpose(2, 0, 1, 3, 4)
-    return (came.reshape(-1, 128), memory_new, normalizer_new, stabilizer_new)
+    out = call(unpack_kernel, jax.ShapeDtypeStruct((8, NP, 2, 16, 128), BF), 1)(
+        upper_at, came.reshape(NP, 2, 8, 16, 128)
+    )
+    return (out.reshape(-1, 128), memory_new, normalizer_new, stabilizer_new)
 
 
 def solution(mesh):

time: 265 us -> 257 us (0.970)
  blocking collectives: 143 us -> 133 us
  starting transfers between devices: 56.5 us -> 62.7 us
  waiting for transfers between devices: 40.8 us -> 36.7 us
    all_to_all x5 -> x1, blocking collectives: 108 us -> 14 us  [exchange(): return lax.all_to_all(parts, axis, split_axis=0, concat_axis=0, tiled=True)]
    all_to_all x0 -> x4, blocking collectives: none -> 85 us  [exchange(): lax.all_to_all(parts, ('zq', 'zp'), split_axis=0, concat_axis=0, axis_ind...]
    all_to_all x0 -> x2, starting transfers between devices: none -> 14.3 us  [exchange(): lax.all_to_all(parts, ('zq', 'zp'), split_axis=0, concat_axis=0, axis_ind...]
    all_to_all x7 -> x5, starting transfers between devices: 45.8 us -> 35.9 us  [exchange(): return lax.all_to_all(parts, axis, split_axis=0, concat_axis=0, tiled=True)]
    all_to_all x7 -> x5, waiting for transfers between devices: 29.4 us -> 20.3 us  [exchange(): return lax.all_to_all(parts, axis, split_axis=0, concat_axis=0, tiled=True)]
    all_to_all x0 -> x2, waiting for transfers between devices: none -> 6 us  [exchange(): lax.all_to_all(parts, ('zq', 'zp'), split_axis=0, concat_axis=0, axis_ind...]
    pallas_call x12 -> x13, Pallas kernels: 9.34 us -> 10 us  [run(): pl.pallas_call(kernel, in_specs=[smem] * scalars + [vmem] * (len(args) -...]
where the time goes in v3:
time: 257 us; the launch traced here: 256 us
  blocking collectives  133 us (52%)
  starting transfers between devices  62.7 us (24%)
  waiting for transfers between devices  36.7 us (14%)
  Pallas kernels  12.3 us (5%)
  local copies, waits for them, and re-layouts  6.31 us (2%)
    all_to_all x4, blocking collectives, exchange(): lax.all_to_all(parts, ('zq', 'zp'), split_axis=0, concat_axis=0, axis_ind...  85 us
    all_to_all x5, starting transfers between devices, exchange(): return lax.all_to_all(parts, axis, split_axis=0, concat_axis=0, tiled=True)  35.9 us
    all_gather x6, blocking collectives, both_cores(): return lax.all_gather(array, 'c')  34.4 us
    all_to_all x5, waiting for transfers between devices, exchange(): return lax.all_to_all(parts, axis, split_axis=0, concat_axis=0, tiled=True)  20.3 us
    all_to_all x2, starting transfers between devices, exchange(): lax.all_to_all(parts, ('zq', 'zp'), split_axis=0, concat_axis=0, axis_ind...  14.3 us
    all_to_all x1, blocking collectives, exchange(): return lax.all_to_all(parts, axis, split_axis=0, concat_axis=0, tiled=True)  14 us
    ppermute x3, starting transfers between devices, swap(): return lax.ppermute(array, 'zp', [(0, 1), (1, 0)])  12.6 us
    ppermute x3, waiting for transfers between devices, swap(): return lax.ppermute(array, 'zp', [(0, 1), (1, 0)])  10.4 us
  transfers between devices with their start and end apart: 10, of which 6 were waited for; matrix products, arithmetic and copies ran while one was open for 1% of the time, Pallas kernels for 2%

profile of v3, /device:TPU:1, one launch (start us, length us, event | category | flops | bytes accessed | tf_op | source)
XLA Modules:
  0.0 255.6 jit_solution(17165646718977836337)
XLA Ops:
  0.7 0.6 copy-done.25
  1.3 0.9 copy-done.3
  2.3 0.9 copy-done.4
  3.2 0.9 copy-done.7
  4.1 1.0 prep.1
  5.1 4.4 %collective-permute-start = (bf16[1680,128]{1,0:T(8,128)(2,1)S(1)}, bf16[1680,128]{1,0:T(8,128)(2,1)S(1)}, u32[]{:S(2)}, u32[]{:S(2)}) collective-permute-start(bf16[1680,128]{1,0:T(8,128)(2,1)S(1)} %get-tuple-element.20), channel_id=1, source_target_pairs={{0,32},{32,0},{1,33},{33,1},{2,34},{34,2},{3,35},{35,3},{4,36},{36... | collective-permute-start | bytes 1290248 | tf_op jit(solution)/shard_map/ppermute | solution.py:26
  9.5 6.4 %all-gather = bf16[3360,128]{1,0:T(8,128)(2,1)S(1)} all-gather(bf16[1680,128]{1,0:T(8,128)(2,1)S(1)} %get-tuple-element.19), channel_id=2, replica_groups=mesh['zq'=8,'zp'=2,'c'=2,'tp'=16] {'c'}, dimensions={0}, use_global_device_ids=true | all-gather | bytes 1290240 | tf_op jit(solution)/shard_map/all_gather | solution.py:30
  16.0 8.1 %all-gather.1 = bf16[3360,128]{1,0:T(8,128)(2,1)S(1)} all-gather(bf16[1680,128]{1,0:T(8,128)(2,1)S(1)} %collective-permute-done), channel_id=3, replica_groups=mesh['zq'=8,'zp'=2,'c'=2,'tp'=16] {'c'}, dimensions={0}, use_global_device_ids=true | all-gather | bytes 1290240 | tf_op jit(solution)/shard_map/all_gather | solution.py:30
  24.1 0.6 shard_map.228
  24.7 33.2 %all_to_all.60.x_ref = bf16[8,16,1408]{2,1,0:T(8,128)(2,1)S(1)} all-to-all(bf16[8,16,1408]{2,1,0:T(8,128)(2,1)S(1)} %bitcast.57), channel_id=1, replica_groups={{0,64,128,192,288,352,416,480},{32,96,160,224,256,320,384,448},{1,65,12..., dimensions={0} | all-to-all | bytes 720896 | tf_op jit(solution)/shard_map/all_to_all | solution.py:36
  57.9 0.9 shard_map.229
  58.7 4.9 %all-to-all-start.1 = ((bf16[8,16,688]{2,1,0:T(8,128)(2,1)}), bf16[8,16,688]{2,1,0:T(8,128)(2,1)S(1)}, u32[]{:S(2)}, u32[]{:S(2)}) async-start(bf16[8,16,688]{2,1,0:T(8,128)(2,1)} %shard_map.229), calls=%async_computation.1 | async-start | bytes 393216 | tf_op jit(solution)/shard_map/all_to_all | solution.py:36
  64.3 5.1 %collective-permute-start.1 = (bf16[1424,128]{1,0:T(8,128)(2,1)S(1)}, bf16[1424,128]{1,0:T(8,128)(2,1)S(1)}, u32[]{:S(2)}, u32[]{:S(2)}) collective-permute-start(bf16[1424,128]{1,0:T(8,128)(2,1)S(1)} %shard_map.230), channel_id=1, source_target_pairs={{0,32},{32,0},{1,33},{33,1},{2,34},{34,2},{3,35},{35,3},{4,36},{36... | collective-permute-start | bytes 1093640 | tf_op jit(solution)/shard_map/ppermute | solution.py:26
  69.4 3.4 %all-gather.2 = bf16[2848,128]{1,0:T(8,128)(2,1)S(1)} all-gather(bf16[1424,128]{1,0:T(8,128)(2,1)S(1)} %shard_map.230), channel_id=4, replica_groups=mesh['zq'=8,'zp'=2,'c'=2,'tp'=16] {'c'}, dimensions={0}, use_global_device_ids=true | all-gather | bytes 1093632 | tf_op jit(solution)/shard_map/all_gather | solution.py:30
  72.9 10.4 %collective-permute-done.1 = bf16[1424,128]{1,0:T(8,128)(2,1)S(1)} collective-permute-done((bf16[1424,128]{1,0:T(8,128)(2,1)S(1)}, bf16[1424,128]{1,0:T(8,128)(2,1)S(1)}, u32[]{:S(2)}, u32[]{:S(2)}) %collective-permute-start.1) | collective-permute-done | bytes 364576 | tf_op jit(solution)/shard_map/ppermute | solution.py:26
  83.3 2.8 %all-gather.3 = bf16[2848,128]{1,0:T(8,128)(2,1)S(1)} all-gather(bf16[1424,128]{1,0:T(8,128)(2,1)S(1)} %collective-permute-done.1), channel_id=5, replica_groups=mesh['zq'=8,'zp'=2,'c'=2,'tp'=16] {'c'}, dimensions={0}, use_global_device_ids=true | all-gather | bytes 1093632 | tf_op jit(solution)/shard_map/all_gather | solution.py:30
  86.1 0.9 shard_map.231
  87.0 6.8 %all-to-all-start.2 = ((bf16[16,8,512]{2,1,0:T(8,128)(2,1)}), bf16[16,8,512]{2,1,0:T(8,128)(2,1)S(1)}, u32[]{:S(2)}, u32[]{:S(2)}) async-start(bf16[16,8,512]{2,1,0:T(8,128)(2,1)} %bitcast.17), calls=%async_computation.2 | async-start | bytes 262144 | tf_op jit(solution)/shard_map/all_to_all | solution.py:39
  93.8 6.8 %all-to-all-done.2.sum_ref = bf16[16,8,512]{2,1,0:T(8,128)(2,1)S(1)} async-done(((bf16[16,8,512]{2,1,0:T(8,128)(2,1)}), bf16[16,8,512]{2,1,0:T(8,128)(2,1)S(1)}, u32[]{:S(2)}, u32[]{:S(2)}) %all-to-all-start.2) | async-done | bytes 131104 | tf_op jit(solution)/shard_map/all_to_all | solution.py:39
  100.6 0.7 shard_map.232
  101.3 0.6 copy-done.18
  101.9 3.5 %all-to-all-start.3 = ((bf16[16,8,512]{2,1,0:T(8,128)(2,1)}), bf16[16,8,512]{2,1,0:T(8,128)(2,1)S(1)}, u32[]{:S(2)}, u32[]{:S(2)}) async-start(bf16[16,8,512]{2,1,0:T(8,128)(2,1)} %get-tuple-element.23), calls=%async_computation.3 | async-start | bytes 262144 | tf_op jit(solution)/shard_map/all_to_all | solution.py:39
  105.4 6.8 %all-to-all-done.3.x_ref = bf16[16,8,512]{2,1,0:T(8,128)(2,1)S(1)} async-done(((bf16[16,8,512]{2,1,0:T(8,128)(2,1)}), bf16[16,8,512]{2,1,0:T(8,128)(2,1)S(1)}, u32[]{:S(2)}, u32[]{:S(2)}) %all-to-all-start.3) | async-done | bytes 131104 | tf_op jit(solution)/shard_map/all_to_all | solution.py:39
  112.2 0.9 shard_map.233
  113.2 9.4 %all-to-all-start.4 = ((bf16[8,16,640]{2,1,0:T(8,128)(2,1)}), bf16[8,16,640]{2,1,0:T(8,128)(2,1)S(1)}, u32[]{:S(2)}, u32[]{:S(2)}) async-start(bf16[8,16,640]{2,1,0:T(8,128)(2,1)} %bitcast.19), calls=%async_computation.4 | async-start | bytes 327680 | tf_op jit(solution)/shard_map/all_to_all | solution.py:36
  122.6 0.9 copy-done.6
  123.5 0.7 shard_map.237
  124.2 3.1 %collective-permute-start.2 = (bf16[2032,128]{1,0:T(8,128)(2,1)S(1)}, bf16[2032,128]{1,0:T(8,128)(2,1)}, u32[]{:S(2)}, u32[]{:S(2)}) collective-permute-start(bf16[2032,128]{1,0:T(8,128)(2,1)S(1)} %shard_map.237), channel_id=1, source_target_pairs={{0,32},{32,0},{1,33},{33,1},{2,34},{34,2},{3,35},{35,3},{4,36},{36... | collective-permute-start | bytes 1560584 | tf_op jit(solution)/shard_map/ppermute | solution.py:26
  128.0 6.0 %all-to-all-done.4.x_ref = bf16[8,16,640]{2,1,0:T(8,128)(2,1)S(1)} async-done(((bf16[8,16,640]{2,1,0:T(8,128)(2,1)}), bf16[8,16,640]{2,1,0:T(8,128)(2,1)S(1)}, u32[]{:S(2)}, u32[]{:S(2)}) %all-to-all-start.4) | async-done | bytes 163872 | tf_op jit(solution)/shard_map/all_to_all | solution.py:36
  134.0 0.6 copy-done.24
  134.6 1.2 shard_map.234
  135.8 15.3 %all_to_all.61.x_ref = bf16[8,16,128]{2,1,0:T(8,128)(2,1)S(1)} all-to-all(bf16[8,16,128]{2,1,0:T(8,128)(2,1)S(1)} %get-tuple-element.25), channel_id=1, replica_groups={{0,64,128,192,288,352,416,480},{32,96,160,224,256,320,384,448},{1,65,12..., dimensions={0} | all-to-all | bytes 65536 | tf_op jit(solution)/shard_map/all_to_all | solution.py:36
  151.1 0.8 shard_map.235
  151.9 3.5 %all-to-all-start.6 = ((bf16[16,8,512]{2,1,0:T(8,128)(2,1)}), bf16[16,8,512]{2,1,0:T(8,128)(2,1)S(1)}, u32[]{:S(2)}, u32[]{:S(2)}) async-start(bf16[16,8,512]{2,1,0:T(8,128)(2,1)} %bitcast.23), calls=%async_computation.6 | async-start | bytes 262144 | tf_op jit(solution)/shard_map/all_to_all | solution.py:39
  155.5 8.2 %all-gather.4 = bf16[4064,128]{1,0:T(8,128)(2,1)S(1)} all-gather(bf16[2032,128]{1,0:T(8,128)(2,1)S(1)} %shard_map.237), channel_id=6, replica_groups=mesh['zq'=8,'zp'=2,'c'=2,'tp'=16] {'c'}, dimensions={0}, use_global_device_ids=true | all-gather | bytes 1560576 | tf_op jit(solution)/shard_map/all_gather | solution.py:30
  163.7 0.7 shard_map.236
  164.4 6.9 %all-to-all-start.7 = ((bf16[16,8,512]{2,1,0:T(8,128)(2,1)}), bf16[16,8,512]{2,1,0:T(8,128)(2,1)}, u32[]{:S(2)}, u32[]{:S(2)}) async-start(bf16[16,8,512]{2,1,0:T(8,128)(2,1)} %get-tuple-element.27), calls=%async_computation.7 | async-start | bytes 262144 | tf_op jit(solution)/shard_map/all_to_all | solution.py:39
  171.3 5.4 %all-gather.5 = bf16[4064,128]{1,0:T(8,128)(2,1)S(1)} all-gather(bf16[2032,128]{1,0:T(8,128)(2,1)} %collective-permute-done.2), channel_id=7, replica_groups=mesh['zq'=8,'zp'=2,'c'=2,'tp'=16] {'c'}, dimensions={0}, use_global_device_ids=true | all-gather | bytes 1560576 | tf_op jit(solution)/shard_map/all_gather | solution.py:30
  176.7 1.5 all-to-all-done.7.x_ref
  178.2 1.5 shard_map.238
  179.7 17.1 %all_to_all.62.x_ref = bf16[8,16,1408]{2,1,0:T(8,128)(2,1)S(1)} all-to-all(bf16[8,16,1408]{2,1,0:T(8,128)(2,1)S(1)} %bitcast.54), channel_id=1, replica_groups={{0,64,128,192,288,352,416,480},{32,96,160,224,256,320,384,448},{1,65,12..., dimensions={0} | all-to-all | bytes 720896 | tf_op jit(solution)/shard_map/all_to_all | solution.py:36
  197.0 19.5 %all_to_all.63.x_ref = bf16[8,16,688]{2,1,0:T(8,128)(2,1)S(1)} all-to-all(bf16[8,16,688]{2,1,0:T(8,128)(2,1)S(1)} %shard_map.239), channel_id=1, replica_groups={{0,64,128,192,288,352,416,480},{32,96,160,224,256,320,384,448},{1,65,12..., dimensions={0} | all-to-all | bytes 352256 | tf_op jit(solution)/shard_map/all_to_all | solution.py:36
  216.8 14.0 %all_to_all.64.sum_ref = bf16[16,8,512]{2,1,0:T(8,128)(2,1)S(1)} all-to-all(bf16[16,8,512]{2,1,0:T(8,128)(2,1)S(1)} %bitcast.56), channel_id=1, replica_groups=mesh['zq'=8,'zp'=2,'c'=2,'tp'=16] {'tp'}, dimensions={0} | all-to-all | bytes 262144 | tf_op jit(solution)/shard_map/all_to_all | solution.py:39
  230.8 0.7 shard_map.241
  231.4 15.1 %all-to-all-start.11 = ((bf16[64,8,128]{2,1,0:T(8,128)(2,1)}), bf16[64,8,128]{2,1,0:T(8,128)(2,1)S(1)}, u32[]{:S(2)}, u32[]{:S(2)}) async-start(bf16[64,8,128]{2,1,0:T(8,128)(2,1)} %shard_map.241), calls=%async_computation.11 | async-start | bytes 262144 | tf_op jit(solution)/shard_map/all_to_all | solution.py:39
  247.3 2.5 multiply_add_fusion
  249.8 5.1 %all-to-all-done.11 = bf16[64,8,128]{2,1,0:T(8,128)(2,1)S(1)} async-done(((bf16[64,8,128]{2,1,0:T(8,128)(2,1)}), bf16[64,8,128]{2,1,0:T(8,128)(2,1)S(1)}, u32[]{:S(2)}, u32[]{:S(2)}) %all-to-all-start.11) | async-done | bytes 131104 | tf_op jit(solution)/shard_map/all_to_all | solution.py:39
  255.0 0.7 shard_map.242
  (58 shorter events, 1.8 us)
Async XLA Ops:
  0.6 0.7 copy-start.25
  0.7 0.7 copy-start.26
  0.7 0.7 copy-start.27
  1.3 0.9 copy-start.3
  2.3 0.9 copy-start.4
  3.2 0.9 copy-start.7
  5.1 10.8 %collective-permute-start = (bf16[1680,128]{1,0:T(8,128)(2,1)S(1)}, bf16[1680,128]{1,0:T(8,128)(2,1)S(1)}, u32[]{:S(2)}, u32[]{:S(2)}) collective-permute-start(bf16[1680,128]{1,0:T(8,128)(2,1)S(1)} %get-tuple-element.20), channel_id=1, source_target_pairs={{0,32},{32,0},{1,33},{33,1},{2,34},{34,2},{3,35},{35,3},{4,36},{36... | collective-permute-start | bytes 1290248 | tf_op jit(solution)/shard_map/ppermute | solution.py:26
  57.8 5.8 %copy-start.9 = (bf16[128,128]{1,0:T(8,128)(2,1)S(1)}, bf16[128,128]{1,0:T(8,128)(2,1)}, u32[]{:S(2)}) copy-start(bf16[128,128]{1,0:T(8,128)(2,1)} %refs_1_.1) | copy-start | bytes 98308
  57.8 5.8 %copy-start.10 = (bf16[128,128]{1,0:T(8,128)(2,1)S(1)}, bf16[128,128]{1,0:T(8,128)(2,1)}, u32[]{:S(2)}) copy-start(bf16[128,128]{1,0:T(8,128)(2,1)} %refs_2_.2) | copy-start | bytes 98308
  57.9 5.8 %copy-start.11 = (bf16[128,128]{1,0:T(8,128)(2,1)S(1)}, bf16[128,128]{1,0:T(8,128)(2,1)}, u32[]{:S(2)}) copy-start(bf16[128,128]{1,0:T(8,128)(2,1)} %refs_3_.1) | copy-start | bytes 98308
  57.9 5.8 %copy-start.12 = (bf16[128,128]{1,0:T(8,128)(2,1)S(1)}, bf16[128,128]{1,0:T(8,128)(2,1)}, u32[]{:S(2)}) copy-start(bf16[128,128]{1,0:T(8,128)(2,1)} %refs_6_.1) | copy-start | bytes 98308
  58.7 5.0 %copy-start.1 = (bf16[688,128]{1,0:T(8,128)(2,1)S(1)}, bf16[688,128]{1,0:T(8,128)(2,1)}, u32[]{:S(2)}) copy-start(bf16[688,128]{1,0:T(8,128)(2,1)} %refs_2_.3) | copy-start | bytes 528388
  58.7 5.0 %copy-start.2 = (bf16[688,128]{1,0:T(8,128)(2,1)S(1)}, bf16[688,128]{1,0:T(8,128)(2,1)}, u32[]{:S(2)}) copy-start(bf16[688,128]{1,0:T(8,128)(2,1)} %refs_8_.1) | copy-start | bytes 528388
  58.7 5.0 %copy-start.8 = (bf16[128,128]{1,0:T(8,128)(2,1)S(1)}, bf16[128,128]{1,0:T(8,128)(2,1)}, u32[]{:S(2)}) copy-start(bf16[128,128]{1,0:T(8,128)(2,1)} %refs_0_.1) | copy-start | bytes 98308
  58.7 5.0 %copy-start.22 = (bf16[128,16]{0,1:T(8,128)(2,1)S(1)}, bf16[128,16]{0,1:T(8,128)(2,1)}, u32[]{:S(2)}) copy-start(bf16[128,16]{0,1:T(8,128)(2,1)} %param.31) | copy-start | bytes 12292
  58.7 5.0 %copy-start.23 = (bf16[128,16]{0,1:T(8,128)(2,1)S(1)}, bf16[128,16]{0,1:T(8,128)(2,1)}, u32[]{:S(2)}) copy-start(bf16[128,16]{0,1:T(8,128)(2,1)} %param.32) | copy-start | bytes 12292
  58.7 27.3 %all-to-all-start.1 = ((bf16[8,16,688]{2,1,0:T(8,128)(2,1)}), bf16[8,16,688]{2,1,0:T(8,128)(2,1)S(1)}, u32[]{:S(2)}, u32[]{:S(2)}) async-start(bf16[8,16,688]{2,1,0:T(8,128)(2,1)} %shard_map.229), calls=%async_computation.1 | async-start | bytes 393216 | tf_op jit(solution)/shard_map/all_to_all | solution.py:36
  64.3 19.0 %collective-permute-start.1 = (bf16[1424,128]{1,0:T(8,128)(2,1)S(1)}, bf16[1424,128]{1,0:T(8,128)(2,1)S(1)}, u32[]{:S(2)}, u32[]{:S(2)}) collective-permute-start(bf16[1424,128]{1,0:T(8,128)(2,1)S(1)} %shard_map.230), channel_id=1, source_target_pairs={{0,32},{32,0},{1,33},{33,1},{2,34},{34,2},{3,35},{35,3},{4,36},{36... | collective-permute-start | bytes 1093640 | tf_op jit(solution)/shard_map/ppermute | solution.py:26
  87.0 13.6 %all-to-all-start.2 = ((bf16[16,8,512]{2,1,0:T(8,128)(2,1)}), bf16[16,8,512]{2,1,0:T(8,128)(2,1)S(1)}, u32[]{:S(2)}, u32[]{:S(2)}) async-start(bf16[16,8,512]{2,1,0:T(8,128)(2,1)} %bitcast.17), calls=%async_computation.2 | async-start | bytes 262144 | tf_op jit(solution)/shard_map/all_to_all | solution.py:39
  101.3 0.6 copy-start.18
  101.9 10.3 %all-to-all-start.3 = ((bf16[16,8,512]{2,1,0:T(8,128)(2,1)}), bf16[16,8,512]{2,1,0:T(8,128)(2,1)S(1)}, u32[]{:S(2)}, u32[]{:S(2)}) async-start(bf16[16,8,512]{2,1,0:T(8,128)(2,1)} %get-tuple-element.23), calls=%async_computation.3 | async-start | bytes 262144 | tf_op jit(solution)/shard_map/all_to_all | solution.py:39
  112.2 10.3 %copy-start.5 = (bf16[128,688]{0,1:T(8,128)(2,1)S(1)}, bf16[128,688]{0,1:T(8,128)(2,1)}, u32[]{:S(2)}) copy-start(bf16[128,688]{0,1:T(8,128)(2,1)} %param.39) | copy-start | bytes 528388
  113.2 20.8 %copy-start = (f32[16,1,128,128]{3,2,1,0:T(8,128)S(1)}, f32[16,1,128,128]{3,2,1,0:T(8,128)}, u32[]{:S(2)}) copy-start(f32[16,1,128,128]{3,2,1,0:T(8,128)} %param.34) | copy-start | bytes 3145732
  113.2 20.8 %all-to-all-start.4 = ((bf16[8,16,640]{2,1,0:T(8,128)(2,1)}), bf16[8,16,640]{2,1,0:T(8,128)(2,1)S(1)}, u32[]{:S(2)}, u32[]{:S(2)}) async-start(bf16[8,16,640]{2,1,0:T(8,128)(2,1)} %bitcast.19), calls=%async_computation.4 | async-start | bytes 327680 | tf_op jit(solution)/shard_map/all_to_all | solution.py:36
  122.6 0.9 copy-start.6
  123.5 10.5 %copy-start.13 = (f32[16,1,128]{2,1,0:T(1,128)S(1)}, f32[16,1,128]{2,1,0:T(1,128)}, u32[]{:S(2)}) copy-start(f32[16,1,128]{2,1,0:T(1,128)} %param.35) | copy-start | bytes 24580
  124.2 47.1 %collective-permute-start.2 = (bf16[2032,128]{1,0:T(8,128)(2,1)S(1)}, bf16[2032,128]{1,0:T(8,128)(2,1)}, u32[]{:S(2)}, u32[]{:S(2)}) collective-permute-start(bf16[2032,128]{1,0:T(8,128)(2,1)S(1)} %shard_map.237), channel_id=1, source_target_pairs={{0,32},{32,0},{1,33},{33,1},{2,34},{34,2},{3,35},{35,3},{4,36},{36... | collective-permute-start | bytes 1560584 | tf_op jit(solution)/shard_map/ppermute | solution.py:26
  134.0 0.7 copy-start.24
  135.8 15.3 %copy-start.14 = (f32[16,128]{1,0:T(8,128)}, f32[16,128]{1,0:T(8,128)S(1)}, u32[]{:S(2)}) copy-start(f32[16,128]{1,0:T(8,128)S(1)} %get-tuple-element.30) | copy-start | bytes 24580
  135.8 15.3 %copy-start.16 = (f32[16,128]{1,0:T(8,128)}, f32[16,128]{1,0:T(8,128)S(1)}, u32[]{:S(2)}) copy-start(f32[16,128]{1,0:T(8,128)S(1)} %get-tuple-element.31) | copy-start | bytes 24580
  135.8 15.3 %copy-start.20 = (f32[16,128]{1,0:T(8,128)}, f32[16,128]{1,0:T(8,128)S(1)}, u32[]{:S(2)}) copy-start(f32[16,128]{1,0:T(8,128)S(1)} %get-tuple-element.29) | copy-start | bytes 24580
  151.9 11.8 %all-to-all-start.6 = ((bf16[16,8,512]{2,1,0:T(8,128)(2,1)}), bf16[16,8,512]{2,1,0:T(8,128)(2,1)S(1)}, u32[]{:S(2)}, u32[]{:S(2)}) async-start(bf16[16,8,512]{2,1,0:T(8,128)(2,1)} %bitcast.23), calls=%async_computation.6 | async-start | bytes 262144 | tf_op jit(solution)/shard_map/all_to_all | solution.py:39
  155.5 8.3 %copy-start.19 = (bf16[1,8,512]{2,1,0:T(8,128)(2,1)S(1)}, bf16[1,8,512]{2,1,0:T(8,128)(2,1)}, u32[]{:S(2)}) copy-start(bf16[1,8,512]{2,1,0:T(8,128)(2,1)} %copy-done.18) | copy-start | bytes 24580
  164.4 13.8 %all-to-all-start.7 = ((bf16[16,8,512]{2,1,0:T(8,128)(2,1)}), bf16[16,8,512]{2,1,0:T(8,128)(2,1)}, u32[]{:S(2)}, u32[]{:S(2)}) async-start(bf16[16,8,512]{2,1,0:T(8,128)(2,1)} %get-tuple-element.27), calls=%async_computation.7 | async-start | bytes 262144 | tf_op jit(solution)/shard_map/all_to_all | solution.py:39
  231.4 15.2 %copy-start.21 = (f32[16,128]{1,0:T(8,128)S(1)}, f32[16,128]{1,0:T(8,128)}, u32[]{:S(2)}) copy-start(f32[16,128]{1,0:T(8,128)} %copy-done.20) | copy-start | bytes 24580
  231.4 15.3 %copy-start.17 = (f32[16,128]{1,0:T(8,128)S(1)}, f32[16,128]{1,0:T(8,128)}, u32[]{:S(2)}) copy-start(f32[16,128]{1,0:T(8,128)} %copy-done.16) | copy-start | bytes 24580
  231.4 23.5 %all-to-all-start.11 = ((bf16[64,8,128]{2,1,0:T(8,128)(2,1)}), bf16[64,8,128]{2,1,0:T(8,128)(2,1)S(1)}, u32[]{:S(2)}, u32[]{:S(2)}) async-start(bf16[64,8,128]{2,1,0:T(8,128)(2,1)} %shard_map.241), calls=%async_computation.11 | async-start | bytes 262144 | tf_op jit(solution)/shard_map/all_to_all | solution.py:39
  246.6 0.7 copy-start.15

commit v4 on v3

--- a/solution.py
+++ b/solution.py
@@ -58,11 +58,11 @@
     ]
 
 
-def scaled_rows(x_ref, gain_ref):
+def scaled_rows(x_ref, gain):
     groups, rows, width = x_ref.shape
     x = x_ref[...].astype(F32).reshape(groups * rows, width)
     squares = jnp.sum(x * x, axis=1, keepdims=True)
-    return (x * gain_ref[...]).astype(BF), squares
+    return (x * gain).astype(BF), squares
 
 
 def put_squares(block, squares, at):
@@ -77,7 +77,7 @@
 
 
 def wide_kernel(x_ref, gain_ref, own_ref, other_ref, out_ref):
-    scaled, squares = scaled_rows(x_ref, gain_ref)
+    scaled, squares = scaled_rows(x_ref, gain_ref[2])
     total = None
     for core in range(2):
         weight = jnp.concatenate([own_ref[core, :WIDE], other_ref[core, :WIDE]], axis=1)
@@ -172,7 +172,7 @@
 
 
 def mix_kernel(x_ref, gain_ref, own_ref, other_ref, out_ref):
-    scaled, squares = scaled_rows(x_ref, gain_ref)
+    scaled, squares = scaled_rows(x_ref, gain_ref[1])
     for pair in range(2):
         total = None
         for core in range(2):
@@ -428,7 +428,7 @@
     copies = exchange(copies, "tp")
 
     mixed = call(mix_kernel, jax.ShapeDtypeStruct((128, MIX), BF))(
-        copies, gains[1], middle_own, middle_other
+        copies, gains, middle_own, middle_other
     )
     summed = exchange(mixed.reshape(8, 16, MIX), "zq")
     small = jax.ShapeDtypeStruct((16, 128), F32)
@@ -457,7 +457,7 @@
     after_mix, copies = call(residual_kernel(1.0), (shard, copied), 1)(zero, came, after_first)
     copies = exchange(copies, "tp")
 
-    wide = call(wide_kernel, wide_shape)(copies, gains[2], last_own, last_other)
+    wide = call(wide_kernel, wide_shape)(copies, gains, last_own, last_other)
     came = half_step(
         wide,
         (

time: 257 us -> 257 us (level)
  blocking collectives: 133 us -> 143 us
  waiting for transfers between devices: 36.7 us -> 29.9 us
  starting transfers between devices: 62.7 us -> 59.2 us
    all_to_all x1 -> x2, blocking collectives: 14 us -> 24 us  [exchange(): return lax.all_to_all(parts, axis, split_axis=0, concat_axis=0, tiled=True)]
    all_to_all x5 -> x4, waiting for transfers between devices: 20.3 us -> 13.5 us  [exchange(): return lax.all_to_all(parts, axis, split_axis=0, concat_axis=0, tiled=True)]
    all_to_all x5 -> x4, starting transfers between devices: 35.9 us -> 32.3 us  [exchange(): return lax.all_to_all(parts, axis, split_axis=0, concat_axis=0, tiled=True)]
    unnamed x56 -> x60, local copies, waits for them, and re-layouts: 6.19 us -> 6.91 us
  transfers between devices with their start and end apart: 10 -> 9, of which waited for: 6 -> 5; matrix products, arithmetic and copies ran while one was open for 1% -> 1% of each run, Pallas kernels for 2% -> 2%
where the time goes in v4:
time: 257 us; the launch traced here: 255 us
  blocking collectives  143 us (56%)
  starting transfers between devices  59.2 us (23%)
  waiting for transfers between devices  29.9 us (12%)
  Pallas kernels  11.7 us (5%)
  local copies, waits for them, and re-layouts  7.02 us (3%)
    all_to_all x4, blocking collectives, exchange(): lax.all_to_all(parts, ('zq', 'zp'), split_axis=0, concat_axis=0, axis_ind...  84.9 us
    all_gather x6, blocking collectives, both_cores(): return lax.all_gather(array, 'c')  34.5 us
    all_to_all x4, starting transfers between devices, exchange(): return lax.all_to_all(parts, axis, split_axis=0, concat_axis=0, tiled=True)  32.3 us
    all_to_all x2, blocking collectives, exchange(): return lax.all_to_all(parts, axis, split_axis=0, concat_axis=0, tiled=True)  24 us
    all_to_all x2, starting transfers between devices, exchange(): lax.all_to_all(parts, ('zq', 'zp'), split_axis=0, concat_axis=0, axis_ind...  14.3 us
    all_to_all x4, waiting for transfers between devices, exchange(): return lax.all_to_all(parts, axis, split_axis=0, concat_axis=0, tiled=True)  13.5 us
    ppermute x3, starting transfers between devices, swap(): return lax.ppermute(array, 'zp', [(0, 1), (1, 0)])  12.6 us
    ppermute x3, waiting for transfers between devices, swap(): return lax.ppermute(array, 'zp', [(0, 1), (1, 0)])  10.4 us
  transfers between devices with their start and end apart: 9, of which 5 were waited for; matrix products, arithmetic and copies ran while one was open for 1% of the time, Pallas kernels for 2%

profile of v4, /device:TPU:1, one launch (start us, length us, event | category | flops | bytes accessed | tf_op | source)
XLA Modules:
  0.0 255.3 jit_solution(7058246777890902894)
XLA Ops:
  0.7 0.6 copy-done.27
  1.3 0.9 copy-done.3
  2.3 0.9 copy-done.4
  3.2 0.9 copy-done.7
  4.1 1.0 prep.1
  5.1 4.4 %collective-permute-start = (bf16[1680,128]{1,0:T(8,128)(2,1)S(1)}, bf16[1680,128]{1,0:T(8,128)(2,1)S(1)}, u32[]{:S(2)}, u32[]{:S(2)}) collective-permute-start(bf16[1680,128]{1,0:T(8,128)(2,1)S(1)} %get-tuple-element.20), channel_id=1, source_target_pairs={{0,32},{32,0},{1,33},{33,1},{2,34},{34,2},{3,35},{35,3},{4,36},{36... | collective-permute-start | bytes 1290248 | tf_op jit(solution)/shard_map/ppermute | solution.py:26
  9.5 6.4 %all-gather = bf16[3360,128]{1,0:T(8,128)(2,1)S(1)} all-gather(bf16[1680,128]{1,0:T(8,128)(2,1)S(1)} %get-tuple-element.19), channel_id=2, replica_groups=mesh['zq'=8,'zp'=2,'c'=2,'tp'=16] {'c'}, dimensions={0}, use_global_device_ids=true | all-gather | bytes 1290240 | tf_op jit(solution)/shard_map/all_gather | solution.py:30
  16.0 8.1 %all-gather.1 = bf16[3360,128]{1,0:T(8,128)(2,1)S(1)} all-gather(bf16[1680,128]{1,0:T(8,128)(2,1)S(1)} %collective-permute-done), channel_id=3, replica_groups=mesh['zq'=8,'zp'=2,'c'=2,'tp'=16] {'c'}, dimensions={0}, use_global_device_ids=true | all-gather | bytes 1290240 | tf_op jit(solution)/shard_map/all_gather | solution.py:30
  24.1 0.6 shard_map.228
  24.7 33.2 %all_to_all.60.x_ref = bf16[8,16,1408]{2,1,0:T(8,128)(2,1)S(1)} all-to-all(bf16[8,16,1408]{2,1,0:T(8,128)(2,1)S(1)} %bitcast.53), channel_id=1, replica_groups={{0,64,128,192,288,352,416,480},{32,96,160,224,256,320,384,448},{1,65,12..., dimensions={0} | all-to-all | bytes 720896 | tf_op jit(solution)/shard_map/all_to_all | solution.py:36
  57.9 0.9 shard_map.229
  58.7 4.9 %all-to-all-start.1 = ((bf16[8,16,688]{2,1,0:T(8,128)(2,1)}), bf16[8,16,688]{2,1,0:T(8,128)(2,1)S(1)}, u32[]{:S(2)}, u32[]{:S(2)}) async-start(bf16[8,16,688]{2,1,0:T(8,128)(2,1)} %shard_map.229), calls=%async_computation.1 | async-start | bytes 393216 | tf_op jit(solution)/shard_map/all_to_all | solution.py:36
  63.7 0.6 shard_map.230
  64.3 5.1 %collective-permute-start.1 = (bf16[1424,128]{1,0:T(8,128)(2,1)S(1)}, bf16[1424,128]{1,0:T(8,128)(2,1)S(1)}, u32[]{:S(2)}, u32[]{:S(2)}) collective-permute-start(bf16[1424,128]{1,0:T(8,128)(2,1)S(1)} %shard_map.230), channel_id=1, source_target_pairs={{0,32},{32,0},{1,33},{33,1},{2,34},{34,2},{3,35},{35,3},{4,36},{36... | collective-permute-start | bytes 1093640 | tf_op jit(solution)/shard_map/ppermute | solution.py:26
  69.4 3.4 %all-gather.2 = bf16[2848,128]{1,0:T(8,128)(2,1)S(1)} all-gather(bf16[1424,128]{1,0:T(8,128)(2,1)S(1)} %shard_map.230), channel_id=4, replica_groups=mesh['zq'=8,'zp'=2,'c'=2,'tp'=16] {'c'}, dimensions={0}, use_global_device_ids=true | all-gather | bytes 1093632 | tf_op jit(solution)/shard_map/all_gather | solution.py:30
  72.9 10.4 %collective-permute-done.1 = bf16[1424,128]{1,0:T(8,128)(2,1)S(1)} collective-permute-done((bf16[1424,128]{1,0:T(8,128)(2,1)S(1)}, bf16[1424,128]{1,0:T(8,128)(2,1)S(1)}, u32[]{:S(2)}, u32[]{:S(2)}) %collective-permute-start.1) | collective-permute-done | bytes 364576 | tf_op jit(solution)/shard_map/ppermute | solution.py:26
  83.3 2.8 %all-gather.3 = bf16[2848,128]{1,0:T(8,128)(2,1)S(1)} all-gather(bf16[1424,128]{1,0:T(8,128)(2,1)S(1)} %collective-permute-done.1), channel_id=5, replica_groups=mesh['zq'=8,'zp'=2,'c'=2,'tp'=16] {'c'}, dimensions={0}, use_global_device_ids=true | all-gather | bytes 1093632 | tf_op jit(solution)/shard_map/all_gather | solution.py:30
  86.1 0.9 shard_map.231
  87.0 6.8 %all-to-all-start.2 = ((bf16[16,8,512]{2,1,0:T(8,128)(2,1)}), bf16[16,8,512]{2,1,0:T(8,128)(2,1)S(1)}, u32[]{:S(2)}, u32[]{:S(2)}) async-start(bf16[16,8,512]{2,1,0:T(8,128)(2,1)} %bitcast.17), calls=%async_computation.2 | async-start | bytes 262144 | tf_op jit(solution)/shard_map/all_to_all | solution.py:39
  93.8 6.8 %all-to-all-done.2.sum_ref = bf16[16,8,512]{2,1,0:T(8,128)(2,1)S(1)} async-done(((bf16[16,8,512]{2,1,0:T(8,128)(2,1)}), bf16[16,8,512]{2,1,0:T(8,128)(2,1)S(1)}, u32[]{:S(2)}, u32[]{:S(2)}) %all-to-all-start.2) | async-done | bytes 131104 | tf_op jit(solution)/shard_map/all_to_all | solution.py:39
  100.7 9.9 %all_to_all.61.x_ref = bf16[16,8,512]{2,1,0:T(8,128)(2,1)S(1)} all-to-all(bf16[16,8,512]{2,1,0:T(8,128)(2,1)S(1)} %get-tuple-element.23), channel_id=1, replica_groups=mesh['zq'=8,'zp'=2,'c'=2,'tp'=16] {'tp'}, dimensions={0} | all-to-all | bytes 262144 | tf_op jit(solution)/shard_map/all_to_all | solution.py:39
  110.6 0.9 shard_map.233
  111.5 9.4 %all-to-all-start.4 = ((bf16[8,16,640]{2,1,0:T(8,128)(2,1)}), bf16[8,16,640]{2,1,0:T(8,128)(2,1)S(1)}, u32[]{:S(2)}, u32[]{:S(2)}) async-start(bf16[8,16,640]{2,1,0:T(8,128)(2,1)} %bitcast.18), calls=%async_computation.4 | async-start | bytes 327680 | tf_op jit(solution)/shard_map/all_to_all | solution.py:36
  120.9 0.9 copy-done.6
  121.9 0.7 shard_map.237
  122.6 3.1 %collective-permute-start.2 = (bf16[2032,128]{1,0:T(8,128)(2,1)S(1)}, bf16[2032,128]{1,0:T(8,128)(2,1)}, u32[]{:S(2)}, u32[]{:S(2)}) collective-permute-start(bf16[2032,128]{1,0:T(8,128)(2,1)S(1)} %shard_map.237), channel_id=1, source_target_pairs={{0,32},{32,0},{1,33},{33,1},{2,34},{34,2},{3,35},{35,3},{4,36},{36... | collective-permute-start | bytes 1560584 | tf_op jit(solution)/shard_map/ppermute | solution.py:26
  126.3 6.0 %all-to-all-done.4.x_ref = bf16[8,16,640]{2,1,0:T(8,128)(2,1)S(1)} async-done(((bf16[8,16,640]{2,1,0:T(8,128)(2,1)}), bf16[8,16,640]{2,1,0:T(8,128)(2,1)S(1)}, u32[]{:S(2)}, u32[]{:S(2)}) %all-to-all-start.4) | async-done | bytes 163872 | tf_op jit(solution)/shard_map/all_to_all | solution.py:36
  132.3 0.7 copy-done.26
  133.0 0.7 copy-done.13
  133.7 1.2 shard_map.234
  134.9 15.2 %all_to_all.62.x_ref = bf16[8,16,128]{2,1,0:T(8,128)(2,1)S(1)} all-to-all(bf16[8,16,128]{2,1,0:T(8,128)(2,1)S(1)} %get-tuple-element.25), channel_id=1, replica_groups={{0,64,128,192,288,352,416,480},{32,96,160,224,256,320,384,448},{1,65,12..., dimensions={0} | all-to-all | bytes 65536 | tf_op jit(solution)/shard_map/all_to_all | solution.py:36
  150.1 0.8 shard_map.235
  150.9 3.5 %all-to-all-start.6 = ((bf16[16,8,512]{2,1,0:T(8,128)(2,1)}), bf16[16,8,512]{2,1,0:T(8,128)(2,1)S(1)}, u32[]{:S(2)}, u32[]{:S(2)}) async-start(bf16[16,8,512]{2,1,0:T(8,128)(2,1)} %bitcast.22), calls=%async_computation.6 | async-start | bytes 262144 | tf_op jit(solution)/shard_map/all_to_all | solution.py:39
  154.4 8.3 %all-gather.4 = bf16[4064,128]{1,0:T(8,128)(2,1)S(1)} all-gather(bf16[2032,128]{1,0:T(8,128)(2,1)S(1)} %shard_map.237), channel_id=6, replica_groups=mesh['zq'=8,'zp'=2,'c'=2,'tp'=16] {'c'}, dimensions={0}, use_global_device_ids=true | all-gather | bytes 1560576 | tf_op jit(solution)/shard_map/all_gather | solution.py:30
  162.8 0.7 shard_map.236
  163.5 0.6 copy-done.20
  164.1 6.9 %all-to-all-start.7 = ((bf16[16,8,512]{2,1,0:T(8,128)(2,1)}), bf16[16,8,512]{2,1,0:T(8,128)(2,1)}, u32[]{:S(2)}, u32[]{:S(2)}) async-start(bf16[16,8,512]{2,1,0:T(8,128)(2,1)} %get-tuple-element.27), calls=%async_computation.7 | async-start | bytes 262144 | tf_op jit(solution)/shard_map/all_to_all | solution.py:39
  171.0 5.4 %all-gather.5 = bf16[4064,128]{1,0:T(8,128)(2,1)S(1)} all-gather(bf16[2032,128]{1,0:T(8,128)(2,1)} %collective-permute-done.2), channel_id=7, replica_groups=mesh['zq'=8,'zp'=2,'c'=2,'tp'=16] {'c'}, dimensions={0}, use_global_device_ids=true | all-gather | bytes 1560576 | tf_op jit(solution)/shard_map/all_gather | solution.py:30
  176.4 1.5 all-to-all-done.7.x_ref
  177.9 1.5 shard_map.238
  179.4 17.1 %all_to_all.63.x_ref = bf16[8,16,1408]{2,1,0:T(8,128)(2,1)S(1)} all-to-all(bf16[8,16,1408]{2,1,0:T(8,128)(2,1)S(1)} %bitcast.50), channel_id=1, replica_groups={{0,64,128,192,288,352,416,480},{32,96,160,224,256,320,384,448},{1,65,12..., dimensions={0} | all-to-all | bytes 720896 | tf_op jit(solution)/shard_map/all_to_all | solution.py:36
  196.6 19.5 %all_to_all.64.x_ref = bf16[8,16,688]{2,1,0:T(8,128)(2,1)S(1)} all-to-all(bf16[8,16,688]{2,1,0:T(8,128)(2,1)S(1)} %shard_map.239), channel_id=1, replica_groups={{0,64,128,192,288,352,416,480},{32,96,160,224,256,320,384,448},{1,65,12..., dimensions={0} | all-to-all | bytes 352256 | tf_op jit(solution)/shard_map/all_to_all | solution.py:36
  216.4 14.1 %all_to_all.65.sum_ref = bf16[16,8,512]{2,1,0:T(8,128)(2,1)S(1)} all-to-all(bf16[16,8,512]{2,1,0:T(8,128)(2,1)S(1)} %bitcast.52), channel_id=1, replica_groups=mesh['zq'=8,'zp'=2,'c'=2,'tp'=16] {'tp'}, dimensions={0} | all-to-all | bytes 262144 | tf_op jit(solution)/shard_map/all_to_all | solution.py:39
  230.5 0.7 shard_map.241
  231.2 15.1 %all-to-all-start.11 = ((bf16[64,8,128]{2,1,0:T(8,128)(2,1)}), bf16[64,8,128]{2,1,0:T(8,128)(2,1)S(1)}, u32[]{:S(2)}, u32[]{:S(2)}) async-start(bf16[64,8,128]{2,1,0:T(8,128)(2,1)} %shard_map.241), calls=%async_computation.11 | async-start | bytes 262144 | tf_op jit(solution)/shard_map/all_to_all | solution.py:39
  247.0 2.5 multiply_add_fusion
  249.5 5.1 %all-to-all-done.11 = bf16[64,8,128]{2,1,0:T(8,128)(2,1)S(1)} async-done(((bf16[64,8,128]{2,1,0:T(8,128)(2,1)}), bf16[64,8,128]{2,1,0:T(8,128)(2,1)S(1)}, u32[]{:S(2)}, u32[]{:S(2)}) %all-to-all-start.11) | async-done | bytes 131104 | tf_op jit(solution)/shard_map/all_to_all | solution.py:39
  254.7 0.7 shard_map.242
  (60 shorter events, 1.3 us)
Async XLA Ops:
  0.6 0.7 copy-start.27
  0.7 0.7 copy-start.28
  0.7 0.7 copy-start.29
  1.3 0.9 copy-start.3
  2.3 0.9 copy-start.4
  3.2 0.9 copy-start.7
  5.1 10.8 %collective-permute-start = (bf16[1680,128]{1,0:T(8,128)(2,1)S(1)}, bf16[1680,128]{1,0:T(8,128)(2,1)S(1)}, u32[]{:S(2)}, u32[]{:S(2)}) collective-permute-start(bf16[1680,128]{1,0:T(8,128)(2,1)S(1)} %get-tuple-element.20), channel_id=1, source_target_pairs={{0,32},{32,0},{1,33},{33,1},{2,34},{34,2},{3,35},{35,3},{4,36},{36... | collective-permute-start | bytes 1290248 | tf_op jit(solution)/shard_map/ppermute | solution.py:26
  57.8 5.8 %copy-start.9 = (bf16[128,128]{1,0:T(8,128)(2,1)S(1)}, bf16[128,128]{1,0:T(8,128)(2,1)}, u32[]{:S(2)}) copy-start(bf16[128,128]{1,0:T(8,128)(2,1)} %refs_1_.1) | copy-start | bytes 98308
  57.8 5.8 %copy-start.10 = (bf16[128,128]{1,0:T(8,128)(2,1)S(1)}, bf16[128,128]{1,0:T(8,128)(2,1)}, u32[]{:S(2)}) copy-start(bf16[128,128]{1,0:T(8,128)(2,1)} %refs_2_.2) | copy-start | bytes 98308
  57.9 5.8 %copy-start.11 = (bf16[128,128]{1,0:T(8,128)(2,1)S(1)}, bf16[128,128]{1,0:T(8,128)(2,1)}, u32[]{:S(2)}) copy-start(bf16[128,128]{1,0:T(8,128)(2,1)} %refs_3_.1) | copy-start | bytes 98308
  57.9 5.8 %copy-start.12 = (bf16[128,128]{1,0:T(8,128)(2,1)S(1)}, bf16[128,128]{1,0:T(8,128)(2,1)}, u32[]{:S(2)}) copy-start(bf16[128,128]{1,0:T(8,128)(2,1)} %refs_6_.1) | copy-start | bytes 98308
  58.7 5.0 %copy-start.1 = (bf16[688,128]{1,0:T(8,128)(2,1)S(1)}, bf16[688,128]{1,0:T(8,128)(2,1)}, u32[]{:S(2)}) copy-start(bf16[688,128]{1,0:T(8,128)(2,1)} %refs_2_.3) | copy-start | bytes 528388
  58.7 5.0 %copy-start.2 = (bf16[688,128]{1,0:T(8,128)(2,1)S(1)}, bf16[688,128]{1,0:T(8,128)(2,1)}, u32[]{:S(2)}) copy-start(bf16[688,128]{1,0:T(8,128)(2,1)} %refs_8_.1) | copy-start | bytes 528388
  58.7 5.0 %copy-start.8 = (bf16[128,128]{1,0:T(8,128)(2,1)S(1)}, bf16[128,128]{1,0:T(8,128)(2,1)}, u32[]{:S(2)}) copy-start(bf16[128,128]{1,0:T(8,128)(2,1)} %refs_0_.1) | copy-start | bytes 98308
  58.7 5.0 %copy-start.24 = (bf16[128,16]{0,1:T(8,128)(2,1)S(1)}, bf16[128,16]{0,1:T(8,128)(2,1)}, u32[]{:S(2)}) copy-start(bf16[128,16]{0,1:T(8,128)(2,1)} %param.31) | copy-start | bytes 12292
  58.7 5.0 %copy-start.25 = (bf16[128,16]{0,1:T(8,128)(2,1)S(1)}, bf16[128,16]{0,1:T(8,128)(2,1)}, u32[]{:S(2)}) copy-start(bf16[128,16]{0,1:T(8,128)(2,1)} %param.32) | copy-start | bytes 12292
  58.7 27.3 %all-to-all-start.1 = ((bf16[8,16,688]{2,1,0:T(8,128)(2,1)}), bf16[8,16,688]{2,1,0:T(8,128)(2,1)S(1)}, u32[]{:S(2)}, u32[]{:S(2)}) async-start(bf16[8,16,688]{2,1,0:T(8,128)(2,1)} %shard_map.229), calls=%async_computation.1 | async-start | bytes 393216 | tf_op jit(solution)/shard_map/all_to_all | solution.py:36
  64.3 19.0 %collective-permute-start.1 = (bf16[1424,128]{1,0:T(8,128)(2,1)S(1)}, bf16[1424,128]{1,0:T(8,128)(2,1)S(1)}, u32[]{:S(2)}, u32[]{:S(2)}) collective-permute-start(bf16[1424,128]{1,0:T(8,128)(2,1)S(1)} %shard_map.230), channel_id=1, source_target_pairs={{0,32},{32,0},{1,33},{33,1},{2,34},{34,2},{3,35},{35,3},{4,36},{36... | collective-permute-start | bytes 1093640 | tf_op jit(solution)/shard_map/ppermute | solution.py:26
  87.0 13.6 %all-to-all-start.2 = ((bf16[16,8,512]{2,1,0:T(8,128)(2,1)}), bf16[16,8,512]{2,1,0:T(8,128)(2,1)S(1)}, u32[]{:S(2)}, u32[]{:S(2)}) async-start(bf16[16,8,512]{2,1,0:T(8,128)(2,1)} %bitcast.17), calls=%async_computation.2 | async-start | bytes 262144 | tf_op jit(solution)/shard_map/all_to_all | solution.py:39
  100.7 9.9 %copy-start.18 = (bf16[1,8,512]{2,1,0:T(8,128)(2,1)}, bf16[1,8,512]{2,1,0:T(8,128)(2,1)S(1)}, u32[]{:S(2)}) copy-start(bf16[1,8,512]{2,1,0:T(8,128)(2,1)S(1)} %get-tuple-element.26.old_ref) | copy-start | bytes 24580
  110.6 10.3 %copy-start.5 = (bf16[128,688]{0,1:T(8,128)(2,1)S(1)}, bf16[128,688]{0,1:T(8,128)(2,1)}, u32[]{:S(2)}) copy-start(bf16[128,688]{0,1:T(8,128)(2,1)} %param.39) | copy-start | bytes 528388
  111.5 20.8 %copy-start = (f32[16,1,128,128]{3,2,1,0:T(8,128)S(1)}, f32[16,1,128,128]{3,2,1,0:T(8,128)}, u32[]{:S(2)}) copy-start(f32[16,1,128,128]{3,2,1,0:T(8,128)} %param.34) | copy-start | bytes 3145732
  111.5 20.8 %all-to-all-start.4 = ((bf16[8,16,640]{2,1,0:T(8,128)(2,1)}), bf16[8,16,640]{2,1,0:T(8,128)(2,1)S(1)}, u32[]{:S(2)}, u32[]{:S(2)}) async-start(bf16[8,16,640]{2,1,0:T(8,128)(2,1)} %bitcast.18), calls=%async_computation.4 | async-start | bytes 327680 | tf_op jit(solution)/shard_map/all_to_all | solution.py:36
  120.9 0.9 copy-start.6
  122.6 48.4 %collective-permute-start.2 = (bf16[2032,128]{1,0:T(8,128)(2,1)S(1)}, bf16[2032,128]{1,0:T(8,128)(2,1)}, u32[]{:S(2)}, u32[]{:S(2)}) collective-permute-start(bf16[2032,128]{1,0:T(8,128)(2,1)S(1)} %shard_map.237), channel_id=1, source_target_pairs={{0,32},{32,0},{1,33},{33,1},{2,34},{34,2},{3,35},{35,3},{4,36},{36... | collective-permute-start | bytes 1560584 | tf_op jit(solution)/shard_map/ppermute | solution.py:26
  132.3 0.7 copy-start.26
  133.0 0.7 copy-start.13
  134.9 15.2 %copy-start.14 = (f32[16,128]{1,0:T(8,128)}, f32[16,128]{1,0:T(8,128)S(1)}, u32[]{:S(2)}) copy-start(f32[16,128]{1,0:T(8,128)S(1)} %get-tuple-element.30) | copy-start | bytes 24580
  134.9 15.2 %copy-start.16 = (f32[16,128]{1,0:T(8,128)}, f32[16,128]{1,0:T(8,128)S(1)}, u32[]{:S(2)}) copy-start(f32[16,128]{1,0:T(8,128)S(1)} %get-tuple-element.31) | copy-start | bytes 24580
  134.9 15.2 %copy-start.22 = (f32[16,128]{1,0:T(8,128)}, f32[16,128]{1,0:T(8,128)S(1)}, u32[]{:S(2)}) copy-start(f32[16,128]{1,0:T(8,128)S(1)} %get-tuple-element.29) | copy-start | bytes 24580
  150.9 11.9 %all-to-all-start.6 = ((bf16[16,8,512]{2,1,0:T(8,128)(2,1)}), bf16[16,8,512]{2,1,0:T(8,128)(2,1)S(1)}, u32[]{:S(2)}, u32[]{:S(2)}) async-start(bf16[16,8,512]{2,1,0:T(8,128)(2,1)} %bitcast.22), calls=%async_computation.6 | async-start | bytes 262144 | tf_op jit(solution)/shard_map/all_to_all | solution.py:39
  154.4 8.4 %copy-start.19 = (bf16[1,8,512]{2,1,0:T(8,128)(2,1)S(1)}, bf16[1,8,512]{2,1,0:T(8,128)(2,1)}, u32[]{:S(2)}) copy-start(bf16[1,8,512]{2,1,0:T(8,128)(2,1)} %copy-done.18) | copy-start | bytes 24580
  163.5 0.6 copy-start.20
  164.1 13.8 %all-to-all-start.7 = ((bf16[16,8,512]{2,1,0:T(8,128)(2,1)}), bf16[16,8,512]{2,1,0:T(8,128)(2,1)}, u32[]{:S(2)}, u32[]{:S(2)}) async-start(bf16[16,8,512]{2,1,0:T(8,128)(2,1)} %get-tuple-element.27), calls=%async_computation.7 | async-start | bytes 262144 | tf_op jit(solution)/shard_map/all_to_all | solution.py:39
  216.4 14.1 %copy-start.21 = (bf16[1,8,512]{2,1,0:T(8,128)(2,1)S(1)}, bf16[1,8,512]{2,1,0:T(8,128)(2,1)}, u32[]{:S(2)}) copy-start(bf16[1,8,512]{2,1,0:T(8,128)(2,1)} %copy-done.20) | copy-start | bytes 24580
  231.2 15.2 %copy-start.23 = (f32[16,128]{1,0:T(8,128)S(1)}, f32[16,128]{1,0:T(8,128)}, u32[]{:S(2)}) copy-start(f32[16,128]{1,0:T(8,128)} %copy-done.22) | copy-start | bytes 24580
  231.2 15.3 %copy-start.17 = (f32[16,128]{1,0:T(8,128)S(1)}, f32[16,128]{1,0:T(8,128)}, u32[]{:S(2)}) copy-start(f32[16,128]{1,0:T(8,128)} %copy-done.16) | copy-start | bytes 24580
  231.2 23.5 %all-to-all-start.11 = ((bf16[64,8,128]{2,1,0:T(8,128)(2,1)}), bf16[64,8,128]{2,1,0:T(8,128)(2,1)S(1)}, u32[]{:S(2)}, u32[]{:S(2)}) async-start(bf16[64,8,128]{2,1,0:T(8,128)(2,1)} %shard_map.241), calls=%async_computation.11 | async-start | bytes 262144 | tf_op jit(solution)/shard_map/all_to_all | solution.py:39
  246.3 0.7 copy-start.15

commit v5 on v4

--- a/solution.py
+++ b/solution.py
@@ -415,15 +415,17 @@
     last_came = swap(last)
 
     first_own, first_other = both_cores(kept), both_cores(came)
-    middle_own, middle_other = both_cores(middle), both_cores(middle_came)
-    last_own, last_other = both_cores(last), both_cores(last_came)
+    middle_own, middle_other = both_cores(middle[:736]), both_cores(middle_came[:736])
+    down_own, down_other = both_cores(down_first), both_cores(middle_came[736:])
+    last_own = both_cores(last)
+    last_other = both_cores(last_came)
 
     shard = jax.ShapeDtypeStruct((1, 8, 512), BF)
     copied = jax.ShapeDtypeStruct((16, 8, 512), BF)
     wide, rows, gains = call(
         first_kernel, (wide_shape, copied, jax.ShapeDtypeStruct((3, 1, 512), F32)), 1
     )(core_at, first_own, first_other)
-    came = half_step(wide, (((0, 736, FFL),), (middle_own, middle_other)))
+    came = half_step(wide, (((0, 0, FFL),), (down_own, down_other)))
     after_first, copies = call(residual_kernel(0.5), (shard, copied), 1)(shard_at, came, rows)
     copies = exchange(copies, "tp")
 

time: 257 us -> 256 us (level)
  blocking collectives: 143 us -> 134 us
  starting transfers between devices: 59.2 us -> 67.6 us
  waiting for transfers between devices: 29.9 us -> 33.9 us
  local copies, waits for them, and re-layouts: 7.02 us -> 4.26 us
    all_to_all x2 -> x1, blocking collectives: 24 us -> 14 us  [exchange(): return lax.all_to_all(parts, axis, split_axis=0, concat_axis=0, tiled=True)]
    all_to_all x4 -> x5, starting transfers between devices: 32.3 us -> 40.7 us  [exchange(): return lax.all_to_all(parts, axis, split_axis=0, concat_axis=0, tiled=True)]
    all_to_all x4 -> x5, waiting for transfers between devices: 13.5 us -> 16.3 us  [exchange(): return lax.all_to_all(parts, axis, split_axis=0, concat_axis=0, tiled=True)]
    unnamed x60 -> x40, local copies, waits for them, and re-layouts: 6.91 us -> 4.11 us
    all_gather x6 -> x8, blocking collectives: 34.5 us -> 36.9 us  [both_cores(): return lax.all_gather(array, 'c')]
  transfers between devices with their start and end apart: 9 -> 10, of which waited for: 5 -> 7; matrix products, arithmetic and copies ran while one was open for 1% -> 1% of each run, Pallas kernels for 2% -> 2%
where the time goes in v5:
time: 256 us; the launch traced here: 255 us
  blocking collectives  134 us (52%)
  starting transfers between devices  67.6 us (26%)
  waiting for transfers between devices  33.9 us (13%)
  Pallas kernels  11.5 us (4%)
  local copies, waits for them, and re-layouts  4.26 us (2%)
    all_to_all x4, blocking collectives, exchange(): lax.all_to_all(parts, ('zq', 'zp'), split_axis=0, concat_axis=0, axis_ind...  82.7 us
    all_to_all x5, starting transfers between devices, exchange(): return lax.all_to_all(parts, axis, split_axis=0, concat_axis=0, tiled=True)  40.7 us
    all_gather x8, blocking collectives, both_cores(): return lax.all_gather(array, 'c')  36.9 us
    all_to_all x5, waiting for transfers between devices, exchange(): return lax.all_to_all(parts, axis, split_axis=0, concat_axis=0, tiled=True)  16.3 us
    all_to_all x2, starting transfers between devices, exchange(): lax.all_to_all(parts, ('zq', 'zp'), split_axis=0, concat_axis=0, axis_ind...  14.3 us
    all_to_all x1, blocking collectives, exchange(): return lax.all_to_all(parts, axis, split_axis=0, concat_axis=0, tiled=True)  14 us
    ppermute x3, starting transfers between devices, swap(): return lax.ppermute(array, 'zp', [(0, 1), (1, 0)])  12.6 us
    ppermute x3, waiting for transfers between devices, swap(): return lax.ppermute(array, 'zp', [(0, 1), (1, 0)])  10.7 us
  transfers between devices with their start and end apart: 10, of which 7 were waited for; matrix products, arithmetic and copies ran while one was open for 1% of the time, Pallas kernels for 2%

profile of v5, /device:TPU:1, one launch (start us, length us, event | category | flops | bytes accessed | tf_op | source)
XLA Modules:
  0.0 254.9 jit_solution(15608958453695006786)
XLA Ops:
  0.7 0.6 copy-done.17
  1.3 0.9 copy-done.3
  2.3 0.9 copy-done.4
  3.2 0.9 copy-done.7
  4.1 1.0 prep.1
  5.1 4.4 %collective-permute-start = (bf16[1680,128]{1,0:T(8,128)(2,1)S(1)}, bf16[1680,128]{1,0:T(8,128)(2,1)S(1)}, u32[]{:S(2)}, u32[]{:S(2)}) collective-permute-start(bf16[1680,128]{1,0:T(8,128)(2,1)S(1)} %get-tuple-element.20), channel_id=1, source_target_pairs={{0,32},{32,0},{1,33},{33,1},{2,34},{34,2},{3,35},{35,3},{4,36},{36... | collective-permute-start | bytes 1290248 | tf_op jit(solution)/shard_map/ppermute | solution.py:26
  9.5 6.4 %all-gather = bf16[3360,128]{1,0:T(8,128)(2,1)S(1)} all-gather(bf16[1680,128]{1,0:T(8,128)(2,1)S(1)} %get-tuple-element.19), channel_id=2, replica_groups=mesh['zq'=8,'zp'=2,'c'=2,'tp'=16] {'c'}, dimensions={0}, use_global_device_ids=true | all-gather | bytes 1290240 | tf_op jit(solution)/shard_map/all_gather | solution.py:30
  16.0 8.1 %all-gather.1 = bf16[3360,128]{1,0:T(8,128)(2,1)S(1)} all-gather(bf16[1680,128]{1,0:T(8,128)(2,1)S(1)} %collective-permute-done), channel_id=3, replica_groups=mesh['zq'=8,'zp'=2,'c'=2,'tp'=16] {'c'}, dimensions={0}, use_global_device_ids=true | all-gather | bytes 1290240 | tf_op jit(solution)/shard_map/all_gather | solution.py:30
  24.7 33.2 %all_to_all.60.x_ref = bf16[8,16,1408]{2,1,0:T(8,128)(2,1)S(1)} all-to-all(bf16[8,16,1408]{2,1,0:T(8,128)(2,1)S(1)} %bitcast.55), channel_id=1, replica_groups={{0,64,128,192,288,352,416,480},{32,96,160,224,256,320,384,448},{1,65,12..., dimensions={0} | all-to-all | bytes 720896 | tf_op jit(solution)/shard_map/all_to_all | solution.py:36
  57.9 0.9 shard_map.229
  58.7 4.9 %all-to-all-start.1 = ((bf16[8,16,688]{2,1,0:T(8,128)(2,1)}), bf16[8,16,688]{2,1,0:T(8,128)(2,1)S(1)}, u32[]{:S(2)}, u32[]{:S(2)}) async-start(bf16[8,16,688]{2,1,0:T(8,128)(2,1)} %shard_map.229), calls=%async_computation.1 | async-start | bytes 393216 | tf_op jit(solution)/shard_map/all_to_all | solution.py:36
  64.3 5.1 %collective-permute-start.1 = (bf16[1424,128]{1,0:T(8,128)(2,1)S(1)}, bf16[1424,128]{1,0:T(8,128)(2,1)S(1)}, u32[]{:S(2)}, u32[]{:S(2)}) collective-permute-start(bf16[1424,128]{1,0:T(8,128)(2,1)S(1)} %shard_map.230), channel_id=1, source_target_pairs={{0,32},{32,0},{1,33},{33,1},{2,34},{34,2},{3,35},{35,3},{4,36},{36... | collective-permute-start | bytes 1093640 | tf_op jit(solution)/shard_map/ppermute | solution.py:26
  69.4 3.2 %all-gather.2 = bf16[1376,128]{1,0:T(8,128)(2,1)S(1)} all-gather(bf16[688,128]{1,0:T(8,128)(2,1)S(1)} %copy-done.1), channel_id=4, replica_groups=mesh['zq'=8,'zp'=2,'c'=2,'tp'=16] {'c'}, dimensions={0}, use_global_device_ids=true | all-gather | bytes 528384 | tf_op jit(solution)/shard_map/all_gather | solution.py:30
  72.6 10.7 %collective-permute-done.1 = bf16[1424,128]{1,0:T(8,128)(2,1)S(1)} collective-permute-done((bf16[1424,128]{1,0:T(8,128)(2,1)S(1)}, bf16[1424,128]{1,0:T(8,128)(2,1)S(1)}, u32[]{:S(2)}, u32[]{:S(2)}) %collective-permute-start.1) | collective-permute-done | bytes 364576 | tf_op jit(solution)/shard_map/ppermute | solution.py:26
  83.3 2.6 %all-gather.3 = bf16[1376,128]{1,0:T(8,128)(2,1)S(1)} all-gather(bf16[688,128]{1,0:T(8,128)(2,1)S(1)} %slice.16), channel_id=5, replica_groups=mesh['zq'=8,'zp'=2,'c'=2,'tp'=16] {'c'}, dimensions={0}, use_global_device_ids=true | all-gather | bytes 528384 | tf_op jit(solution)/shard_map/all_gather | solution.py:30
  85.8 0.9 shard_map.231
  86.8 6.8 %all-to-all-start.2 = ((bf16[16,8,512]{2,1,0:T(8,128)(2,1)}), bf16[16,8,512]{2,1,0:T(8,128)(2,1)S(1)}, u32[]{:S(2)}, u32[]{:S(2)}) async-start(bf16[16,8,512]{2,1,0:T(8,128)(2,1)} %bitcast.17), calls=%async_computation.2 | async-start | bytes 262144 | tf_op jit(solution)/shard_map/all_to_all | solution.py:39
  93.6 6.8 %all-to-all-done.2.sum_ref = bf16[16,8,512]{2,1,0:T(8,128)(2,1)S(1)} async-done(((bf16[16,8,512]{2,1,0:T(8,128)(2,1)}), bf16[16,8,512]{2,1,0:T(8,128)(2,1)S(1)}, u32[]{:S(2)}, u32[]{:S(2)}) %all-to-all-start.2) | async-done | bytes 131104 | tf_op jit(solution)/shard_map/all_to_all | solution.py:39
  100.4 0.7 shard_map.232
  101.1 3.5 %all-to-all-start.3 = ((bf16[16,8,512]{2,1,0:T(8,128)(2,1)}), bf16[16,8,512]{2,1,0:T(8,128)(2,1)S(1)}, u32[]{:S(2)}, u32[]{:S(2)}) async-start(bf16[16,8,512]{2,1,0:T(8,128)(2,1)} %get-tuple-element.23), calls=%async_computation.3 | async-start | bytes 262144 | tf_op jit(solution)/shard_map/all_to_all | solution.py:39
  104.6 3.5 %all-gather.4 = bf16[1472,128]{1,0:T(8,128)(2,1)S(1)} all-gather(bf16[736,128]{1,0:T(8,128)(2,1)S(1)} %slice.17), channel_id=6, replica_groups=mesh['zq'=8,'zp'=2,'c'=2,'tp'=16] {'c'}, dimensions={0}, use_global_device_ids=true | all-gather | bytes 565248 | tf_op jit(solution)/shard_map/all_gather | solution.py:30
  108.1 2.2 all-gather.5
  110.3 1.1 all-to-all-done.3.x_ref
  111.4 0.9 shard_map.233
  112.3 9.4 %all-to-all-start.4 = ((bf16[8,16,640]{2,1,0:T(8,128)(2,1)}), bf16[8,16,640]{2,1,0:T(8,128)(2,1)S(1)}, u32[]{:S(2)}, u32[]{:S(2)}) async-start(bf16[8,16,640]{2,1,0:T(8,128)(2,1)} %bitcast.20), calls=%async_computation.4 | async-start | bytes 327680 | tf_op jit(solution)/shard_map/all_to_all | solution.py:36
  121.7 0.7 shard_map.237
  122.5 3.1 %collective-permute-start.2 = (bf16[2032,128]{1,0:T(8,128)(2,1)S(1)}, bf16[2032,128]{1,0:T(8,128)(2,1)}, u32[]{:S(2)}, u32[]{:S(2)}) collective-permute-start(bf16[2032,128]{1,0:T(8,128)(2,1)S(1)} %shard_map.237), channel_id=1, source_target_pairs={{0,32},{32,0},{1,33},{33,1},{2,34},{34,2},{3,35},{35,3},{4,36},{36... | collective-permute-start | bytes 1560584 | tf_op jit(solution)/shard_map/ppermute | solution.py:26
  126.2 6.9 %all-to-all-done.4.x_ref = bf16[8,16,640]{2,1,0:T(8,128)(2,1)S(1)} async-done(((bf16[8,16,640]{2,1,0:T(8,128)(2,1)}), bf16[8,16,640]{2,1,0:T(8,128)(2,1)S(1)}, u32[]{:S(2)}, u32[]{:S(2)}) %all-to-all-start.4) | async-done | bytes 163872 | tf_op jit(solution)/shard_map/all_to_all | solution.py:36
  133.1 0.6 copy-done.16
  133.8 1.2 shard_map.234
  135.0 15.2 %all_to_all.61.x_ref = bf16[8,16,128]{2,1,0:T(8,128)(2,1)S(1)} all-to-all(bf16[8,16,128]{2,1,0:T(8,128)(2,1)S(1)} %get-tuple-element.25), channel_id=1, replica_groups={{0,64,128,192,288,352,416,480},{32,96,160,224,256,320,384,448},{1,65,12..., dimensions={0} | all-to-all | bytes 65536 | tf_op jit(solution)/shard_map/all_to_all | solution.py:36
  150.1 0.8 shard_map.235
  151.0 7.5 %all-to-all-start.6 = ((bf16[16,8,512]{2,1,0:T(8,128)(2,1)}), bf16[16,8,512]{2,1,0:T(8,128)(2,1)S(1)}, u32[]{:S(2)}, u32[]{:S(2)}) async-start(bf16[16,8,512]{2,1,0:T(8,128)(2,1)} %bitcast.24), calls=%async_computation.6 | async-start | bytes 262144 | tf_op jit(solution)/shard_map/all_to_all | solution.py:39
  158.4 6.2 %all-gather.6 = bf16[4064,128]{1,0:T(8,128)(2,1)S(1)} all-gather(bf16[2032,128]{1,0:T(8,128)(2,1)S(1)} %shard_map.237), channel_id=8, replica_groups=mesh['zq'=8,'zp'=2,'c'=2,'tp'=16] {'c'}, dimensions={0}, use_global_device_ids=true | all-gather | bytes 1560576 | tf_op jit(solution)/shard_map/all_gather | solution.py:30
  164.6 0.7 all-to-all-done.6.sum_ref
  165.3 0.7 shard_map.236
  166.0 6.2 %all-to-all-start.7 = ((bf16[16,8,512]{2,1,0:T(8,128)(2,1)}), bf16[16,8,512]{2,1,0:T(8,128)(2,1)S(1)}, u32[]{:S(2)}, u32[]{:S(2)}) async-start(bf16[16,8,512]{2,1,0:T(8,128)(2,1)} %get-tuple-element.27), calls=%async_computation.7 | async-start | bytes 262144 | tf_op jit(solution)/shard_map/all_to_all | solution.py:39
  172.2 4.8 %all-gather.7 = bf16[4064,128]{1,0:T(8,128)(2,1)S(1)} all-gather(bf16[2032,128]{1,0:T(8,128)(2,1)} %collective-permute-done.2), channel_id=9, replica_groups=mesh['zq'=8,'zp'=2,'c'=2,'tp'=16] {'c'}, dimensions={0}, use_global_device_ids=true | all-gather | bytes 1560576 | tf_op jit(solution)/shard_map/all_gather | solution.py:30
  177.0 2.0 all-to-all-done.7.x_ref
  179.0 0.6 shard_map.238
  179.6 17.1 %all_to_all.62.x_ref = bf16[8,16,1408]{2,1,0:T(8,128)(2,1)S(1)} all-to-all(bf16[8,16,1408]{2,1,0:T(8,128)(2,1)S(1)} %bitcast.50), channel_id=1, replica_groups={{0,64,128,192,288,352,416,480},{32,96,160,224,256,320,384,448},{1,65,12..., dimensions={0} | all-to-all | bytes 720896 | tf_op jit(solution)/shard_map/all_to_all | solution.py:36
  196.9 17.3 %all_to_all.63.x_ref = bf16[8,16,688]{2,1,0:T(8,128)(2,1)S(1)} all-to-all(bf16[8,16,688]{2,1,0:T(8,128)(2,1)S(1)} %shard_map.239), channel_id=1, replica_groups={{0,64,128,192,288,352,416,480},{32,96,160,224,256,320,384,448},{1,65,12..., dimensions={0} | all-to-all | bytes 352256 | tf_op jit(solution)/shard_map/all_to_all | solution.py:36
  214.5 14.0 %all_to_all.64.sum_ref = bf16[16,8,512]{2,1,0:T(8,128)(2,1)S(1)} all-to-all(bf16[16,8,512]{2,1,0:T(8,128)(2,1)S(1)} %bitcast.53), channel_id=1, replica_groups=mesh['zq'=8,'zp'=2,'c'=2,'tp'=16] {'tp'}, dimensions={0} | all-to-all | bytes 262144 | tf_op jit(solution)/shard_map/all_to_all | solution.py:39
  228.5 0.7 shard_map.241
  229.2 16.7 %all-to-all-start.11 = ((bf16[64,8,128]{2,1,0:T(8,128)(2,1)}), bf16[64,8,128]{2,1,0:T(8,128)(2,1)S(1)}, u32[]{:S(2)}, u32[]{:S(2)}) async-start(bf16[64,8,128]{2,1,0:T(8,128)(2,1)} %shard_map.241), calls=%async_computation.11 | async-start | bytes 262144 | tf_op jit(solution)/shard_map/all_to_all | solution.py:39
  246.0 2.6 %multiply_add_fusion = f32[16,1,128,128]{3,2,1,0:T(8,128)} fusion(f32[16,1,128,128]{3,2,1,0:T(8,128)} %param.34, f32[16,128]{1,0:T(8,128)S(1)} %get-tuple-element.31, f32[16,128]{1,0:T(8,128)S(1)} %get-tuple-element.30, f32[16]{0:T(128)S(1)} %slice_reduce_fusion), kind=kLoop, calls=%fused_computation | loop fusion | flops 786432 | bytes 2113600 | tf_op jit(solution)/shard_map/add | solution.py:450
  248.6 5.7 %all-to-all-done.11 = bf16[64,8,128]{2,1,0:T(8,128)(2,1)S(1)} async-done(((bf16[64,8,128]{2,1,0:T(8,128)(2,1)}), bf16[64,8,128]{2,1,0:T(8,128)(2,1)S(1)}, u32[]{:S(2)}, u32[]{:S(2)}) %all-to-all-start.11) | async-done | bytes 131104 | tf_op jit(solution)/shard_map/all_to_all | solution.py:39
  254.3 0.7 shard_map.242
  (46 shorter events, 1.9 us)
Async XLA Ops:
  0.6 0.7 copy-start.17
  0.7 0.7 copy-start.18
  0.7 0.7 copy-start.19
  1.3 0.9 copy-start.3
  2.3 0.9 copy-start.4
  3.2 0.9 copy-start.7
  5.1 10.8 %collective-permute-start = (bf16[1680,128]{1,0:T(8,128)(2,1)S(1)}, bf16[1680,128]{1,0:T(8,128)(2,1)S(1)}, u32[]{:S(2)}, u32[]{:S(2)}) collective-permute-start(bf16[1680,128]{1,0:T(8,128)(2,1)S(1)} %get-tuple-element.20), channel_id=1, source_target_pairs={{0,32},{32,0},{1,33},{33,1},{2,34},{34,2},{3,35},{35,3},{4,36},{36... | collective-permute-start | bytes 1290248 | tf_op jit(solution)/shard_map/ppermute | solution.py:26
  57.8 5.8 %copy-start.9 = (bf16[128,128]{1,0:T(8,128)(2,1)S(1)}, bf16[128,128]{1,0:T(8,128)(2,1)}, u32[]{:S(2)}) copy-start(bf16[128,128]{1,0:T(8,128)(2,1)} %refs_1_.1) | copy-start | bytes 98308
  57.8 5.8 %copy-start.10 = (bf16[128,128]{1,0:T(8,128)(2,1)S(1)}, bf16[128,128]{1,0:T(8,128)(2,1)}, u32[]{:S(2)}) copy-start(bf16[128,128]{1,0:T(8,128)(2,1)} %refs_2_.2) | copy-start | bytes 98308
  57.9 5.8 %copy-start.11 = (bf16[128,128]{1,0:T(8,128)(2,1)S(1)}, bf16[128,128]{1,0:T(8,128)(2,1)}, u32[]{:S(2)}) copy-start(bf16[128,128]{1,0:T(8,128)(2,1)} %refs_3_.1) | copy-start | bytes 98308
  57.9 5.8 %copy-start.12 = (bf16[128,128]{1,0:T(8,128)(2,1)S(1)}, bf16[128,128]{1,0:T(8,128)(2,1)}, u32[]{:S(2)}) copy-start(bf16[128,128]{1,0:T(8,128)(2,1)} %refs_6_.1) | copy-start | bytes 98308
  58.7 5.0 %copy-start.1 = (bf16[688,128]{1,0:T(8,128)(2,1)S(1)}, bf16[688,128]{1,0:T(8,128)(2,1)}, u32[]{:S(2)}) copy-start(bf16[688,128]{1,0:T(8,128)(2,1)} %refs_8_.1) | copy-start | bytes 528388
  58.7 5.0 %copy-start.2 = (bf16[688,128]{1,0:T(8,128)(2,1)S(1)}, bf16[688,128]{1,0:T(8,128)(2,1)}, u32[]{:S(2)}) copy-start(bf16[688,128]{1,0:T(8,128)(2,1)} %refs_2_.3) | copy-start | bytes 528388
  58.7 5.0 %copy-start.8 = (bf16[128,128]{1,0:T(8,128)(2,1)S(1)}, bf16[128,128]{1,0:T(8,128)(2,1)}, u32[]{:S(2)}) copy-start(bf16[128,128]{1,0:T(8,128)(2,1)} %refs_0_.1) | copy-start | bytes 98308
  58.7 5.0 %copy-start.14 = (bf16[128,16]{0,1:T(8,128)(2,1)S(1)}, bf16[128,16]{0,1:T(8,128)(2,1)}, u32[]{:S(2)}) copy-start(bf16[128,16]{0,1:T(8,128)(2,1)} %param.31) | copy-start | bytes 12292
  58.7 5.0 %copy-start.15 = (bf16[128,16]{0,1:T(8,128)(2,1)S(1)}, bf16[128,16]{0,1:T(8,128)(2,1)}, u32[]{:S(2)}) copy-start(bf16[128,16]{0,1:T(8,128)(2,1)} %param.32) | copy-start | bytes 12292
  58.7 27.1 %all-to-all-start.1 = ((bf16[8,16,688]{2,1,0:T(8,128)(2,1)}), bf16[8,16,688]{2,1,0:T(8,128)(2,1)S(1)}, u32[]{:S(2)}, u32[]{:S(2)}) async-start(bf16[8,16,688]{2,1,0:T(8,128)(2,1)} %shard_map.229), calls=%async_computation.1 | async-start | bytes 393216 | tf_op jit(solution)/shard_map/all_to_all | solution.py:36
  64.3 19.0 %collective-permute-start.1 = (bf16[1424,128]{1,0:T(8,128)(2,1)S(1)}, bf16[1424,128]{1,0:T(8,128)(2,1)S(1)}, u32[]{:S(2)}, u32[]{:S(2)}) collective-permute-start(bf16[1424,128]{1,0:T(8,128)(2,1)S(1)} %shard_map.230), channel_id=1, source_target_pairs={{0,32},{32,0},{1,33},{33,1},{2,34},{34,2},{3,35},{35,3},{4,36},{36... | collective-permute-start | bytes 1093640 | tf_op jit(solution)/shard_map/ppermute | solution.py:26
  86.8 13.6 %all-to-all-start.2 = ((bf16[16,8,512]{2,1,0:T(8,128)(2,1)}), bf16[16,8,512]{2,1,0:T(8,128)(2,1)S(1)}, u32[]{:S(2)}, u32[]{:S(2)}) async-start(bf16[16,8,512]{2,1,0:T(8,128)(2,1)} %bitcast.17), calls=%async_computation.2 | async-start | bytes 262144 | tf_op jit(solution)/shard_map/all_to_all | solution.py:39
  101.1 10.3 %all-to-all-start.3 = ((bf16[16,8,512]{2,1,0:T(8,128)(2,1)}), bf16[16,8,512]{2,1,0:T(8,128)(2,1)S(1)}, u32[]{:S(2)}, u32[]{:S(2)}) async-start(bf16[16,8,512]{2,1,0:T(8,128)(2,1)} %get-tuple-element.23), calls=%async_computation.3 | async-start | bytes 262144 | tf_op jit(solution)/shard_map/all_to_all | solution.py:39
  108.1 13.6 %copy-start.6 = (bf16[128,688]{0,1:T(8,128)(2,1)S(1)}, bf16[128,688]{0,1:T(8,128)(2,1)}, u32[]{:S(2)}) copy-start(bf16[128,688]{0,1:T(8,128)(2,1)} %param.40) | copy-start | bytes 528388
  111.4 21.7 %copy-start = (f32[16,1,128,128]{3,2,1,0:T(8,128)S(1)}, f32[16,1,128,128]{3,2,1,0:T(8,128)}, u32[]{:S(2)}) copy-start(f32[16,1,128,128]{3,2,1,0:T(8,128)} %param.34) | copy-start | bytes 3145732
  112.3 9.4 %copy-start.5 = (bf16[128,688]{0,1:T(8,128)(2,1)S(1)}, bf16[128,688]{0,1:T(8,128)(2,1)}, u32[]{:S(2)}) copy-start(bf16[128,688]{0,1:T(8,128)(2,1)} %param.39) | copy-start | bytes 528388
  112.3 20.8 %all-to-all-start.4 = ((bf16[8,16,640]{2,1,0:T(8,128)(2,1)}), bf16[8,16,640]{2,1,0:T(8,128)(2,1)S(1)}, u32[]{:S(2)}, u32[]{:S(2)}) async-start(bf16[8,16,640]{2,1,0:T(8,128)(2,1)} %bitcast.20), calls=%async_computation.4 | async-start | bytes 327680 | tf_op jit(solution)/shard_map/all_to_all | solution.py:36
  121.7 11.4 %copy-start.13 = (f32[16,1,128]{2,1,0:T(1,128)S(1)}, f32[16,1,128]{2,1,0:T(1,128)}, u32[]{:S(2)}) copy-start(f32[16,1,128]{2,1,0:T(1,128)} %param.35) | copy-start | bytes 24580
  122.5 49.7 %collective-permute-start.2 = (bf16[2032,128]{1,0:T(8,128)(2,1)S(1)}, bf16[2032,128]{1,0:T(8,128)(2,1)}, u32[]{:S(2)}, u32[]{:S(2)}) collective-permute-start(bf16[2032,128]{1,0:T(8,128)(2,1)S(1)} %shard_map.237), channel_id=1, source_target_pairs={{0,32},{32,0},{1,33},{33,1},{2,34},{34,2},{3,35},{35,3},{4,36},{36... | collective-permute-start | bytes 1560584 | tf_op jit(solution)/shard_map/ppermute | solution.py:26
  133.1 0.7 copy-start.16
  151.0 14.3 %all-to-all-start.6 = ((bf16[16,8,512]{2,1,0:T(8,128)(2,1)}), bf16[16,8,512]{2,1,0:T(8,128)(2,1)S(1)}, u32[]{:S(2)}, u32[]{:S(2)}) async-start(bf16[16,8,512]{2,1,0:T(8,128)(2,1)} %bitcast.24), calls=%async_computation.6 | async-start | bytes 262144 | tf_op jit(solution)/shard_map/all_to_all | solution.py:39
  166.0 13.1 %all-to-all-start.7 = ((bf16[16,8,512]{2,1,0:T(8,128)(2,1)}), bf16[16,8,512]{2,1,0:T(8,128)(2,1)S(1)}, u32[]{:S(2)}, u32[]{:S(2)}) async-start(bf16[16,8,512]{2,1,0:T(8,128)(2,1)} %get-tuple-element.27), calls=%async_computation.7 | async-start | bytes 262144 | tf_op jit(solution)/shard_map/all_to_all | solution.py:39
  229.2 25.1 %all-to-all-start.11 = ((bf16[64,8,128]{2,1,0:T(8,128)(2,1)}), bf16[64,8,128]{2,1,0:T(8,128)(2,1)S(1)}, u32[]{:S(2)}, u32[]{:S(2)}) async-start(bf16[64,8,128]{2,1,0:T(8,128)(2,1)} %shard_map.241), calls=%async_computation.11 | async-start | bytes 262144 | tf_op jit(solution)/shard_map/all_to_all | solution.py:39
